TPU v7x, 512 devices: a whole 4x8x8 slice. The times are simulated.
512 devices in a mesh: sp: 64 (over z, y), tp: 4 (over x), dp: 2 (over core).
Axes of the slice: x: 4, y: 8, z: 8, core: 2. Of those that a mesh axis runs over, the one named last changes fastest.
Arguments:
- latent: bfloat16 [2, 8192, 2048], P('dp', ('sp', 'tp')), may hold values from -10 to 10
- condition: bfloat16 [2, 2048], P('dp'), may hold values from -6 to 6
- context: bfloat16 [2, 512, 2048], P('dp', 'sp'), may hold values from -6 to 6
- context_source: bfloat16 [2048], replicated, may hold values from -6 to 6
- mod_weight: bfloat16 [3, 2048, 2048], P(None, 'sp', 'tp'), may hold values from -0.125 to 0.125
- norm_gain: bfloat16 [2048], replicated, may hold values from 0.099609375 to 1.8984375
- w_x: bfloat16 [2048, 2048], P('dp', 'tp'), may hold values from -0.125 to 0.125
- w_b: bfloat16 [2048, 512], P('dp', 'tp'), may hold values from -0.125 to 0.125
- w_c: bfloat16 [2048, 512], P('dp', 'tp'), may hold values from -0.125 to 0.125
- w_z: bfloat16 [2048, 2048], P('dp', 'tp'), may hold values from -0.125 to 0.125
- w_dt: bfloat16 [2, 2048, 32], P(None, 'dp', 'tp'), may hold values from -0.125 to 0.125
- conv_x: bfloat16 [3, 2048], P(None, 'tp'), may hold values from -3.5 to 3.5
- conv_b: bfloat16 [3, 512], P(None, 'tp'), may hold values from -3.5 to 3.5
- conv_c: bfloat16 [3, 512], P(None, 'tp'), may hold values from -3.5 to 3.5
- decay_rate: float32 [2, 32], P(None, 'tp'), may hold values from 0 to 1, as said below
- out_gain: bfloat16 [2048], P('tp'), may hold values from 0.099609375 to 1.8984375
- w_out: bfloat16 [2048, 2048], P(('tp', 'dp')), may hold values from -0.125 to 0.125
Outputs:
- update: bfloat16 [2, 8192, 2048], P('dp', ('sp', 'tp'))
Inputs may be any that keep to these rules, and one draw needn't show every extreme that they name: `decay_rate`: positive rates.
All inputs are finite; a program needn't handle non-finite values.
Results may differ from a plain program's by a relative error of at most 0.014.
Values may be sent and summed in bfloat16 or wider, within the bound.
No kernel may reach another device: no remote copies, remote signals or barrier semaphores. Data moves between devices by JAX's collectives and lax.ppermute only.
A program may use at most 128 MiB of HBM per device.

v0:
```python
import functools

import jax
import jax.numpy as jnp
from jax import lax
from jax.sharding import Mesh
from jax.sharding import PartitionSpec as P

STATE = 128
BLOCK = 128
SP = ("sp_0", "sp_1")
SP_TP = ("sp_0", "sp_1", "tp")


EPSILON = 1e-06


def over_axes(x, axes):
    return functools.reduce(lax.psum, axes, x)


def laid_out(tiles, dim):
    tiles = jnp.moveaxis(tiles, 0, dim)
    dims = tiles.shape
    return tiles.reshape(*dims[:dim], dims[dim] * dims[dim + 1], *dims[dim + 2 :])


def sent_to_all(x, axis):
    peers = lax.axis_size(axis)
    return lax.all_to_all(jnp.broadcast_to(x[None], (peers, *x.shape)), axis, 0, 0, tiled=True)


def gather_directly(x, axis, dim):
    return laid_out(sent_to_all(x, axis), dim)


def sent_together(arrays, axis, dim, along):
    ends, at = ([], 0)
    for a in arrays[:-1]:
        at += a.shape[along]
        ends.append(at)
    both = jnp.concatenate(arrays, axis=along)
    return tuple(jnp.split(lax.all_gather(both, axis, axis=dim, tiled=True), ends, axis=along))


def with_halo(x, sides, width):
    for axis, dim in sides:
        peers, length = (lax.axis_size(axis), x.shape[dim])
        up = [(i, (i + 1) % peers) for i in range(peers - 1)]
        down = [(j, i) for i, j in up]
        last = lax.slice_in_dim(x, length - width, length, axis=dim)
        leading = lax.slice_in_dim(x, 0, width, axis=dim)
        before = lax.ppermute(last, axis, up)
        after = lax.ppermute(leading, axis, down)
        x = jnp.concatenate([before, x, after], axis=dim)
    return x


def neutral_like(x, identity):
    return jax.tree.map(
        lambda a, e: jnp.broadcast_to(jnp.asarray(e, a.dtype), a.shape), x, identity
    )


def entering_2(x, axes, combine, identity, reverse):
    before = start = neutral_like(x, identity)
    total = x
    for axis in reversed(axes):
        peers, place = (lax.axis_size(axis), lax.axis_index(axis))
        pieces = jax.tree.map(
            lambda part, kind: lax.all_gather(part.astype(kind), axis),
            total,
            (jnp.bfloat16, jnp.bfloat16),
        )
        inside, total = (start, start)
        for k in reversed(range(peers)) if reverse else range(peers):
            passed = k > place if reverse else k < place
            total = combine(
                total, jax.tree.map(lambda part, own: part[k].astype(own.dtype), pieces, x)
            )
            inside = jax.tree.map(lambda new, old: jnp.where(passed, new, old), total, inside)
        before = combine(inside, before)
    return before


def split_up(x, dim, peers):
    before, after = (x.shape[:dim], x.shape[dim + 1 :])
    return jnp.moveaxis(x.reshape(*before, peers, -1, *after), dim, 0)


def sum_at_owner(x, axis, dim):
    peers = lax.axis_size(axis)
    tiles = lax.all_to_all(split_up(x, dim, peers), axis, 0, 0, tiled=True)
    return jnp.sum(tiles.astype(jnp.float32), axis=0)


def rounded(values):
    return lax.optimization_barrier(values.astype(jnp.bfloat16)).astype(jnp.float32)


def modulated(source, gain_vec, shift_vec, scale_vec):
    values = source.astype(jnp.float32)
    normed = values * lax.rsqrt(jnp.mean(values * values, axis=-1, keepdims=True) + EPSILON)
    return (normed * gain_vec.astype(jnp.float32) * (1.0 + scale_vec) + shift_vec).astype(
        jnp.bfloat16
    )


def convolved(padded, weight, total_rows):
    wide_vals = padded.astype(jnp.float32)
    tap_weights = weight.astype(jnp.float32)
    summed = jnp.zeros((total_rows, wide_vals.shape[1]), jnp.float32)
    for offset in range(weight.shape[0]):
        summed = summed + wide_vals[offset : offset + total_rows] * tap_weights[offset]
    return jax.nn.silu(summed).astype(jnp.bfloat16)


def final_state(x_vals, b_vals, step_size, rate_head, groups):
    total_rows, head_count = step_size.shape
    per_group = head_count // groups
    moved_x = rounded(
        x_vals.reshape(total_rows, head_count, -1).astype(jnp.float32) * step_size[:, :, None]
    )
    running = jnp.cumsum(-rate_head * step_size, axis=0)
    weight = jnp.exp(running[-1:] - running)
    scaled = (moved_x * weight[:, :, None]).reshape(total_rows, groups, per_group, -1)
    b_wide = b_vals.reshape(total_rows, groups, -1).astype(jnp.float32)
    ctx_state = jnp.einsum("sgn,sghp->ghpn", b_wide, scaled)
    return (ctx_state, running[-1].reshape(groups, per_group))


def combine_states(earlier, later_part):
    return (
        earlier[0] + later_part[0],
        earlier[1] * jnp.exp(later_part[0])[:, :, None, None] + later_part[1],
    )


def direction_terms(x_vals, b_vals, c_vals, step_size, rate_head, groups):
    total_rows, head_count = step_size.shape
    per_group = head_count // groups
    blocks = total_rows // BLOCK
    moved_x = (
        x_vals.reshape(total_rows, head_count, -1).astype(jnp.float32) * step_size[:, :, None]
    ).astype(jnp.bfloat16)
    head_dim = moved_x.shape[2]
    x_blocks = moved_x.reshape(blocks, BLOCK, groups, per_group, head_dim)
    b_blocks = b_vals.reshape(blocks, BLOCK, groups, -1)
    c_blocks = c_vals.reshape(blocks, BLOCK, groups, -1)
    running = jnp.cumsum((-rate_head * step_size).reshape(blocks, BLOCK, head_count), axis=1)
    across = jnp.swapaxes(running, 1, 2)
    spread = across[:, :, :, None] - across[:, :, None, :]
    lower_part = lax.broadcasted_iota(jnp.int32, (BLOCK, BLOCK), 0) >= lax.broadcasted_iota(
        jnp.int32, (BLOCK, BLOCK), 1
    )
    decay_mask = jnp.where(lower_part, jnp.exp(jnp.minimum(spread, 0.0)), 0.0).reshape(
        blocks, groups, per_group, BLOCK, BLOCK
    )
    scores = jnp.einsum("clgn,csgn->cgls", c_blocks, b_blocks, preferred_element_type=jnp.float32)
    weights = (scores[:, :, None] * decay_mask).astype(jnp.bfloat16)
    inside = jnp.einsum("cghls,csghp->clghp", weights, x_blocks, preferred_element_type=jnp.float32)
    to_end = jnp.exp(running[:, -1:, :] - running).reshape(blocks, BLOCK, groups, per_group, 1)
    x_end = (x_blocks.astype(jnp.float32) * to_end).astype(jnp.bfloat16)
    fresh_state = jnp.einsum(
        "csgn,csghp->cghpn", b_blocks, x_end, preferred_element_type=jnp.float32
    )
    totals = running[:, -1, :].reshape(blocks, groups, per_group)

    def advance(carried_in, inputs):
        return (carried_in * jnp.exp(inputs[1])[:, :, None, None] + inputs[0], carried_in)

    ending, before = lax.scan(
        advance, jnp.zeros(fresh_state.shape[1:], jnp.float32), (fresh_state, totals)
    )
    return (inside, before, ending, totals, running, c_blocks)


def direction_output(terms, incoming):
    inside, before, ending, totals, running, c_blocks = terms
    blocks, length, groups, per_group, head_dim = inside.shape
    offset_sum = jnp.cumsum(totals, axis=0) - totals
    entering = before + jnp.exp(offset_sum)[:, :, :, None, None] * incoming[None]
    carried = jnp.einsum(
        "clgn,cghpn->clghp",
        c_blocks,
        entering.astype(jnp.bfloat16),
        preferred_element_type=jnp.float32,
    )
    growth = jnp.exp(running).reshape(blocks, length, groups, per_group, 1)
    return (inside + growth * carried).reshape(blocks * length, -1)


def shards(
    latent,
    condition,
    context,
    context_source,
    mod_weight,
    norm_gain,
    w_x,
    w_b,
    w_c,
    w_z,
    w_dt,
    conv_x,
    conv_b,
    conv_c,
    decay_rate,
    out_gain,
    w_out,
):
    row_count = mod_weight.shape[1]
    activations = jnp.stack(
        [
            jax.nn.silu(condition[0].astype(jnp.float32)),
            jax.nn.silu(context_source.astype(jnp.float32)),
        ]
    ).astype(jnp.bfloat16)
    own_rows = lax.dynamic_slice_in_dim(activations, lax.axis_index(SP) * row_count, row_count, 1)
    partial_value = jnp.einsum(
        "ar,krc->kac", own_rows, mod_weight, preferred_element_type=jnp.float32
    )
    summed = over_axes(partial_value, SP)
    mod_vectors = gather_directly(summed, "tp", 2)
    full_x, full_b, full_c, full_z, full_fwd, full_bwd, full_out = (
        *sent_together((w_x, w_b, w_c, w_z, w_dt[0], w_dt[1]), "dp", 0, 1),
        lax.all_gather(w_out, "dp", axis=0, tiled=True),
    )
    inner_cols = full_x.shape[1]
    gn_cols = full_b.shape[1]
    head_count = full_fwd.shape[1]
    groups = gn_cols // STATE
    mixed_cols = inner_cols + gn_cols
    reach_rows = conv_x.shape[0] // 2
    rate_fwd = decay_rate[0]
    rate_bwd = decay_rate[1]
    all_weights = jnp.concatenate([full_x, full_b, full_c, full_fwd, full_bwd, full_z], axis=1)
    ctx_weight = jnp.concatenate([full_x, full_b, full_fwd, full_bwd], axis=1)
    taps_all = jnp.concatenate([conv_x, conv_b, conv_c], axis=1)
    ctx_taps = jnp.concatenate([conv_x, conv_b], axis=1)
    ctx_rows = modulated(context[0], norm_gain, mod_vectors[0, 1], mod_vectors[1, 1])
    own_features = jnp.dot(ctx_rows, ctx_weight, preferred_element_type=jnp.float32).astype(
        jnp.bfloat16
    )
    features = gather_directly(own_features, SP, 0)
    total_rows = features.shape[0]
    padded = jnp.pad(features[:, :mixed_cols], ((reach_rows, reach_rows), (0, 0)))
    smoothed = convolved(padded, ctx_taps, total_rows)
    step_size = jax.nn.softplus(features[:, mixed_cols:].astype(jnp.float32))
    ctx_x = smoothed[:, :inner_cols]
    ctx_b = smoothed[:, inner_cols:]
    state_fwd, _ = final_state(ctx_x, ctx_b, step_size[:, :head_count], rate_fwd, groups)
    state_bwd, _ = final_state(
        jnp.flip(ctx_x, 0),
        jnp.flip(ctx_b, 0),
        jnp.flip(step_size[:, head_count:], 0),
        rate_bwd,
        groups,
    )
    latent_rows = modulated(latent[0], norm_gain, mod_vectors[0, 0], mod_vectors[1, 0])
    features = jnp.dot(
        gather_directly(latent_rows, "tp", 0), all_weights, preferred_element_type=jnp.float32
    ).astype(jnp.bfloat16)
    total_rows = features.shape[0]
    padded = with_halo(features[:, : mixed_cols + gn_cols], ((SP, 0),), reach_rows)
    smoothed = convolved(padded, taps_all, total_rows)
    x_vals = smoothed[:, :inner_cols]
    b_vals = smoothed[:, inner_cols:mixed_cols]
    c_vals = smoothed[:, mixed_cols:]
    base_col = mixed_cols + gn_cols
    step_size = jax.nn.softplus(
        features[:, base_col : base_col + 2 * head_count].astype(jnp.float32)
    )
    gate_in = features[:, base_col + 2 * head_count :]
    forward_terms = direction_terms(
        x_vals, b_vals, c_vals, step_size[:, :head_count], rate_fwd, groups
    )
    backward_terms = direction_terms(
        jnp.flip(x_vals, 0),
        jnp.flip(b_vals, 0),
        jnp.flip(c_vals, 0),
        jnp.flip(step_size[:, head_count:], 0),
        rate_bwd,
        groups,
    )
    fwd_total = jnp.sum(forward_terms[3], axis=0)
    bwd_total = jnp.sum(backward_terms[3], axis=0)
    empty = (jnp.zeros_like(fwd_total), jnp.zeros_like(forward_terms[2]))
    prefix_decay, prefix_state = entering_2(
        (fwd_total, forward_terms[2]), SP, combine_states, empty, False
    )
    suffix_decay, suffix_state = entering_2(
        (bwd_total, backward_terms[2]), SP, combine_states, empty, True
    )
    out_fwd = direction_output(
        forward_terms, prefix_state + jnp.exp(prefix_decay)[:, :, None, None] * state_fwd
    )
    out_bwd = jnp.flip(
        direction_output(
            backward_terms, suffix_state + jnp.exp(suffix_decay)[:, :, None, None] * state_bwd
        ),
        0,
    )
    gated = (out_fwd + out_bwd) * jax.nn.silu(gate_in.astype(jnp.float32))
    grouped = gated.reshape(total_rows, groups, -1)
    normed = (
        grouped
        * lax.rsqrt(jnp.mean(grouped * grouped, axis=-1, keepdims=True) + EPSILON)
        * out_gain.reshape(groups, -1).astype(jnp.float32)
    )
    normed_out = normed.reshape(total_rows, -1).astype(jnp.bfloat16)
    mixed = sum_at_owner(
        jnp.dot(normed_out, full_out, preferred_element_type=jnp.float32).astype(jnp.bfloat16),
        "tp",
        0,
    )
    return (mod_vectors[2, 0] * mixed).astype(jnp.bfloat16)[None]


def solution(mesh):
    torus = Mesh(
        mesh.devices.reshape(8, 8, mesh.shape["tp"], mesh.shape["dp"]), ("sp_0", "sp_1", "tp", "dp")
    )
    placed = (
        P("dp", SP_TP, None),
        P("dp", None),
        P("dp", SP, None),
        P(),
        P(None, SP, "tp"),
        P(),
        P("dp", "tp"),
        P("dp", "tp"),
        P("dp", "tp"),
        P("dp", "tp"),
        P(None, "dp", "tp"),
        P(None, "tp"),
        P(None, "tp"),
        P(None, "tp"),
        P(None, "tp"),
        P("tp"),
        P(("tp", "dp"), None),
    )
    return jax.shard_map(
        shards, mesh=torus, in_specs=placed, out_specs=P("dp", SP_TP, None), check_vma=False
    )
```

profile of v0, /device:TPU:1, one launch (start us, length us, event | category | flops | bytes accessed | tf_op | source)
XLA Modules:
  0.0 347.1 jit_solution(8498954441574411239)
XLA Ops:
  6.5 0.8 slice_bitcast_fusion.32
  7.7 5.4 %concatenate.20 = bf16[1024,1296]{1,0:T(8,128)(2,1)} concatenate(bf16[1024,512]{1,0:T(8,128)(2,1)} %param.23, bf16[1024,128]{1,0:T(8,128)(2,1)} %param.24, bf16[1024,128]{1,0:T(8,128)(2,1)} %param.25, bf16[1024,512]{1,0:T(8,128)(2,1)} %param.26, bf16[1024,8]{1,0:T(8,128)(2,1)S(1)} %copy.97, bf16[1024,8]{1,0:T(8,128)(2,1)S(1)} %copy.98), dimensions={1} | concatenate | bytes 5308416 | tf_op jit(solution)/shard_map/concatenate | solution.py:42
  14.0 29.8 %psum.14 = f32[3,2,512]{2,1,0:T(2,128)S(1)} all-reduce(f32[3,2,512]{2,1,0:T(2,128)S(1)} %convolution_bitcast_fusion.4), channel_id=1, replica_groups=mesh['sp_0'=8,'sp_1'=8,'tp'=4,'dp'=2] {'sp_0'}, use_global_device_ids=true, to_apply=%region_0.1 | all-reduce | flops 3072 | bytes 24576 | tf_op jit(solution)/shard_map/psum | solution.py:19
  43.8 23.1 %psum.15 = f32[3,2,512]{2,1,0:T(2,128)S(1)} all-reduce(f32[3,2,512]{2,1,0:T(2,128)S(1)} %psum.14), channel_id=1, replica_groups=mesh['sp_0'=8,'sp_1'=8,'tp'=4,'dp'=2] {'sp_1'}, use_global_device_ids=true, to_apply=%region_1.2 | all-reduce | flops 3072 | bytes 24576 | tf_op jit(solution)/shard_map/psum | solution.py:19
  67.5 4.0 %all-to-all-start = ((f32[4,3,2,512]{3,2,1,0:T(2,128)}), f32[4,3,2,512]{3,2,1,0:T(2,128)S(1)}, u32[]{:S(2)}, u32[]{:S(2)}) async-start(f32[4,3,2,512]{3,2,1,0:T(2,128)} %broadcast_in_dim.22), calls=%async_computation | async-start | bytes 98304 | tf_op jit(solution)/shard_map/all_to_all | solution.py:30
  71.7 4.2 %all-to-all-done = f32[4,3,2,512]{3,2,1,0:T(2,128)S(1)} async-done(((f32[4,3,2,512]{3,2,1,0:T(2,128)}), f32[4,3,2,512]{3,2,1,0:T(2,128)S(1)}, u32[]{:S(2)}, u32[]{:S(2)}) %all-to-all-start) | async-done | bytes 49184 | tf_op jit(solution)/shard_map/all_to_all | solution.py:30
  76.7 0.8 broadcast_in_dim.24
  77.5 4.1 %all-to-all-start.1 = ((bf16[4,32,2048]{2,1,0:T(8,128)(2,1)}), bf16[4,32,2048]{2,1,0:T(8,128)(2,1)}, u32[]{:S(2)}, u32[]{:S(2)}) async-start(bf16[4,32,2048]{2,1,0:T(8,128)(2,1)} %broadcast_in_dim.24), calls=%async_computation.1 | async-start | bytes 1048576 | tf_op jit(solution)/shard_map/all_to_all | solution.py:30
  81.9 1.9 split.19
  83.8 3.1 split.20
  86.8 2.1 split.18
  88.9 9.4 %concatenate.21 = bf16[2048,1296]{1,0:T(8,128)(2,1)} concatenate(bf16[2048,768]{1,0:T(8,128)(2,1)S(1)} %split.18, bf16[2048,16]{1,0:T(8,128)(2,1)} %split.19, bf16[2048,512]{1,0:T(8,128)(2,1)} %split.20), dimensions={1} | concatenate | bytes 10616832 | tf_op jit(solution)/shard_map/concatenate | solution.py:237
  98.3 5.1 %convolution_convert_fusion.1 = bf16[128,1296]{0,1:T(8,128)(2,1)S(1)} fusion(bf16[128,2048]{1,0:T(8,128)(2,1)} %bitcast.7, bf16[2048,1296]{1,0:T(8,128)(2,1)} %concatenate.21), kind=kOutput, calls=%fused_computation.5 | convolution fusion | flops 679643136 | bytes 6164480 | tf_op jit(solution)/shard_map/dot_general | solution.py:261
  104.8 1.7 collective-permute-start
  106.5 1.3 collective-permute-start.1
  109.1 3.8 %collective-permute-done.1 = bf16[1,768]{0,1:T(8,128)(2,1)S(1)} collective-permute-done((bf16[1,768]{0,1:T(8,128)(2,1)S(1)}, bf16[1,768]{0,1:T(8,128)(2,1)S(1)}, u32[]{:S(2)}, u32[]{:S(2)}) %collective-permute-start.1) | collective-permute-done | bytes 1568 | tf_op jit(solution)/shard_map/ppermute | solution.py:54
  113.8 0.8 slice_convert_fusion.34
  115.1 0.8 fusion.15
  117.6 0.8 fusion.14
  118.5 13.1 %all_gather.48 = bf16[8,1,8]{2,1,0:T(2,128)(2,1)S(1)} all-gather(bf16[1,1,8]{2,1,0:T(2,128)(2,1)S(1)} %slice.999), channel_id=1, replica_groups=mesh['sp_0'=8,'sp_1'=8,'tp'=4,'dp'=2] {'sp_1'}, dimensions={0}, use_global_device_ids=true | all-gather | bytes 144 | tf_op jit(solution)/shard_map/all_gather | solution.py:71
  131.7 35.6 %all-gather.19.cloned.1.call-done = bf16[64,64,128]{2,1,0:T(8,128)(2,1)} async-done(((bf16[8,64,128]{2,1,0:T(8,128)(2,1)}), bf16[64,64,128]{2,1,0:T(8,128)(2,1)}) %all-gather.19.cloned.1.call-update) | async-done | bytes 1048592 | tf_op jit(solution)/shard_map/all_gather | solution.py:71
  167.2 2.3 fusion.159
  169.6 11.2 %all_gather.43 = bf16[8,1,8]{2,1,0:T(2,128)(2,1)S(1)} all-gather(bf16[1,1,8]{2,1,0:T(2,128)(2,1)S(1)} %slice.1000), channel_id=1, replica_groups=mesh['sp_0'=8,'sp_1'=8,'tp'=4,'dp'=2] {'sp_1'}, dimensions={0}, use_global_device_ids=true | all-gather | bytes 144 | tf_op jit(solution)/shard_map/all_gather | solution.py:71
  180.9 28.2 %all-gather.17.cloned.1.call-done = bf16[64,64,128]{2,1,0:T(8,128)(2,1)} async-done(((bf16[8,64,128]{2,1,0:T(8,128)(2,1)}), bf16[64,64,128]{2,1,0:T(8,128)(2,1)}) %all-gather.17.cloned.1.call-update) | async-done | bytes 1048592 | tf_op jit(solution)/shard_map/all_gather | solution.py:71
  209.1 2.2 fusion.160
  213.4 13.5 %all_gather.49 = bf16[8,1,8]{2,1,0:T(2,128)(2,1)S(1)} all-gather(bf16[1,1,8]{2,1,0:T(2,128)(2,1)S(1)} %get-tuple-element.103), channel_id=1, replica_groups=mesh['sp_0'=8,'sp_1'=8,'tp'=4,'dp'=2] {'sp_0'}, dimensions={0}, use_global_device_ids=true | all-gather | bytes 144 | tf_op jit(solution)/shard_map/all_gather | solution.py:71
  227.6 10.5 %all_gather.44 = bf16[8,1,8]{2,1,0:T(2,128)(2,1)S(1)} all-gather(bf16[1,1,8]{2,1,0:T(2,128)(2,1)S(1)} %get-tuple-element.83), channel_id=1, replica_groups=mesh['sp_0'=8,'sp_1'=8,'tp'=4,'dp'=2] {'sp_0'}, dimensions={0}, use_global_device_ids=true | all-gather | bytes 144 | tf_op jit(solution)/shard_map/all_gather | solution.py:71
  238.8 1.7 slice-done
  241.2 1.0 broadcast_in_dim.26
  242.2 8.2 %all-to-all-start.2 = ((bf16[64,8,656]{2,1,0:T(8,128)(2,1)}), bf16[64,8,656]{2,1,0:T(8,128)(2,1)S(1)}, u32[]{:S(2)}, u32[]{:S(2)}) async-start(bf16[64,8,656]{2,1,0:T(8,128)(2,1)} %broadcast_in_dim.26), calls=%async_computation.2 | async-start | bytes 1572864 | tf_op jit(solution)/shard_map/all_to_all | solution.py:30
  253.8 0.8 fusion.320
  254.6 0.8 fusion.332
  255.4 11.4 %all-to-all-done.2 = bf16[64,8,656]{2,1,0:T(8,128)(2,1)S(1)} async-done(((bf16[64,8,656]{2,1,0:T(8,128)(2,1)}), bf16[64,8,656]{2,1,0:T(8,128)(2,1)S(1)}, u32[]{:S(2)}, u32[]{:S(2)}) %all-to-all-start.2) | async-done | bytes 671776 | tf_op jit(solution)/shard_map/all_to_all | solution.py:30
  267.8 1.0 slice_convert_fusion.35
  269.4 1.1 reduce-window.14
  271.9 1.1 reduce-window.16
  273.2 0.7 add_bitcast_fusion
  273.9 1.3 rev.37
  275.5 1.7 multiply_convert_fusion.2
  277.3 6.3 %rev.35 = bf16[512,512]{1,0:T(8,128)(2,1)S(1)} reverse(bf16[512,512]{1,0:T(8,128)(2,1)} %get-tuple-element.48), dimensions={0} | reverse | bytes 1048576 | tf_op jit(solution)/shard_map/jit(_flip)/rev | solution.py:254
  284.7 3.3 fusion.13
  288.1 1.3 fusion.6
  289.7 10.8 %all-gather.11.cloned.1.call-done = bf16[8,1,8,64,128]{4,3,2,1,0:T(8,128)(2,1)} async-done(((bf16[1,1,8,64,128]{4,3,2,1,0:T(8,128)(2,1)}), bf16[8,1,8,64,128]{4,3,2,1,0:T(8,128)(2,1)}) %all-gather.11.cloned.1.call-update) | async-done | bytes 1048592 | tf_op jit(solution)/shard_map/all_gather | solution.py:71
  300.8 2.6 fusion.12
  303.9 21.7 %all-gather.15.cloned.1.call-done = bf16[512,2048]{1,0:T(8,128)(2,1)} async-done(((bf16[256,2048]{1,0:T(8,128)(2,1)}), bf16[512,2048]{1,0:T(8,128)(2,1)}) %all-gather.15.cloned.1.call-update) | async-done | bytes 2097168 | tf_op jit(solution)/shard_map/all_gather | solution.py:227
  325.5 2.1 convolution_convert_fusion
  327.7 11.9 %all_to_all.20 = bf16[4,32,2048]{2,1,0:T(8,128)(2,1)S(1)} all-to-all(bf16[4,32,2048]{2,1,0:T(8,128)(2,1)S(1)} %bitcast.494), channel_id=1, replica_groups=mesh['sp_0'=8,'sp_1'=8,'tp'=4,'dp'=2] {'tp'}, dimensions={0} | all-to-all | bytes 1048576 | tf_op jit(solution)/shard_map/all_to_all | solution.py:93
  339.6 0.7 fusion.120
  (271 shorter events, 21.2 us)
Async XLA Ops:
  6.5 75.3 %all-gather.9.cloned.1.call-start = ((), (), s32[]{:S(2)}) async-start(), calls=%async_computation.4 | async-start | bytes 8650752 | tf_op jit(solution)/shard_map/all_gather | solution.py:43
  13.1 58.5 %copy-start.3 = (bf16[1,32,2048]{2,1,0:T(8,128)(2,1)S(1)}, bf16[1,32,2048]{2,1,0:T(8,128)(2,1)}, u32[]{:S(2)}) copy-start(bf16[1,32,2048]{2,1,0:T(8,128)(2,1)} %param.17) | copy-start | bytes 393220
  13.1 58.6 %copy-start.25 = (bf16[2048]{0:T(1024)(128)(2,1)S(1)}, bf16[2048]{0:T(1024)(128)(2,1)}, u32[]{:S(2)}) copy-start(bf16[2048]{0:T(1024)(128)(2,1)} %param.22) | copy-start | bytes 12292
  13.1 68.6 %copy-start.15 = (bf16[3,512]{1,0:T(4,128)(2,1)S(1)}, bf16[3,512]{1,0:T(4,128)(2,1)}, u32[]{:S(2)}) copy-start(bf16[3,512]{1,0:T(4,128)(2,1)} %param.28) | copy-start | bytes 9220
  13.1 68.6 %copy-start.30 = (bf16[3,128]{1,0:T(4,128)(2,1)S(1)}, bf16[3,128]{1,0:T(4,128)(2,1)}, u32[]{:S(2)}) copy-start(bf16[3,128]{1,0:T(4,128)(2,1)} %param.29) | copy-start | bytes 2308
  13.1 68.6 %copy-start.66 = (bf16[3,128]{1,0:T(4,128)(2,1)S(1)}, bf16[3,128]{1,0:T(4,128)(2,1)}, u32[]{:S(2)}) copy-start(bf16[3,128]{1,0:T(4,128)(2,1)} %param.30) | copy-start | bytes 2308
  13.1 68.7 %copy-start.68 = (f32[2,8]{1,0:T(2,128)S(1)}, f32[2,8]{1,0:T(2,128)}, u32[]{:S(2)}) copy-start(f32[2,8]{1,0:T(2,128)} %param.31) | copy-start | bytes 196
  67.5 8.4 %all-to-all-start = ((f32[4,3,2,512]{3,2,1,0:T(2,128)}), f32[4,3,2,512]{3,2,1,0:T(2,128)S(1)}, u32[]{:S(2)}, u32[]{:S(2)}) async-start(f32[4,3,2,512]{3,2,1,0:T(2,128)} %broadcast_in_dim.22), calls=%async_computation | async-start | bytes 98304 | tf_op jit(solution)/shard_map/all_to_all | solution.py:30
  77.5 20.8 %all-to-all-start.1 = ((bf16[4,32,2048]{2,1,0:T(8,128)(2,1)}), bf16[4,32,2048]{2,1,0:T(8,128)(2,1)}, u32[]{:S(2)}, u32[]{:S(2)}) async-start(bf16[4,32,2048]{2,1,0:T(8,128)(2,1)} %broadcast_in_dim.24), calls=%async_computation.1 | async-start | bytes 1048576 | tf_op jit(solution)/shard_map/all_to_all | solution.py:30
  81.7 85.5 %all-gather.19.cloned.1.call-start = ((), (), s32[]{:S(2)}) async-start(), calls=%async_computation.9 | async-start | bytes 1179648 | tf_op jit(solution)/shard_map/all_gather | solution.py:71
  81.8 21.7 %copy-start.23 = (f32[8]{0:T(128)}, f32[8]{0:T(128)S(1)}, u32[]{:S(2)}) copy-start(f32[8]{0:T(128)S(1)} %get-tuple-element.112) | copy-start | bytes 100
  81.8 21.8 %copy-start.21 = (f32[8]{0:T(128)}, f32[8]{0:T(128)S(1)}, u32[]{:S(2)}) copy-start(f32[8]{0:T(128)S(1)} %get-tuple-element.113) | copy-start | bytes 100
  104.8 4.3 %collective-permute-start = (bf16[1,768]{0,1:T(8,128)(2,1)S(1)}, bf16[1,768]{0,1:T(8,128)(2,1)S(1)}, u32[]{:S(2)}, u32[]{:S(2)}) collective-permute-start(bf16[1,768]{0,1:T(8,128)(2,1)S(1)} %get-tuple-element.49), channel_id=1, source_target_pairs={{0,8},{8,16},{16,24},{24,32},{32,40},{40,48},{48,56},{56,64},{64,7... | collective-permute-start | bytes 4616 | tf_op jit(solution)/shard_map/ppermute | solution.py:53
  106.5 6.4 %collective-permute-start.1 = (bf16[1,768]{0,1:T(8,128)(2,1)S(1)}, bf16[1,768]{0,1:T(8,128)(2,1)S(1)}, u32[]{:S(2)}, u32[]{:S(2)}) collective-permute-start(bf16[1,768]{0,1:T(8,128)(2,1)S(1)} %get-tuple-element.50), channel_id=1, source_target_pairs={{8,0},{16,8},{24,16},{32,24},{40,32},{48,40},{56,48},{64,56},{72,6... | collective-permute-start | bytes 4616 | tf_op jit(solution)/shard_map/ppermute | solution.py:54
  115.9 93.1 %all-gather.17.cloned.1.call-start = ((), (), s32[]{:S(2)}) async-start(), calls=%async_computation.8 | async-start | bytes 1179648 | tf_op jit(solution)/shard_map/all_gather | solution.py:71
  117.5 94.5 %copy-start.16 = (bf16[3,512]{1,0:T(4,128)(2,1)S(1)}, bf16[3,512]{1,0:T(4,128)(2,1)}, u32[]{:S(2)}) copy-start(bf16[3,512]{1,0:T(4,128)(2,1)} %param.28) | copy-start | bytes 9220
  117.6 94.5 %copy-start.31 = (bf16[3,128]{1,0:T(4,128)(2,1)S(1)}, bf16[3,128]{1,0:T(4,128)(2,1)}, u32[]{:S(2)}) copy-start(bf16[3,128]{1,0:T(4,128)(2,1)} %param.29) | copy-start | bytes 2308
  117.6 95.1 %copy-start.11 = (bf16[1,8,2048]{2,1,0:T(8,128)(2,1)S(1)}, bf16[1,8,2048]{2,1,0:T(8,128)(2,1)}, u32[]{:S(2)}) copy-start(bf16[1,8,2048]{2,1,0:T(8,128)(2,1)} %param.19) | copy-start | bytes 98308
  117.6 95.2 %copy-start.67 = (bf16[512]{0:T(512)(128)(2,1)S(1)}, bf16[512]{0:T(512)(128)(2,1)}, u32[]{:S(2)}) copy-start(bf16[512]{0:T(512)(128)(2,1)} %param.32) | copy-start | bytes 3076
  118.5 165.9 %all-gather.13.cloned.1.call-start = ((), (), s32[]{:S(2)}) async-start(), calls=%async_computation.6 | async-start | bytes 1179648 | tf_op jit(solution)/shard_map/all_gather | solution.py:71
  131.6 38.0 %copy-start.49 = (f32[8]{0:T(128)}, f32[8]{0:T(128)S(1)}, u32[]{:S(2)}) copy-start(f32[8]{0:T(128)S(1)} %get-tuple-element.104) | copy-start | bytes 100
  131.6 38.0 %copy-start.51 = (f32[8]{0:T(128)}, f32[8]{0:T(128)S(1)}, u32[]{:S(2)}) copy-start(f32[8]{0:T(128)S(1)} %get-tuple-element.105) | copy-start | bytes 100
  131.6 38.0 %copy-start.53 = (f32[8]{0:T(128)}, f32[8]{0:T(128)S(1)}, u32[]{:S(2)}) copy-start(f32[8]{0:T(128)S(1)} %get-tuple-element.106) | copy-start | bytes 100
  131.6 38.0 %copy-start.55 = (f32[8]{0:T(128)}, f32[8]{0:T(128)S(1)}, u32[]{:S(2)}) copy-start(f32[8]{0:T(128)S(1)} %get-tuple-element.107) | copy-start | bytes 100
  131.6 38.0 %copy-start.57 = (f32[8]{0:T(128)}, f32[8]{0:T(128)S(1)}, u32[]{:S(2)}) copy-start(f32[8]{0:T(128)S(1)} %get-tuple-element.108) | copy-start | bytes 100
  131.6 38.0 %copy-start.59 = (f32[8]{0:T(128)}, f32[8]{0:T(128)S(1)}, u32[]{:S(2)}) copy-start(f32[8]{0:T(128)S(1)} %get-tuple-element.109) | copy-start | bytes 100
  131.7 38.0 %copy-start.61 = (f32[8]{0:T(128)}, f32[8]{0:T(128)S(1)}, u32[]{:S(2)}) copy-start(f32[8]{0:T(128)S(1)} %get-tuple-element.110) | copy-start | bytes 100
  131.7 38.0 %copy-start.63 = (f32[8]{0:T(128)}, f32[8]{0:T(128)S(1)}, u32[]{:S(2)}) copy-start(f32[8]{0:T(128)S(1)} %get-tuple-element.111) | copy-start | bytes 100
  169.5 131.0 %all-gather.11.cloned.1.call-start = ((), (), s32[]{:S(2)}) async-start(), calls=%async_computation.5 | async-start | bytes 1179648 | tf_op jit(solution)/shard_map/all_gather | solution.py:71
  180.8 31.2 %copy-start.33 = (f32[8]{0:T(128)}, f32[8]{0:T(128)S(1)}, u32[]{:S(2)}) copy-start(f32[8]{0:T(128)S(1)} %get-tuple-element.84) | copy-start | bytes 100
  180.8 31.2 %copy-start.35 = (f32[8]{0:T(128)}, f32[8]{0:T(128)S(1)}, u32[]{:S(2)}) copy-start(f32[8]{0:T(128)S(1)} %get-tuple-element.85) | copy-start | bytes 100
  180.8 57.9 %copy-start.37 = (f32[8]{0:T(128)}, f32[8]{0:T(128)S(1)}, u32[]{:S(2)}) copy-start(f32[8]{0:T(128)S(1)} %get-tuple-element.86) | copy-start | bytes 100
  180.8 57.9 %copy-start.39 = (f32[8]{0:T(128)}, f32[8]{0:T(128)S(1)}, u32[]{:S(2)}) copy-start(f32[8]{0:T(128)S(1)} %get-tuple-element.87) | copy-start | bytes 100
  180.9 57.9 %copy-start.41 = (f32[8]{0:T(128)}, f32[8]{0:T(128)S(1)}, u32[]{:S(2)}) copy-start(f32[8]{0:T(128)S(1)} %get-tuple-element.88) | copy-start | bytes 100
  180.9 57.9 %copy-start.43 = (f32[8]{0:T(128)}, f32[8]{0:T(128)S(1)}, u32[]{:S(2)}) copy-start(f32[8]{0:T(128)S(1)} %get-tuple-element.89) | copy-start | bytes 100
  180.9 57.9 %copy-start.45 = (f32[8]{0:T(128)}, f32[8]{0:T(128)S(1)}, u32[]{:S(2)}) copy-start(f32[8]{0:T(128)S(1)} %get-tuple-element.90) | copy-start | bytes 100
  180.9 57.9 %copy-start.47 = (f32[8]{0:T(128)}, f32[8]{0:T(128)S(1)}, u32[]{:S(2)}) copy-start(f32[8]{0:T(128)S(1)} %get-tuple-element.91) | copy-start | bytes 100
  211.4 114.2 %all-gather.15.cloned.1.call-start = ((), (), s32[]{:S(2)}) async-start(), calls=%async_computation.7 | async-start | bytes 3145728 | tf_op jit(solution)/shard_map/all_gather | solution.py:227
  242.2 24.7 %all-to-all-start.2 = ((bf16[64,8,656]{2,1,0:T(8,128)(2,1)}), bf16[64,8,656]{2,1,0:T(8,128)(2,1)S(1)}, u32[]{:S(2)}, u32[]{:S(2)}) async-start(bf16[64,8,656]{2,1,0:T(8,128)(2,1)} %broadcast_in_dim.26), calls=%async_computation.2 | async-start | bytes 1572864 | tf_op jit(solution)/shard_map/all_to_all | solution.py:30
  284.5 16.0 %copy-start.2 = (bf16[512,8,64]{0,2,1:T(8,128)(2,1)S(1)}, bf16[512,8,64]{0,2,1:T(8,128)(2,1)}, u32[]{:S(2)}) copy-start(bf16[512,8,64]{0,2,1:T(8,128)(2,1)} %multiply_convert_fusion.2) | copy-start | bytes 1572868
  284.5 16.0 %copy-start.26 = (f32[128,8]{0,1:T(8,128)S(1)}, f32[128,8]{0,1:T(8,128)}, u32[]{:S(2)}) copy-start(f32[128,8]{0,1:T(8,128)} %get-tuple-element.72) | copy-start | bytes 12292
  284.5 16.0 %copy-start.34 = (f32[8]{0:T(128)S(1)}, f32[8]{0:T(128)}, u32[]{:S(2)}) copy-start(f32[8]{0:T(128)} %copy-done.33) | copy-start | bytes 100
  284.5 16.0 %copy-start.36 = (f32[8]{0:T(128)S(1)}, f32[8]{0:T(128)}, u32[]{:S(2)}) copy-start(f32[8]{0:T(128)} %copy-done.35) | copy-start | bytes 100
  284.5 16.0 %copy-start.38 = (f32[8]{0:T(128)S(1)}, f32[8]{0:T(128)}, u32[]{:S(2)}) copy-start(f32[8]{0:T(128)} %copy-done.37) | copy-start | bytes 100
  284.5 16.0 %copy-start.40 = (f32[8]{0:T(128)S(1)}, f32[8]{0:T(128)}, u32[]{:S(2)}) copy-start(f32[8]{0:T(128)} %copy-done.39) | copy-start | bytes 100
  284.6 16.0 %copy-start.42 = (f32[8]{0:T(128)S(1)}, f32[8]{0:T(128)}, u32[]{:S(2)}) copy-start(f32[8]{0:T(128)} %copy-done.41) | copy-start | bytes 100
  284.6 16.0 %copy-start.44 = (f32[8]{0:T(128)S(1)}, f32[8]{0:T(128)}, u32[]{:S(2)}) copy-start(f32[8]{0:T(128)} %copy-done.43) | copy-start | bytes 100
  300.8 24.8 %copy-start.20 = (f32[512]{0:T(512)S(1)}, f32[512]{0:T(512)}, u32[]{:S(2)}) copy-start(f32[512]{0:T(512)} %convert_element_type.1335) | copy-start | bytes 6148
  (47 other events, 383.7 us)
Sparse Core Ops, SparseCore 0:
  13.3 31.0 all-gather.8
  116.1 51.1 all-gather.18
  169.3 39.7 all-gather.16
  211.0 41.0 all-gather.12
  254.0 46.4 all-gather.10
  302.5 22.9 all-gather.14
where the time goes:
time: 349 us; the launch traced here: 347 us
  waiting for transfers between devices  117 us (34%)
  blocking collectives  113 us (32%)
  local copies, waits for them, and re-layouts  40.7 us (12%)
  other arithmetic  23 us (7%)
  starting transfers between devices  19.6 us (6%)
  matrix products  18.9 us (5%)
  between operations  15 us (4%)
    all_gather x4, waiting for transfers between devices, entering_2(): lax.all_gather(part.astype(kind), axis)  74.5 us
    psum x2, blocking collectives, over_axes(): return functools.reduce(lax.psum, axes, x)  52.9 us
    all_gather x4, blocking collectives, entering_2(): lax.all_gather(part.astype(kind), axis)  48.2 us
    all_gather x1, waiting for transfers between devices, shards(): lax.all_gather(w_out, 'dp', axis=0, tiled=True)  21.7 us
    all_to_all x3, starting transfers between devices, sent_to_all(): lax.all_to_all(jnp.broadcast_to(x[None], (peers, *x.shape)), axis, 0, 0,...  16.4 us
    all_to_all x3, waiting for transfers between devices, sent_to_all(): lax.all_to_all(jnp.broadcast_to(x[None], (peers, *x.shape)), axis, 0, 0,...  15.7 us
    all_to_all x1, blocking collectives, sum_at_owner(): tiles = lax.all_to_all(split_up(x, dim, peers), axis, 0, 0, tiled=True)  11.9 us
    concatenate x1, local copies, waits for them, and re-layouts, shards(): jnp.concatenate([full_x, full_b, full_c, full_fwd, full_bwd, full_z], axi...  9.42 us
  transfers between devices with their start and end apart: 11, of which 8 were waited for; matrix products, arithmetic and copies ran while one was open for 18% of the time, Pallas kernels for 0%

commit v1 on v0

v1 whole, which is shorter than its diff:
```python
import functools

import jax
import jax.numpy as jnp
from jax import lax
from jax.experimental import pallas as pl
from jax.experimental.pallas import tpu as pltpu
from jax.sharding import Mesh
from jax.sharding import PartitionSpec as P

SP = ("sp_0", "sp_1")
ALL = ("sp_0", "sp_1", "tp")
EPSILON = 1e-06
INTERPRET = False

D = 2048
HALF = D // 2
TOK = 128
OWN = 32
INNER = 512
HEADS = 8
HD = 64
STATE = 128
NSP = 64
CTX_DEV = 8
CTX = NSP * CTX_DEV
XB = INNER + STATE
XBC = INNER + 2 * STATE
COLS = XBC + INNER + 128
ROWS = TOK + 16

f32 = jnp.float32
bf16 = jnp.bfloat16
HIGHEST = lax.Precision.HIGHEST


def silu(v):
    return v / (1.0 + jnp.exp(-v))


def softplus(v):
    return jnp.maximum(v, 0.0) + jnp.log1p(jnp.exp(-jnp.abs(v)))


def rounded(v):
    return v.astype(bf16).astype(f32)


def lanes(shape):
    return lax.broadcasted_iota(jnp.int32, shape, 1)


def rows_of(shape):
    return lax.broadcasted_iota(jnp.int32, shape, 0)


def per_channel(table, first, chunk):
    left = table[:, first + 2 * chunk : first + 2 * chunk + 1]
    right = table[:, first + 2 * chunk + 1 : first + 2 * chunk + 2]
    shape = (table.shape[0], 128)
    return jnp.where(lanes(shape) < HD, left, right)


def project_kernel(
    place_ref, lat_ref, gain_ref, mod_ref, own_ref, other_ref, tap_ref, rate_ref,
    send_ref, x_ref, b_ref, c_ref, z_ref, step_ref, run_ref, gate_ref,
    h_ref, conv_ref,
):
    core = place_ref[0]
    at = place_ref[1]
    mods = []
    for t in range(4):
        total = mod_ref[t]
        for y in range(1, 8):
            total = total + mod_ref[4 * y + t]
        mods.append(total)
    squares = jnp.zeros((ROWS, 128), f32)
    for c in range(16):
        v = lat_ref[:, c * 128 : (c + 1) * 128].astype(f32)
        squares = squares + v * v
    inv = lax.rsqrt(jnp.sum(squares, axis=1, keepdims=True) * (1.0 / D) + EPSILON)
    inv_main, inv_ctx = inv[: ROWS - 8], inv[ROWS - 8 :]
    for c in range(16):
        t, q = c // 4, c % 4
        cols = slice(c * 128, (c + 1) * 128)
        v = lat_ref[:, cols].astype(f32)
        gain = gain_ref[0:1, cols].astype(f32)
        shift, scale = mods[t][q : q + 1], mods[t][4 + q : 5 + q]
        cshift, cscale = mods[t][8 + q : 9 + q], mods[t][12 + q : 13 + q]
        gate_ref[0:1, cols] = mods[t][16 + q : 17 + q]
        main = v[: ROWS - 8] * inv_main * gain * (1.0 + scale) + shift
        ctx = v[ROWS - 8 :] * inv_ctx * gain * (1.0 + cscale) + cshift
        h_ref[0:TOK, cols] = main[:TOK].astype(bf16)
        h_ref[TOK:ROWS, cols] = jnp.concatenate([main[TOK:], ctx], axis=0).astype(bf16)
    mine = pl.multiple_of(core * HALF, HALF)
    theirs = pl.multiple_of((1 - core) * HALF, HALF)

    def project(first, width):
        cols = slice(first, first + width)
        out = jnp.dot(h_ref[:, pl.ds(mine, HALF)], own_ref[:, cols], preferred_element_type=f32)
        out = out + jnp.dot(
            h_ref[:, pl.ds(theirs, HALF)], other_ref[:, cols], preferred_element_type=f32
        )
        return rounded(out)

    dt = project(XBC + INNER, 128)
    step = softplus(dt[:TOK])
    step_ref[...] = step
    log_decay = -(rate_ref[0:1, :] * step)
    ri, ci = rows_of((TOK, TOK)), lanes((TOK, TOK))
    lower = jnp.where(ri >= ci, 1.0, 0.0).astype(f32)
    upper = jnp.where(ri <= ci, 1.0, 0.0).astype(f32)
    ahead = jnp.dot(lower, log_decay, preferred_element_type=f32, precision=HIGHEST)
    behind = jnp.dot(upper, log_decay, preferred_element_type=f32, precision=HIGHEST)
    run = jnp.where(ci < HEADS, ahead, behind)
    run_ref[...] = run
    total = jnp.where(lanes((1, 128)) < HEADS, run[TOK - 1 : TOK], run[0:1])
    to_end = jnp.exp(total - run)

    before_ok = jnp.where(at > 0, 1.0, 0.0)
    after_ok = jnp.where(at < NSP - 1, 1.0, 0.0)

    def convolved(first, width):
        cols = slice(first, first + width)
        p = project(first, width)
        conv_ref[8 : 8 + TOK, cols] = p[:TOK]
        conv_ref[0:8, cols] = jnp.broadcast_to(p[TOK : TOK + 1] * before_ok, (8, width))
        conv_ref[8 + TOK : 16 + TOK, cols] = jnp.broadcast_to(
            p[TOK + 1 : TOK + 2] * after_ok, (8, width)
        )
        summed = (
            conv_ref[7 : 7 + TOK, cols] * tap_ref[0:1, cols]
            + conv_ref[8 : 8 + TOK, cols] * tap_ref[1:2, cols]
            + conv_ref[9 : 9 + TOK, cols] * tap_ref[2:3, cols]
        )
        return silu(summed).astype(bf16), p[TOK + 8 :]

    b_in, ctx_b = convolved(INNER, STATE)
    b_ref[...] = b_in
    x_in, ctx_x = convolved(0, INNER)
    x_ref[...] = x_in

    states = []
    for first in (0, HEADS):
        parts = []
        for q in range(4):
            moved = rounded(x_in[:, q * 128 : (q + 1) * 128].astype(f32) * per_channel(step, first, q))
            parts.append((moved * per_channel(to_end, first, q)).astype(bf16))
        states.append(
            lax.dot_general(
                jnp.concatenate(parts, axis=1), b_in, (((0,), (0,)), ((), ())),
                preferred_element_type=f32,
            ).reshape(NSP, 8, STATE)
        )
    send_ref[:, 0:16, :] = jnp.concatenate(states, axis=1).astype(bf16)

    ctx_dt = dt[TOK + 8 :]
    high = rounded(total)
    low = rounded(total - high)
    lane = lanes((8, 128))
    blocks = []
    for head in range(HEADS):
        misc = jnp.zeros((8, 128), f32)
        for spot, table, col in (
            (8, ctx_dt, head), (9, ctx_dt, HEADS + head), (10, high, head), (11, low, head),
            (12, high, HEADS + head), (13, low, HEADS + head),
        ):
            misc = jnp.where(lane == spot, table[:, col : col + 1], misc)
        for k in range(8):
            j = head * 8 + k
            chunk = ctx_x[:, (j // 16) * 128 : (j // 16 + 1) * 128]
            shift = (128 - 8 * (j % 16)) % 128
            if shift:
                chunk = pltpu.roll(chunk, shift, 1)
            blocks.append(jnp.concatenate([ctx_b, jnp.where(lane < 8, chunk, misc)], axis=0))
    for j in range(NSP):
        send_ref[j, 16:32, :] = blocks[j].astype(bf16)

    c_in, _ = convolved(XB, STATE)
    c_ref[...] = c_in
    z_ref[...] = project(XBC, INNER)[:TOK].astype(bf16)


def inside_kernel(x_ref, b_ref, c_ref, step_ref, run_ref, y_ref):
    step, run = step_ref[...], run_ref[...]
    turned = run.T
    scores = lax.dot_general(
        c_ref[...], b_ref[...], (((1,), (1,)), ((), ())), preferred_element_type=f32
    )
    ri, ci = rows_of((TOK, TOK)), lanes((TOK, TOK))
    for q in range(4):
        cols = slice(q * 128, (q + 1) * 128)
        x = x_ref[:, cols].astype(f32)
        moved = jnp.concatenate(
            [(x * per_channel(step, first, q)).astype(bf16) for first in (0, HEADS)], axis=0
        )
        outs = []
        for head in (2 * q, 2 * q + 1):
            weights = []
            for first, kept in ((0, ri >= ci), (HEADS, ri <= ci)):
                k = first + head
                spread = run[:, k : k + 1] - turned[k : k + 1, :]
                decay = jnp.where(kept, jnp.exp(jnp.minimum(spread, 0.0)), 0.0)
                weights.append((scores * decay).astype(bf16))
            outs.append(
                jnp.dot(jnp.concatenate(weights, axis=1), moved, preferred_element_type=f32)
            )
        y_ref[:, cols] = jnp.where(ci < HD, outs[0], outs[1])


def owner_kernel(rate_ref, recv_ref, tap_b_ref, tap_x_ref, out_ref, pad_ref, held_ref):
    def conv(values, tap_ref):
        pad_ref[0:8, :] = jnp.zeros((8, 128), f32)
        pad_ref[8 + CTX : 16 + CTX, :] = jnp.zeros((8, 128), f32)
        pad_ref[8 : 8 + CTX, :] = values
        summed = (
            pad_ref[7 : 7 + CTX, :] * tap_ref[0:1, :]
            + values * tap_ref[1:2, :]
            + pad_ref[9 : 9 + CTX, :] * tap_ref[2:3, :]
        )
        return silu(summed)

    both = recv_ref[:, 16:32, :].astype(f32)
    raw_b = both[:, 0:8, :].reshape(CTX, 128)
    misc = both[:, 8:16, :].reshape(CTX, 128)
    ctx_b = conv(raw_b, tap_b_ref).astype(bf16)
    ctx_x = rounded(conv(misc, tap_x_ref))
    step = softplus(misc)
    lane = lanes((CTX, 128))
    decay = -jnp.where(lane == 8, rate_ref[0] * step, rate_ref[1] * step)
    wide = jnp.where(lane < HD, decay[:, 8:9], decay[:, 9:10])
    high = rounded(wide)
    mid = rounded(wide - high)
    low = rounded(wide - high - mid)
    spot = lane % 4
    parts = jnp.where(spot == 0, high, jnp.where(spot == 1, mid, jnp.where(spot == 2, low, 0.0)))
    parts = parts.astype(bf16)
    ri, ci = rows_of((CTX, CTX)), lanes((CTX, CTX))
    later = jnp.where(ci > ri, 1.0, 0.0).astype(bf16)
    earlier = jnp.where(ci < ri, 1.0, 0.0).astype(bf16)
    fsum = jnp.dot(later, parts, preferred_element_type=f32)
    bsum = jnp.dot(earlier, parts, preferred_element_type=f32)
    wf = jnp.exp(fsum[:, 0:1] + fsum[:, 1:2] + fsum[:, 2:3])
    wb = jnp.exp(bsum[:, 64:65] + bsum[:, 65:66] + bsum[:, 66:67])
    xf = rounded(ctx_x * step[:, 8:9]) * wf
    xb = rounded(ctx_x * step[:, 9:10]) * wb
    x16 = jnp.where(lane < 8, xf, pltpu.roll(xb, 8, 1))
    x_high = rounded(x16)
    x_low = x16 - x_high
    x32 = jnp.where(lane < 16, x_high, jnp.where(lane < 32, pltpu.roll(x_low, 16, 1), 0.0))
    start = lax.dot_general(
        x32.astype(bf16), ctx_b, (((0,), (0,)), ((), ())), preferred_element_type=f32
    )
    ahead = start[0:8] + start[16:24]
    behind = start[8:16] + start[24:32]
    grow_f = jnp.exp(jnp.broadcast_to(misc[:, 10:11] + misc[:, 11:12], (CTX, 128))).reshape(
        NSP, 8, 128
    )
    grow_b = jnp.exp(jnp.broadcast_to(misc[:, 12:13] + misc[:, 13:14], (CTX, 128))).reshape(
        NSP, 8, 128
    )
    fresh = recv_ref[:, 0:16, :].astype(f32)
    for k in range(NSP):
        m = NSP - 1 - k
        held_ref[k, 0:8, :] = ahead
        held_ref[m, 8:16, :] = behind
        ahead = ahead * grow_f[k] + fresh[k, 0:8]
        behind = behind * grow_b[m] + fresh[m, 8:16]
    out_ref[...] = held_ref[...].astype(bf16)


def output_kernel(
    place_ref, state_ref, c_ref, y_ref, run_ref, z_ref, gain_ref, own_ref, other_ref,
    out_ref, ny_ref,
):
    core = place_ref[0]
    states = state_ref[...].astype(f32)
    growth = jnp.exp(run_ref[...])
    c_in = c_ref[...]
    ahead = states[:, 0:8, :].reshape(INNER, STATE).astype(bf16)
    behind = states[:, 8:16, :].reshape(INNER, STATE).astype(bf16)
    dims = (((1,), (1,)), ((), ()))
    carried_f = lax.dot_general(c_in, ahead, dims, preferred_element_type=f32)
    carried_b = lax.dot_general(c_in, behind, dims, preferred_element_type=f32)
    squares = jnp.zeros((TOK, 128), f32)
    gated = []
    for q in range(4):
        cols = slice(q * 128, (q + 1) * 128)
        y = (
            y_ref[:, cols]
            + per_channel(growth, 0, q) * carried_f[:, cols]
            + per_channel(growth, HEADS, q) * carried_b[:, cols]
        )
        g = y * silu(z_ref[:, cols].astype(f32))
        squares = squares + g * g
        gated.append(g)
    inv = lax.rsqrt(jnp.sum(squares, axis=1, keepdims=True) * (1.0 / INNER) + EPSILON)
    for q in range(4):
        cols = slice(q * 128, (q + 1) * 128)
        ny_ref[:, cols] = (gated[q] * inv * gain_ref[0:1, cols].astype(f32)).astype(bf16)
    half = INNER // 2
    mine = ny_ref[:, pl.ds(pl.multiple_of(core * half, half), half)]
    theirs = ny_ref[:, pl.ds(pl.multiple_of((1 - core) * half, half), half)]
    for n in range(4):
        cols = slice(n * 512, (n + 1) * 512)
        out = jnp.dot(mine, own_ref[:, cols], preferred_element_type=f32)
        out = out + jnp.dot(theirs, other_ref[:, cols], preferred_element_type=f32)
        out_ref[:, cols] = out.astype(bf16)


def call(kernel, out_shape, n_args, smem, scratch=(), flops=10**8, name=None):
    vmem = pl.BlockSpec(memory_space=pltpu.VMEM)
    in_specs = [pl.BlockSpec(memory_space=pltpu.SMEM) if i in smem else vmem for i in range(n_args)]
    many = isinstance(out_shape, (list, tuple))
    return pl.pallas_call(
        kernel,
        out_shape=out_shape,
        in_specs=in_specs,
        out_specs=[vmem] * len(out_shape) if many else vmem,
        scratch_shapes=list(scratch),
        compiler_params=pltpu.CompilerParams(vmem_limit_bytes=30 * 2**20),
        cost_estimate=pl.CostEstimate(flops=flops, bytes_accessed=2**20, transcendentals=0),
        interpret=INTERPRET,
        name=name,
    )


def project_call(*args):
    shape = jax.ShapeDtypeStruct
    return call(
        project_kernel,
        [
            shape((NSP, 32, 128), bf16),
            shape((TOK, INNER), bf16),
            shape((TOK, STATE), bf16),
            shape((TOK, STATE), bf16),
            shape((TOK, INNER), bf16),
            shape((TOK, 128), f32),
            shape((TOK, 128), f32),
            shape((1, D), f32),
        ],
        8,
        (0,),
        [pltpu.VMEM((ROWS, D), bf16), pltpu.VMEM((TOK + 16, XBC), f32)],
        name="project",
    )(*args)


def inside_call(*args):
    return call(inside_kernel, jax.ShapeDtypeStruct((TOK, INNER), f32), 5, (), name="inside")(*args)


def owner_call(*args):
    return call(
        owner_kernel,
        jax.ShapeDtypeStruct((NSP, 16, 128), bf16),
        4,
        (0,),
        [pltpu.VMEM((CTX + 16, 128), f32), pltpu.VMEM((NSP, 16, 128), f32)],
        name="owner",
    )(*args)


def output_call(*args):
    return call(
        output_kernel,
        jax.ShapeDtypeStruct((TOK, D), bf16),
        9,
        (0,),
        [pltpu.VMEM((TOK, INNER), bf16)],
        name="output",
    )(*args)


def swapped(x):
    return lax.ppermute(x, "dp", [(0, 1), (1, 0)])


def exchanged(x, axes):
    return lax.all_to_all(x, axes, 0, 0, tiled=True)


def sent_to_all(x, peers, axes):
    return exchanged(jnp.broadcast_to(x[None], (peers, *x.shape)), axes)


def joined_weights(w_x, w_b, w_c, w_z, w_dt):
    steps = jnp.concatenate([w_dt[0], w_dt[1]], axis=1)
    steps = jnp.pad(steps, ((0, 0), (0, 128 - steps.shape[1])))
    return jnp.concatenate([w_x, w_b, w_c, w_z, steps], axis=1)


def owner_taps(conv_x, conv_b, at):
    own = lax.dynamic_slice_in_dim(conv_x, at * 8, 8, 1)
    tap_x = jnp.pad(own.astype(f32), ((0, 0), (0, 120)))
    return conv_b.astype(f32), tap_x


def shards(
    latent, condition, context, context_source, mod_weight, norm_gain,
    w_x, w_b, w_c, w_z, w_dt, conv_x, conv_b, conv_c, decay_rate, out_gain, w_out,
):
    at = lax.axis_index(SP)
    core = lax.axis_index("dp")
    place = jnp.stack([core, at]).astype(jnp.int32)
    row_count = mod_weight.shape[1]

    act = jnp.stack(
        [silu(condition[0].astype(f32)), silu(context_source.astype(f32))]
    ).astype(bf16)
    act = lax.dynamic_slice_in_dim(act, at * row_count, row_count, 1)
    part = jnp.einsum("ar,krc->akc", act, mod_weight, preferred_element_type=f32)
    part = jnp.stack([part[0, 0], part[0, 1], part[1, 0], part[1, 1], part[0, 2]])
    part = part.reshape(20, 128)
    part = jnp.sum(sent_to_all(part, 8, "sp_0"), axis=0)
    mods = sent_to_all(part, 32, ("sp_1", "tp"))

    rows = latent[0]
    tp = lax.axis_index("tp")
    edge = jnp.where(tp == 3, rows[OWN - 1 :], rows[:1])
    pairs = [(4 * i + 3, 4 * i + 4) for i in range(NSP - 1)]
    pairs += [(j, i) for i, j in pairs]
    halo = lax.ppermute(edge, ALL, pairs)
    packed = jnp.concatenate([rows, jnp.pad(halo, ((0, 7), (0, 0)))], axis=0)
    block = sent_to_all(packed, 4, "tp")
    all_rows = jnp.concatenate(
        [
            block[:, :OWN].reshape(TOK, D),
            block[0, OWN : OWN + 1],
            block[3, OWN : OWN + 1],
            jnp.zeros((6, D), bf16),
            context[0],
        ],
        axis=0,
    )

    weights = joined_weights(w_x, w_b, w_c, w_z, w_dt)
    other_weights = swapped(weights)
    other_out = swapped(w_out)

    taps = jnp.concatenate([conv_x, conv_b, conv_c], axis=1).astype(f32)
    rates = jnp.pad(decay_rate.reshape(1, 2 * HEADS), ((0, 0), (0, 128 - 2 * HEADS)))
    tap_b, tap_x = owner_taps(conv_x, conv_b, at)
    own_rates = lax.dynamic_slice_in_dim(decay_rate, at // 8, 1, 1)[:, 0]

    send, x_in, b_in, c_in, z_in, step, run, gate = project_call(
        place, all_rows, norm_gain[None], mods, weights, other_weights, taps, rates
    )
    received = exchanged(send, SP)
    y_in = inside_call(x_in, b_in, c_in, step, run)
    states = exchanged(owner_call(own_rates, received, tap_b, tap_x), SP)
    partial = output_call(
        place, states, c_in, y_in, run, z_in, out_gain[None], w_out, other_out
    )
    tiles = exchanged(partial.reshape(4, OWN, D), "tp")
    mixed = jnp.sum(tiles.astype(f32), axis=0)
    return (gate * mixed).astype(bf16)[None]


def solution(mesh):
    torus = Mesh(
        mesh.devices.reshape(8, 8, mesh.shape["tp"], mesh.shape["dp"]), ("sp_0", "sp_1", "tp", "dp")
    )
    sp_tp = ("sp_0", "sp_1", "tp")
    placed = (
        P("dp", sp_tp, None),
        P("dp", None),
        P("dp", SP, None),
        P(),
        P(None, SP, "tp"),
        P(),
        P("dp", "tp"),
        P("dp", "tp"),
        P("dp", "tp"),
        P("dp", "tp"),
        P(None, "dp", "tp"),
        P(None, "tp"),
        P(None, "tp"),
        P(None, "tp"),
        P(None, "tp"),
        P("tp"),
        P(("tp", "dp"), None),
    )
    return jax.shard_map(
        shards, mesh=torus, in_specs=placed, out_specs=P("dp", sp_tp, None), check_vma=False
    )
```

time: 349 us -> 138 us (0.40)
  the two profiles are of different devices: /device:TPU:1 before, /device:TPU:8 now
where the time goes in v1:
time: 138 us; the launch traced here: 137 us
  waiting for transfers between devices  43 us (31%)
  starting transfers between devices  42.9 us (31%)
  local copies, waits for them, and re-layouts  24.7 us (18%)
  blocking collectives  11.8 us (9%)
  Pallas kernels  9.75 us (7%)
  other arithmetic  4.03 us (3%)
    all_to_all x5, waiting for transfers between devices, exchanged(): return lax.all_to_all(x, axes, 0, 0, tiled=True)  43 us
    all_to_all x5, starting transfers between devices, exchanged(): return lax.all_to_all(x, axes, 0, 0, tiled=True)  34.5 us
    all_to_all x1, blocking collectives, exchanged(): return lax.all_to_all(x, axes, 0, 0, tiled=True)  11.8 us
    unnamed x44, local copies, waits for them, and re-layouts  9.91 us
    concatenate x1, local copies, waits for them, and re-layouts, shards(): jnp.concatenate([block[:, :OWN].reshape(TOK, D), block[0, OWN:OWN + 1], b...  5.17 us
    ppermute x1, starting transfers between devices, shards(): halo = lax.ppermute(edge, ALL, pairs)  4.55 us
    pallas_call x1, Pallas kernels, project_call(): call(project_kernel, [shape((NSP, 32, 128), bf16), shape((TOK, INNER), bf...  4.42 us
    ppermute x2, starting transfers between devices, swapped(): return lax.ppermute(x, 'dp', [(0, 1), (1, 0)])  3.84 us
  transfers between devices with their start and end apart: 8, of which 5 were waited for; matrix products, arithmetic and copies ran while one was open for 13% of the time, Pallas kernels for 3%

profile of v1, /device:TPU:8, one launch (start us, length us, event | category | flops | bytes accessed | tf_op | source)
XLA Modules:
  0.0 136.7 jit_solution(5882483402733481767)
XLA Ops:
  0.0 0.8 slice_bitcast_fusion.1
  1.0 1.4 %constant_dynamic-update-slice_fusion.3 = bf16[1024,1408]{1,0:T(8,128)(2,1)S(1)} fusion(bf16[1024,512]{1,0:T(8,128)(2,1)} %param.23), kind=kLoop, calls=%fused_computation.14 | loop fusion | bytes 2097152
  2.4 1.0 constant_dynamic-update-slice_fusion.2
  3.7 1.9 %collective-permute-start.1 = (bf16[1024,1408]{1,0:T(8,128)(2,1)S(1)}, bf16[1024,1408]{1,0:T(8,128)(2,1)}, u32[]{:S(2)}, u32[]{:S(2)}) collective-permute-start(bf16[1024,1408]{1,0:T(8,128)(2,1)S(1)} %pad_dynamic-update-slice_fusion.own_ref), channel_id=1, source_target_pairs={{0,1},{1,0},{2,3},{3,2},{4,5},{5,4},{6,7},{7,6},{8,9},{9,8},{10,11... | collective-permute-start | bytes 8650760 | tf_op jit(solution)/shard_map/ppermute | solution.py:376
  5.6 0.8 fusion.6
  6.4 4.6 %collective-permute-start = (bf16[1,2048]{1,0:T(2,128)(2,1)S(1)}, bf16[1,2048]{1,0:T(2,128)(2,1)S(1)}, u32[]{:S(2)}, u32[]{:S(2)}) collective-permute-start(bf16[1,2048]{1,0:T(2,128)(2,1)S(1)} %fusion.6), channel_id=1, source_target_pairs={{6,8},{14,16},{22,24},{30,32},{38,40},{46,48},{54,56},{62,64},{70,... | collective-permute-start | bytes 12296 | tf_op jit(solution)/shard_map/ppermute | solution.py:423
  11.1 0.2 fusion.9
  11.4 0.6 broadcast_in_dim.33
  12.0 10.3 %all-to-all-start.1 = ((f32[8,20,128]{2,1,0:T(8,128)}), f32[8,20,128]{2,1,0:T(8,128)S(1)}, u32[]{:S(2)}, u32[]{:S(2)}) async-start(f32[8,20,128]{2,1,0:T(8,128)} %broadcast_in_dim.33), calls=%async_computation.1 | async-start | bytes 196608 | tf_op jit(solution)/shard_map/all_to_all | solution.py:380
  22.3 0.9 fusion.2
  23.3 7.9 %all-to-all-done.1 = f32[8,20,128]{2,1,0:T(8,128)S(1)} async-done(((f32[8,20,128]{2,1,0:T(8,128)}), f32[8,20,128]{2,1,0:T(8,128)S(1)}, u32[]{:S(2)}, u32[]{:S(2)}) %all-to-all-start.1) | async-done | bytes 81952 | tf_op jit(solution)/shard_map/all_to_all | solution.py:380
  31.2 0.9 broadcast_in_dim.14
  32.1 4.2 %all-to-all-start = ((bf16[4,40,2048]{2,1,0:T(8,128)(2,1)}), bf16[4,40,2048]{2,1,0:T(8,128)(2,1)}, u32[]{:S(2)}, u32[]{:S(2)}) async-start(bf16[4,40,2048]{2,1,0:T(8,128)(2,1)} %broadcast_in_dim.14), calls=%async_computation | async-start | bytes 1310720 | tf_op jit(solution)/shard_map/all_to_all | solution.py:380
  36.3 0.6 broadcast_in_dim.31.gain_ref
  37.0 0.5 pad.20.rate_ref
  37.5 8.7 %all-to-all-done = bf16[4,40,2048]{2,1,0:T(8,128)(2,1)} async-done(((bf16[4,40,2048]{2,1,0:T(8,128)(2,1)}), bf16[4,40,2048]{2,1,0:T(8,128)(2,1)}, u32[]{:S(2)}, u32[]{:S(2)}) %all-to-all-start) | async-done | bytes 655392 | tf_op jit(solution)/shard_map/all_to_all | solution.py:380
  46.2 0.8 broadcast_in_dim.34
  47.0 8.4 %all-to-all-start.2 = ((f32[32,20,128]{2,1,0:T(8,128)}), f32[32,20,128]{2,1,0:T(8,128)S(1)}, u32[]{:S(2)}, u32[]{:S(2)}) async-start(f32[32,20,128]{2,1,0:T(8,128)} %broadcast_in_dim.34), calls=%async_computation.2 | async-start | bytes 786432 | tf_op jit(solution)/shard_map/all_to_all | solution.py:380
  55.5 0.7 maximum_convert_fusion.tap_ref
  56.2 1.9 %slice.50 = bf16[4,32,2048]{2,1,0:T(8,128)(2,1)} slice(bf16[4,40,2048]{2,1,0:T(8,128)(2,1)} %all-to-all-done), slice={[0:4], [0:32], [0:2048]} | slice | bytes 1048576 | tf_op jit(solution)/shard_map/slice | solution.py:428
  58.1 0.8 slice_bitcast_fusion.2
  58.9 5.2 %concatenate.16.lat_ref = bf16[144,2048]{1,0:T(8,128)(2,1)} concatenate(bf16[128,2048]{1,0:T(8,128)(2,1)} %bitcast.37, bf16[1,2048]{1,0:T(2,128)(2,1)S(1)} %get-tuple-element.22, bf16[1,2048]{1,0:T(2,128)(2,1)S(1)} %get-tuple-element.21, bf16[6,2048]{1,0:T(8,128)(2,1)S(1)} %broadcast_in_dim.30, bf16[8,2048]{1,0:T(8,128)(2,1)} %bitcast.39), dimensions={0} | concatenate | bytes 1179648 | tf_op jit(solution)/shard_map/concatenate | solution.py:426
  64.1 3.6 %all-to-all-done.2.mod_ref = f32[32,20,128]{2,1,0:T(8,128)S(1)} async-done(((f32[32,20,128]{2,1,0:T(8,128)}), f32[32,20,128]{2,1,0:T(8,128)S(1)}, u32[]{:S(2)}, u32[]{:S(2)}) %all-to-all-start.2) | async-done | bytes 327712 | tf_op jit(solution)/shard_map/all_to_all | solution.py:380
  67.7 1.1 copy-done.1
  68.7 0.7 copy-done.8
  69.4 0.6 copy-done.13
  70.1 4.4 %project.1 = (bf16[64,32,128]{2,1,0:T(8,128)(2,1)S(1)}, bf16[128,512]{1,0:T(8,128)(2,1)S(1)}, bf16[128,128]{1,0:T(8,128)(2,1)S(1)}, bf16[128,128]{1,0:T(8,128)(2...) custom-call(s32[2]{0:T(128)S(1)} %pad_add_fusion.place_ref, ...), custom_call_target="tpu_custom_call" | custom-call | flops 100000000 | bytes 1048576 | tf_op jit(solution)/shard_map/project/pallas_call | solution.py:330
  74.5 0.8 copy-done.3
  75.3 0.6 copy-done.4
  75.9 0.7 copy-done.6
  76.6 0.6 copy-done.9
  77.2 0.6 copy-done.11
  77.8 6.4 %all-to-all-start.3 = ((bf16[64,32,128]{2,1,0:T(8,128)(2,1)}), bf16[64,32,128]{2,1,0:T(8,128)(2,1)S(1)}, u32[]{:S(2)}, u32[]{:S(2)}) async-start(bf16[64,32,128]{2,1,0:T(8,128)(2,1)} %copy-done.3), calls=%async_computation.3 | async-start | bytes 1048576 | tf_op jit(solution)/shard_map/all_to_all | solution.py:380
  84.2 1.9 %collective-permute-start.2 = (bf16[256,2048]{1,0:T(8,128)(2,1)}, bf16[256,2048]{1,0:T(8,128)(2,1)S(1)}, u32[]{:S(2)}, u32[]{:S(2)}) collective-permute-start(bf16[256,2048]{1,0:T(8,128)(2,1)} %own_ref.1), channel_id=1, source_target_pairs={{0,1},{1,0},{2,3},{3,2},{4,5},{5,4},{6,7},{7,6},{8,9},{9,8},{10,11... | collective-permute-start | bytes 3145736 | tf_op jit(solution)/shard_map/ppermute | solution.py:376
  86.2 0.7 convert_element_type.39.tap_b_ref
  86.9 0.9 dynamic-slice_reduce_fusion.rate_ref
  87.7 0.8 constant_dynamic-slice_fusion
  88.5 13.0 %all-to-all-done.3.recv_ref = bf16[64,32,128]{2,1,0:T(8,128)(2,1)S(1)} async-done(((bf16[64,32,128]{2,1,0:T(8,128)(2,1)}), bf16[64,32,128]{2,1,0:T(8,128)(2,1)S(1)}, u32[]{:S(2)}, u32[]{:S(2)}) %all-to-all-start.3) | async-done | bytes 524320 | tf_op jit(solution)/shard_map/all_to_all | solution.py:380
  101.5 3.0 %owner.1 = bf16[64,16,128]{2,1,0:T(8,128)(2,1)} custom-call(f32[2]{0:T(128)S(1)} %dynamic-slice_reduce_fusion.rate_ref, bf16[64,32,128]{2,1,0:T(8,128)(2,1)S(1)} %all-to-all-done.3.recv_ref, f32[3,128]{1,0:T(4,128)S(1)} %convert_element_type.39.tap_b_ref, f32[3,128]{1,0:T(4,128)S(1)} %pad_convert_fusion.tap_x_ref), custom_call_target="tpu_custom_call" | custom-call | flops 100000000 | bytes 1048576 | tf_op jit(solution)/shard_map/owner/pallas_call | solution.py:354
  104.5 5.2 %all-to-all-start.4 = ((bf16[64,16,128]{2,1,0:T(8,128)(2,1)}), bf16[64,16,128]{2,1,0:T(8,128)(2,1)S(1)}, u32[]{:S(2)}, u32[]{:S(2)}) async-start(bf16[64,16,128]{2,1,0:T(8,128)(2,1)} %owner.1), calls=%async_computation.4 | async-start | bytes 524288 | tf_op jit(solution)/shard_map/all_to_all | solution.py:380
  109.7 0.7 broadcast_in_dim.35.gain_ref
  110.4 0.9 copy-done.7
  111.3 0.8 copy-done.10
  112.0 0.9 inside.1.y_ref
  112.9 9.7 %all-to-all-done.4.state_ref = bf16[64,16,128]{2,1,0:T(8,128)(2,1)S(1)} async-done(((bf16[64,16,128]{2,1,0:T(8,128)(2,1)}), bf16[64,16,128]{2,1,0:T(8,128)(2,1)S(1)}, u32[]{:S(2)}, u32[]{:S(2)}) %all-to-all-start.4) | async-done | bytes 262176 | tf_op jit(solution)/shard_map/all_to_all | solution.py:380
  122.7 1.5 %output.1 = bf16[128,2048]{1,0:T(8,128)(2,1)S(1)} custom-call(s32[2]{0:T(128)S(1)} %pad_add_fusion.place_ref, bf16[64,16,128]{2,1,0:T(8,128)(2,1)S(1)} %all-to-all-done.4.state_ref, bf16[128,128]{1,0:T(8,128)(2,1)S(1)} %get-tuple-element.15.c_ref, f32[128,512]{1,0:T(8,128)S(1)} %inside.1.y_ref, f32[128,128]{1,0:T(8,128)S(1)} %get-tuple-element.19.run_ref, ...), custom_call_target="tpu_custom_call" | custom-call | flops 100000000 | bytes 1048576 | tf_op jit(solution)/shard_map/output/pallas_call | solution.py:365
  124.2 11.8 %all_to_all.30 = bf16[4,32,2048]{2,1,0:T(8,128)(2,1)S(1)} all-to-all(bf16[4,32,2048]{2,1,0:T(8,128)(2,1)S(1)} %bitcast.35), channel_id=1, replica_groups=mesh['sp_0'=8,'sp_1'=8,'tp'=4,'dp'=2] {'tp'}, dimensions={0} | all-to-all | bytes 1048576 | tf_op jit(solution)/shard_map/all_to_all | solution.py:380
  136.1 0.7 fusion.1
  (50 shorter events, 0.8 us)
Async XLA Ops:
  0.0 11.1 %copy-start = (bf16[3,32,512]{2,1,0:T(8,128)(2,1)S(1)}, bf16[3,32,512]{2,1,0:T(8,128)(2,1)}, u32[]{:S(2)}) copy-start(bf16[3,32,512]{2,1,0:T(8,128)(2,1)} %param.21) | copy-start | bytes 294916
  0.0 3.4 %copy-start.15 = (bf16[1024,128]{1,0:T(8,128)(2,1)S(1)}, bf16[1024,128]{1,0:T(8,128)(2,1)}, u32[]{:S(2)}) copy-start(bf16[1024,128]{1,0:T(8,128)(2,1)} %param.25) | copy-start | bytes 786436
  1.0 2.5 %copy-start.14 = (bf16[1024,512]{1,0:T(8,128)(2,1)S(1)}, bf16[1024,512]{1,0:T(8,128)(2,1)}, u32[]{:S(2)}) copy-start(bf16[1024,512]{1,0:T(8,128)(2,1)} %param.26) | copy-start | bytes 3145732
  1.0 10.0 %copy-start.18 = (bf16[2048]{0:T(1024)(128)(2,1)S(1)}, bf16[2048]{0:T(1024)(128)(2,1)}, u32[]{:S(2)}) copy-start(bf16[2048]{0:T(1024)(128)(2,1)} %param.20) | copy-start | bytes 12292
  1.0 10.0 %copy-start.16 = (bf16[1,2048]{1,0:T(2,128)(2,1)S(1)}, bf16[1,2048]{1,0:T(2,128)(2,1)}, u32[]{:S(2)}) copy-start(bf16[1,2048]{1,0:T(2,128)(2,1)} %param.18) | copy-start | bytes 12292
  3.5 32.8 %copy-start.17 = (bf16[2048]{0:T(1024)(128)(2,1)S(1)}, bf16[2048]{0:T(1024)(128)(2,1)}, u32[]{:S(2)}) copy-start(bf16[2048]{0:T(1024)(128)(2,1)} %param.22) | copy-start | bytes 12292
  3.5 33.4 %copy-start.19 = (f32[2,8]{1,0:T(2,128)S(1)}, f32[2,8]{1,0:T(2,128)}, u32[]{:S(2)}) copy-start(f32[2,8]{1,0:T(2,128)} %param.31) | copy-start | bytes 196
  3.7 64.0 %collective-permute-start.1 = (bf16[1024,1408]{1,0:T(8,128)(2,1)S(1)}, bf16[1024,1408]{1,0:T(8,128)(2,1)}, u32[]{:S(2)}, u32[]{:S(2)}) collective-permute-start(bf16[1024,1408]{1,0:T(8,128)(2,1)S(1)} %pad_dynamic-update-slice_fusion.own_ref), channel_id=1, source_target_pairs={{0,1},{1,0},{2,3},{3,2},{4,5},{5,4},{6,7},{7,6},{8,9},{9,8},{10,11... | collective-permute-start | bytes 8650760 | tf_op jit(solution)/shard_map/ppermute | solution.py:376
  6.4 15.9 %collective-permute-start = (bf16[1,2048]{1,0:T(2,128)(2,1)S(1)}, bf16[1,2048]{1,0:T(2,128)(2,1)S(1)}, u32[]{:S(2)}, u32[]{:S(2)}) collective-permute-start(bf16[1,2048]{1,0:T(2,128)(2,1)S(1)} %fusion.6), channel_id=1, source_target_pairs={{6,8},{14,16},{22,24},{30,32},{38,40},{46,48},{54,56},{62,64},{70,... | collective-permute-start | bytes 12296 | tf_op jit(solution)/shard_map/ppermute | solution.py:423
  12.0 19.2 %all-to-all-start.1 = ((f32[8,20,128]{2,1,0:T(8,128)}), f32[8,20,128]{2,1,0:T(8,128)S(1)}, u32[]{:S(2)}, u32[]{:S(2)}) async-start(f32[8,20,128]{2,1,0:T(8,128)} %broadcast_in_dim.33), calls=%async_computation.1 | async-start | bytes 196608 | tf_op jit(solution)/shard_map/all_to_all | solution.py:380
  32.1 14.1 %all-to-all-start = ((bf16[4,40,2048]{2,1,0:T(8,128)(2,1)}), bf16[4,40,2048]{2,1,0:T(8,128)(2,1)}, u32[]{:S(2)}, u32[]{:S(2)}) async-start(bf16[4,40,2048]{2,1,0:T(8,128)(2,1)} %broadcast_in_dim.14), calls=%async_computation | async-start | bytes 1310720 | tf_op jit(solution)/shard_map/all_to_all | solution.py:380
  47.0 20.7 %all-to-all-start.2 = ((f32[32,20,128]{2,1,0:T(8,128)}), f32[32,20,128]{2,1,0:T(8,128)S(1)}, u32[]{:S(2)}, u32[]{:S(2)}) async-start(f32[32,20,128]{2,1,0:T(8,128)} %broadcast_in_dim.34), calls=%async_computation.2 | async-start | bytes 786432 | tf_op jit(solution)/shard_map/all_to_all | solution.py:380
  67.7 1.1 copy-start.1
  68.7 0.7 copy-start.8
  69.4 0.6 copy-start.13
  74.5 0.8 copy-start.3
  75.3 0.6 copy-start.4
  75.9 0.7 copy-start.6
  76.6 0.6 copy-start.9
  77.2 0.6 copy-start.11
  77.8 44.9 %copy-start.2 = (bf16[256,2048]{1,0:T(8,128)(2,1)S(1)}, bf16[256,2048]{1,0:T(8,128)(2,1)}, u32[]{:S(2)}) copy-start(bf16[256,2048]{1,0:T(8,128)(2,1)} %own_ref.1) | copy-start | bytes 3145732
  77.8 44.9 %copy-start.5 = (bf16[128,512]{1,0:T(8,128)(2,1)S(1)}, bf16[128,512]{1,0:T(8,128)(2,1)}, u32[]{:S(2)}) copy-start(bf16[128,512]{1,0:T(8,128)(2,1)} %copy-done.4) | copy-start | bytes 393220
  77.8 23.7 %all-to-all-start.3 = ((bf16[64,32,128]{2,1,0:T(8,128)(2,1)}), bf16[64,32,128]{2,1,0:T(8,128)(2,1)S(1)}, u32[]{:S(2)}, u32[]{:S(2)}) async-start(bf16[64,32,128]{2,1,0:T(8,128)(2,1)} %copy-done.3), calls=%async_computation.3 | async-start | bytes 1048576 | tf_op jit(solution)/shard_map/all_to_all | solution.py:380
  84.2 28.7 %collective-permute-start.2 = (bf16[256,2048]{1,0:T(8,128)(2,1)}, bf16[256,2048]{1,0:T(8,128)(2,1)S(1)}, u32[]{:S(2)}, u32[]{:S(2)}) collective-permute-start(bf16[256,2048]{1,0:T(8,128)(2,1)} %own_ref.1), channel_id=1, source_target_pairs={{0,1},{1,0},{2,3},{3,2},{4,5},{5,4},{6,7},{7,6},{8,9},{9,8},{10,11... | collective-permute-start | bytes 3145736 | tf_op jit(solution)/shard_map/ppermute | solution.py:376
  104.5 18.2 %all-to-all-start.4 = ((bf16[64,16,128]{2,1,0:T(8,128)(2,1)}), bf16[64,16,128]{2,1,0:T(8,128)(2,1)S(1)}, u32[]{:S(2)}, u32[]{:S(2)}) async-start(bf16[64,16,128]{2,1,0:T(8,128)(2,1)} %owner.1), calls=%async_computation.4 | async-start | bytes 524288 | tf_op jit(solution)/shard_map/all_to_all | solution.py:380
  110.3 0.9 copy-start.7
  111.3 0.8 copy-start.10
  112.0 24.0 %copy-start.12 = (f32[1,2048]{1,0:T(1,128)S(1)}, f32[1,2048]{1,0:T(1,128)}, u32[]{:S(2)}) copy-start(f32[1,2048]{1,0:T(1,128)} %copy-done.11) | copy-start | bytes 24580

commit v2 on v1

--- a/solution.py
+++ b/solution.py
@@ -1,5 +1,3 @@
-import functools
-
 import jax
 import jax.numpy as jnp
 from jax import lax
@@ -7,6 +5,7 @@
 from jax.experimental.pallas import tpu as pltpu
 from jax.sharding import Mesh
 from jax.sharding import PartitionSpec as P
+
 
 SP = ("sp_0", "sp_1")
 ALL = ("sp_0", "sp_1", "tp")
@@ -26,7 +25,6 @@
 CTX = NSP * CTX_DEV
 XB = INNER + STATE
 XBC = INNER + 2 * STATE
-COLS = XBC + INNER + 128
 ROWS = TOK + 16
 
 f32 = jnp.float32
@@ -61,84 +59,114 @@
     return jnp.where(lanes(shape) < HD, left, right)
 
 
+def softened(p, taps, first_col, conv_ref, before_ok, after_ok):
+    width = p.shape[1]
+    cols = slice(first_col, first_col + width)
+    conv_ref[8 : 8 + TOK, :width] = p[:TOK]
+    conv_ref[0:8, :width] = jnp.broadcast_to(p[TOK : TOK + 1] * before_ok, (8, width))
+    conv_ref[8 + TOK : 16 + TOK, :width] = jnp.broadcast_to(
+        p[TOK + 1 : TOK + 2] * after_ok, (8, width)
+    )
+    summed = (
+        conv_ref[7 : 7 + TOK, :width] * taps[1:2, cols]
+        + conv_ref[8 : 8 + TOK, :width] * taps[2:3, cols]
+        + conv_ref[9 : 9 + TOK, :width] * taps[3:4, cols]
+    )
+    return silu(summed).astype(bf16)
+
+
+def ends(at):
+    return jnp.where(at > 0, 1.0, 0.0), jnp.where(at < NSP - 1, 1.0, 0.0)
+
+
+def projected(h_ref, core, own_ref, other_ref, cols):
+    mine = pl.multiple_of(core * HALF, HALF)
+    theirs = pl.multiple_of((1 - core) * HALF, HALF)
+    out = jnp.dot(h_ref[:, pl.ds(mine, HALF)], own_ref[:, cols], preferred_element_type=f32)
+    return rounded(
+        out
+        + jnp.dot(h_ref[:, pl.ds(theirs, HALF)], other_ref[:, cols], preferred_element_type=f32)
+    )
+
+
 def project_kernel(
-    place_ref, lat_ref, gain_ref, mod_ref, own_ref, other_ref, tap_ref, rate_ref,
-    send_ref, x_ref, b_ref, c_ref, z_ref, step_ref, run_ref, gate_ref,
-    h_ref, conv_ref,
+    place_ref, mod_ref, blk0_ref, blk1_ref, blk2_ref, blk3_ref, ctx_ref, misc_ref,
+    own_x, other_x, own_s, other_s,
+    send_hbm, h_hbm, xb_hbm, sr_hbm, gate_hbm,
+    send_ref, h_ref, xb_ref, sr_ref, gate_ref, conv_ref, sems,
 ):
-    core = place_ref[0]
-    at = place_ref[1]
+    def store(i, src, dst):
+        copy = pltpu.make_async_copy(src, dst, sems.at[i])
+        copy.start()
+        return copy
+
+    core, at, tp = place_ref[0], place_ref[1], place_ref[2]
+    blocks = (blk0_ref, blk1_ref, blk2_ref, blk3_ref)
+    origin = [lax.rem(tp + 4 - s, 4) for s in range(4)]
+    is_first = [jnp.where(o == 0, 1.0, 0.0) for o in origin]
+    is_last = [jnp.where(o == 3, 1.0, 0.0) for o in origin]
     mods = []
     for t in range(4):
         total = mod_ref[t]
         for y in range(1, 8):
             total = total + mod_ref[4 * y + t]
         mods.append(total)
-    squares = jnp.zeros((ROWS, 128), f32)
-    for c in range(16):
-        v = lat_ref[:, c * 128 : (c + 1) * 128].astype(f32)
-        squares = squares + v * v
-    inv = lax.rsqrt(jnp.sum(squares, axis=1, keepdims=True) * (1.0 / D) + EPSILON)
-    inv_main, inv_ctx = inv[: ROWS - 8], inv[ROWS - 8 :]
+
+    def inverse(ref):
+        squares = jnp.zeros((ref.shape[0], 128), f32)
+        for c in range(16):
+            v = ref[:, c * 128 : (c + 1) * 128].astype(f32)
+            squares = squares + v * v
+        return lax.rsqrt(jnp.sum(squares, axis=1, keepdims=True) * (1.0 / D) + EPSILON)
+
+    inv = [inverse(ref) for ref in blocks]
+    inv_ctx = inverse(ctx_ref)
+    row8 = rows_of((8, 128))
     for c in range(16):
         t, q = c // 4, c % 4
         cols = slice(c * 128, (c + 1) * 128)
-        v = lat_ref[:, cols].astype(f32)
-        gain = gain_ref[0:1, cols].astype(f32)
+        gain = misc_ref[0:1, cols]
         shift, scale = mods[t][q : q + 1], mods[t][4 + q : 5 + q]
         cshift, cscale = mods[t][8 + q : 9 + q], mods[t][12 + q : 13 + q]
-        gate_ref[0:1, cols] = mods[t][16 + q : 17 + q]
-        main = v[: ROWS - 8] * inv_main * gain * (1.0 + scale) + shift
-        ctx = v[ROWS - 8 :] * inv_ctx * gain * (1.0 + cscale) + cshift
-        h_ref[0:TOK, cols] = main[:TOK].astype(bf16)
-        h_ref[TOK:ROWS, cols] = jnp.concatenate([main[TOK:], ctx], axis=0).astype(bf16)
-    mine = pl.multiple_of(core * HALF, HALF)
-    theirs = pl.multiple_of((1 - core) * HALF, HALF)
-
-    def project(first, width):
-        cols = slice(first, first + width)
-        out = jnp.dot(h_ref[:, pl.ds(mine, HALF)], own_ref[:, cols], preferred_element_type=f32)
-        out = out + jnp.dot(
-            h_ref[:, pl.ds(theirs, HALF)], other_ref[:, cols], preferred_element_type=f32
-        )
-        return rounded(out)
-
-    dt = project(XBC + INNER, 128)
-    step = softplus(dt[:TOK])
-    step_ref[...] = step
-    log_decay = -(rate_ref[0:1, :] * step)
+        gate_ref[:, cols] = jnp.broadcast_to(mods[t][16 + q : 17 + q], (8, 128))
+        before = jnp.zeros((8, 128), f32)
+        after = jnp.zeros((8, 128), f32)
+        for s in range(4):
+            h = blocks[s][:, cols].astype(f32) * inv[s] * gain * (1.0 + scale) + shift
+            h_ref[pl.ds(pl.multiple_of(origin[s] * OWN, OWN), OWN), cols] = h[:OWN].astype(bf16)
+            before = before + h[OWN:] * is_first[s]
+            after = after + h[OWN:] * is_last[s]
+        halo = jnp.where(row8 == 0, before, pltpu.roll(after, 1, 0))
+        ctx = ctx_ref[:, cols].astype(f32) * inv_ctx * gain * (1.0 + cscale) + cshift
+        h_ref[TOK:ROWS, cols] = jnp.concatenate([halo, ctx], axis=0).astype(bf16)
+    stores = [store(0, h_ref, h_hbm), store(1, gate_ref, gate_hbm)]
+
+    p = projected(h_ref, core, own_s, other_s, slice(2 * STATE, 2 * STATE + 128))
+    step = softplus(p[:TOK])
+    ctx_dt = p[TOK + 8 :]
+    log_decay = -(misc_ref[4:5, 0:128] * step)
     ri, ci = rows_of((TOK, TOK)), lanes((TOK, TOK))
     lower = jnp.where(ri >= ci, 1.0, 0.0).astype(f32)
     upper = jnp.where(ri <= ci, 1.0, 0.0).astype(f32)
     ahead = jnp.dot(lower, log_decay, preferred_element_type=f32, precision=HIGHEST)
     behind = jnp.dot(upper, log_decay, preferred_element_type=f32, precision=HIGHEST)
     run = jnp.where(ci < HEADS, ahead, behind)
-    run_ref[...] = run
+    sr_ref[:, 0:128] = step
+    sr_ref[:, 128:256] = run
+    stores.append(store(2, sr_ref, sr_hbm))
     total = jnp.where(lanes((1, 128)) < HEADS, run[TOK - 1 : TOK], run[0:1])
     to_end = jnp.exp(total - run)
 
-    before_ok = jnp.where(at > 0, 1.0, 0.0)
-    after_ok = jnp.where(at < NSP - 1, 1.0, 0.0)
-
-    def convolved(first, width):
-        cols = slice(first, first + width)
-        p = project(first, width)
-        conv_ref[8 : 8 + TOK, cols] = p[:TOK]
-        conv_ref[0:8, cols] = jnp.broadcast_to(p[TOK : TOK + 1] * before_ok, (8, width))
-        conv_ref[8 + TOK : 16 + TOK, cols] = jnp.broadcast_to(
-            p[TOK + 1 : TOK + 2] * after_ok, (8, width)
-        )
-        summed = (
-            conv_ref[7 : 7 + TOK, cols] * tap_ref[0:1, cols]
-            + conv_ref[8 : 8 + TOK, cols] * tap_ref[1:2, cols]
-            + conv_ref[9 : 9 + TOK, cols] * tap_ref[2:3, cols]
-        )
-        return silu(summed).astype(bf16), p[TOK + 8 :]
-
-    b_in, ctx_b = convolved(INNER, STATE)
-    b_ref[...] = b_in
-    x_in, ctx_x = convolved(0, INNER)
-    x_ref[...] = x_in
+    before_ok, after_ok = ends(at)
+    p = projected(h_ref, core, own_s, other_s, slice(0, STATE))
+    ctx_b = p[TOK + 8 :]
+    b_in = softened(p, misc_ref, INNER, conv_ref, before_ok, after_ok)
+    xb_ref[:, INNER:] = b_in
+    p = projected(h_ref, core, own_x, other_x, slice(0, INNER))
+    ctx_x = p[TOK + 8 :]
+    x_in = softened(p, misc_ref, 0, conv_ref, before_ok, after_ok)
+    xb_ref[:, :INNER] = x_in
+    stores.append(store(3, xb_ref, xb_hbm))
 
     states = []
     for first in (0, HEADS):
@@ -154,11 +182,9 @@
         )
     send_ref[:, 0:16, :] = jnp.concatenate(states, axis=1).astype(bf16)
 
-    ctx_dt = dt[TOK + 8 :]
     high = rounded(total)
     low = rounded(total - high)
     lane = lanes((8, 128))
-    blocks = []
     for head in range(HEADS):
         misc = jnp.zeros((8, 128), f32)
         for spot, table, col in (
@@ -172,25 +198,33 @@
             shift = (128 - 8 * (j % 16)) % 128
             if shift:
                 chunk = pltpu.roll(chunk, shift, 1)
-            blocks.append(jnp.concatenate([ctx_b, jnp.where(lane < 8, chunk, misc)], axis=0))
-    for j in range(NSP):
-        send_ref[j, 16:32, :] = blocks[j].astype(bf16)
-
-    c_in, _ = convolved(XB, STATE)
-    c_ref[...] = c_in
-    z_ref[...] = project(XBC, INNER)[:TOK].astype(bf16)
-
-
-def inside_kernel(x_ref, b_ref, c_ref, step_ref, run_ref, y_ref):
-    step, run = step_ref[...], run_ref[...]
+            send_ref[j, 16:32, :] = jnp.concatenate(
+                [ctx_b, jnp.where(lane < 8, chunk, misc)], axis=0
+            ).astype(bf16)
+    stores.append(store(4, send_ref, send_hbm))
+    for copy in stores:
+        copy.wait()
+
+
+def inside_kernel(
+    place_ref, h_ref, own_z, other_z, own_s, other_s, xb_ref, sr_ref, misc_ref,
+    y_ref, c_out_ref, z_ref, conv_ref,
+):
+    core, at = place_ref[0], place_ref[1]
+    before_ok, after_ok = ends(at)
+    p = projected(h_ref, core, own_s, other_s, slice(STATE, 2 * STATE))
+    c_in = softened(p, misc_ref, INNER + STATE, conv_ref, before_ok, after_ok)
+    c_out_ref[...] = c_in
+    z_ref[...] = projected(h_ref, core, own_z, other_z, slice(0, INNER))[:TOK].astype(bf16)
+    step, run = sr_ref[:, 0:128], sr_ref[:, 128:256]
     turned = run.T
     scores = lax.dot_general(
-        c_ref[...], b_ref[...], (((1,), (1,)), ((), ())), preferred_element_type=f32
+        c_in, xb_ref[:, INNER:], (((1,), (1,)), ((), ())), preferred_element_type=f32
     )
     ri, ci = rows_of((TOK, TOK)), lanes((TOK, TOK))
     for q in range(4):
         cols = slice(q * 128, (q + 1) * 128)
-        x = x_ref[:, cols].astype(f32)
+        x = xb_ref[:, cols].astype(f32)
         moved = jnp.concatenate(
             [(x * per_channel(step, first, q)).astype(bf16) for first in (0, HEADS)], axis=0
         )
@@ -270,12 +304,12 @@
 
 
 def output_kernel(
-    place_ref, state_ref, c_ref, y_ref, run_ref, z_ref, gain_ref, own_ref, other_ref,
+    place_ref, state_ref, c_ref, y_ref, sr_ref, z_ref, gain_ref, own_ref, other_ref,
     out_ref, ny_ref,
 ):
     core = place_ref[0]
     states = state_ref[...].astype(f32)
-    growth = jnp.exp(run_ref[...])
+    growth = jnp.exp(sr_ref[:, 128:256])
     c_in = c_ref[...]
     ahead = states[:, 0:8, :].reshape(INNER, STATE).astype(bf16)
     behind = states[:, 8:16, :].reshape(INNER, STATE).astype(bf16)
@@ -308,46 +342,54 @@
         out_ref[:, cols] = out.astype(bf16)
 
 
-def call(kernel, out_shape, n_args, smem, scratch=(), flops=10**8, name=None):
-    vmem = pl.BlockSpec(memory_space=pltpu.VMEM)
-    in_specs = [pl.BlockSpec(memory_space=pltpu.SMEM) if i in smem else vmem for i in range(n_args)]
+def call(kernel, out_shape, n_args, smem, scratch=(), hbm=(), hbm_out=False, flops=10**8):
+    space = {i: pltpu.SMEM for i in smem} | {i: pltpu.HBM for i in hbm}
+    in_specs = [pl.BlockSpec(memory_space=space.get(i, pltpu.VMEM)) for i in range(n_args)]
+    out = pl.BlockSpec(memory_space=pltpu.HBM if hbm_out else pltpu.VMEM)
     many = isinstance(out_shape, (list, tuple))
     return pl.pallas_call(
         kernel,
         out_shape=out_shape,
         in_specs=in_specs,
-        out_specs=[vmem] * len(out_shape) if many else vmem,
+        out_specs=[out] * len(out_shape) if many else out,
         scratch_shapes=list(scratch),
         compiler_params=pltpu.CompilerParams(vmem_limit_bytes=30 * 2**20),
         cost_estimate=pl.CostEstimate(flops=flops, bytes_accessed=2**20, transcendentals=0),
         interpret=INTERPRET,
-        name=name,
     )
 
 
 def project_call(*args):
-    shape = jax.ShapeDtypeStruct
+    outs = [
+        ((NSP, 32, 128), bf16), ((ROWS, D), bf16), ((TOK, XB), bf16), ((TOK, 256), f32),
+        ((8, D), f32),
+    ]
     return call(
         project_kernel,
+        [pltpu.HBM(*o) for o in outs],
+        12,
+        (0,),
         [
-            shape((NSP, 32, 128), bf16),
-            shape((TOK, INNER), bf16),
-            shape((TOK, STATE), bf16),
-            shape((TOK, STATE), bf16),
-            shape((TOK, INNER), bf16),
-            shape((TOK, 128), f32),
-            shape((TOK, 128), f32),
-            shape((1, D), f32),
+            *(pltpu.VMEM(*o) for o in outs),
+            pltpu.VMEM((TOK + 16, INNER), f32),
+            pltpu.SemaphoreType.DMA((5,)),
         ],
-        8,
+        hbm_out=True,
+    )(*args)
+
+
+def inside_call(*args):
+    return call(
+        inside_kernel,
+        [
+            jax.ShapeDtypeStruct((TOK, INNER), f32),
+            jax.ShapeDtypeStruct((TOK, STATE), bf16),
+            jax.ShapeDtypeStruct((TOK, INNER), bf16),
+        ],
+        9,
         (0,),
-        [pltpu.VMEM((ROWS, D), bf16), pltpu.VMEM((TOK + 16, XBC), f32)],
-        name="project",
+        [pltpu.VMEM((TOK + 16, STATE), f32)],
     )(*args)
-
-
-def inside_call(*args):
-    return call(inside_kernel, jax.ShapeDtypeStruct((TOK, INNER), f32), 5, (), name="inside")(*args)
 
 
 def owner_call(*args):
@@ -357,7 +399,6 @@
         4,
         (0,),
         [pltpu.VMEM((CTX + 16, 128), f32), pltpu.VMEM((NSP, 16, 128), f32)],
-        name="owner",
     )(*args)
 
 
@@ -368,7 +409,6 @@
         9,
         (0,),
         [pltpu.VMEM((TOK, INNER), bf16)],
-        name="output",
     )(*args)
 
 
@@ -384,10 +424,23 @@
     return exchanged(jnp.broadcast_to(x[None], (peers, *x.shape)), axes)
 
 
-def joined_weights(w_x, w_b, w_c, w_z, w_dt):
+def small_weights(w_b, w_c, w_dt):
     steps = jnp.concatenate([w_dt[0], w_dt[1]], axis=1)
     steps = jnp.pad(steps, ((0, 0), (0, 128 - steps.shape[1])))
-    return jnp.concatenate([w_x, w_b, w_c, w_z, steps], axis=1)
+    return jnp.concatenate([w_b, w_c, steps], axis=1)
+
+
+def packed_vectors(norm_gain, conv_x, conv_b, conv_c, decay_rate):
+    taps = jnp.concatenate([conv_x, conv_b, conv_c], axis=1).astype(f32)
+    rates = decay_rate.reshape(1, 2 * HEADS)
+    return jnp.concatenate(
+        [
+            norm_gain.astype(f32)[None],
+            jnp.pad(taps, ((0, 0), (0, D - XBC))),
+            jnp.pad(rates, ((0, 3), (0, D - 2 * HEADS))),
+        ],
+        axis=0,
+    )
 
 
 def owner_taps(conv_x, conv_b, at):
@@ -402,8 +455,15 @@
 ):
     at = lax.axis_index(SP)
     core = lax.axis_index("dp")
-    place = jnp.stack([core, at]).astype(jnp.int32)
+    tp = lax.axis_index("tp")
+    place = jnp.stack([core, at, tp]).astype(jnp.int32)
     row_count = mod_weight.shape[1]
+
+    rows = latent[0]
+    edge = jnp.where(tp == 3, rows[OWN - 1 :], rows[:1])
+    pairs = [(4 * i + 3, 4 * i + 4) for i in range(NSP - 1)]
+    pairs += [(j, i) for i, j in pairs]
+    halo = lax.ppermute(edge, ALL, pairs)
 
     act = jnp.stack(
         [silu(condition[0].astype(f32)), silu(context_source.astype(f32))]
@@ -412,49 +472,40 @@
     part = jnp.einsum("ar,krc->akc", act, mod_weight, preferred_element_type=f32)
     part = jnp.stack([part[0, 0], part[0, 1], part[1, 0], part[1, 1], part[0, 2]])
     part = part.reshape(20, 128)
-    part = jnp.sum(sent_to_all(part, 8, "sp_0"), axis=0)
+    part = sent_to_all(part, 8, "sp_0")
+    part = jnp.sum(part, axis=0)
     mods = sent_to_all(part, 32, ("sp_1", "tp"))
 
-    rows = latent[0]
-    tp = lax.axis_index("tp")
-    edge = jnp.where(tp == 3, rows[OWN - 1 :], rows[:1])
-    pairs = [(4 * i + 3, 4 * i + 4) for i in range(NSP - 1)]
-    pairs += [(j, i) for i, j in pairs]
-    halo = lax.ppermute(edge, ALL, pairs)
     packed = jnp.concatenate([rows, jnp.pad(halo, ((0, 7), (0, 0)))], axis=0)
-    block = sent_to_all(packed, 4, "tp")
-    all_rows = jnp.concatenate(
-        [
-            block[:, :OWN].reshape(TOK, D),
-            block[0, OWN : OWN + 1],
-            block[3, OWN : OWN + 1],
-            jnp.zeros((6, D), bf16),
-            context[0],
-        ],
-        axis=0,
-    )
-
-    weights = joined_weights(w_x, w_b, w_c, w_z, w_dt)
-    other_weights = swapped(weights)
+    blocks = [packed]
+    for s in (1, 2, 3):
+        blocks.append(lax.ppermute(packed, "tp", [(i, (i + s) % 4) for i in range(4)]))
+
+    small = small_weights(w_b, w_c, w_dt)
+    other_x = swapped(w_x)
+    other_small = swapped(small)
+    other_z = swapped(w_z)
     other_out = swapped(w_out)
 
-    taps = jnp.concatenate([conv_x, conv_b, conv_c], axis=1).astype(f32)
-    rates = jnp.pad(decay_rate.reshape(1, 2 * HEADS), ((0, 0), (0, 128 - 2 * HEADS)))
+    misc = packed_vectors(norm_gain, conv_x, conv_b, conv_c, decay_rate)
     tap_b, tap_x = owner_taps(conv_x, conv_b, at)
     own_rates = lax.dynamic_slice_in_dim(decay_rate, at // 8, 1, 1)[:, 0]
 
-    send, x_in, b_in, c_in, z_in, step, run, gate = project_call(
-        place, all_rows, norm_gain[None], mods, weights, other_weights, taps, rates
+    send, h, xb, sr, gate = project_call(
+        place, mods, *blocks, context[0], misc, w_x, other_x, small, other_small
     )
     received = exchanged(send, SP)
-    y_in = inside_call(x_in, b_in, c_in, step, run)
-    states = exchanged(owner_call(own_rates, received, tap_b, tap_x), SP)
+    y_in, c_in, z_in = inside_call(
+        place, h, w_z, other_z, small, other_small, xb, sr, misc
+    )
+    entering = owner_call(own_rates, received, tap_b, tap_x)
+    states = exchanged(entering, SP)
     partial = output_call(
-        place, states, c_in, y_in, run, z_in, out_gain[None], w_out, other_out
+        place, states, c_in, y_in, sr, z_in, out_gain[None], w_out, other_out
     )
     tiles = exchanged(partial.reshape(4, OWN, D), "tp")
     mixed = jnp.sum(tiles.astype(f32), axis=0)
-    return (gate * mixed).astype(bf16)[None]
+    return (gate[0:1] * mixed).astype(bf16)[None]
 
 
 def solution(mesh):
@@ -481,6 +532,7 @@
         P("tp"),
         P(("tp", "dp"), None),
     )
+
     return jax.shard_map(
         shards, mesh=torus, in_specs=placed, out_specs=P("dp", sp_tp, None), check_vma=False
     )

time: 138 us -> 127 us (0.920)
  starting transfers between devices: 42.9 us -> 65.7 us
  local copies, waits for them, and re-layouts: 24.7 us -> 8.44 us
  blocking collectives: 11.8 us -> 0 us
  waiting for transfers between devices: 43 us -> 33.5 us
  Pallas kernels: 9.75 us -> 12.7 us
    all_to_all x5, waiting for transfers between devices: 43 us -> 29.5 us  [exchanged(): return lax.all_to_all(x, axes, 0, 0, tiled=True)]
    all_to_all x1 -> x0, blocking collectives: 11.8 us -> none  [exchanged(): return lax.all_to_all(x, axes, 0, 0, tiled=True)]
    ppermute x0 -> x3, starting transfers between devices: none -> 11.3 us  [shards(): lax.ppermute(packed, 'tp', [(i, (i + s) % 4) for i in range(4)])]
    all_to_all x5, starting transfers between devices: 34.5 us -> 41 us  [exchanged(): return lax.all_to_all(x, axes, 0, 0, tiled=True)]
    concatenate x3 -> x1, local copies, waits for them, and re-layouts: 5.44 us -> 0.17 us  [small_weights(): steps = jnp.concatenate([w_dt[0], w_dt[1]], axis=1)]
    unnamed x44 -> x42, local copies, waits for them, and re-layouts: 9.91 us -> 4.84 us
    ppermute x2 -> x4, starting transfers between devices: 3.84 us -> 8.79 us  [swapped(): return lax.ppermute(x, 'dp', [(0, 1), (1, 0)])]
    ppermute x0 -> x3, waiting for transfers between devices: none -> 3.94 us  [shards(): lax.ppermute(packed, 'tp', [(i, (i + s) % 4) for i in range(4)])]
  transfers between devices with their start and end apart: 8 -> 13, of which waited for: 5 -> 6; matrix products, arithmetic and copies ran while one was open for 13% -> 4% of each run, Pallas kernels for 3% -> 4%
where the time goes in v2:
time: 127 us; the launch traced here: 126 us
  starting transfers between devices  65.7 us (52%)
  waiting for transfers between devices  33.5 us (26%)
  Pallas kernels  12.7 us (10%)
  local copies, waits for them, and re-layouts  8.44 us (7%)
  other arithmetic  4.68 us (4%)
    all_to_all x5, starting transfers between devices, exchanged(): return lax.all_to_all(x, axes, 0, 0, tiled=True)  41 us
    all_to_all x5, waiting for transfers between devices, exchanged(): return lax.all_to_all(x, axes, 0, 0, tiled=True)  29.5 us
    ppermute x3, starting transfers between devices, shards(): lax.ppermute(packed, 'tp', [(i, (i + s) % 4) for i in range(4)])  11.3 us
    ppermute x4, starting transfers between devices, swapped(): return lax.ppermute(x, 'dp', [(0, 1), (1, 0)])  8.79 us
    unnamed x42, local copies, waits for them, and re-layouts  4.84 us
    ppermute x1, starting transfers between devices, shards(): halo = lax.ppermute(edge, ALL, pairs)  4.55 us
    pallas_call x1, Pallas kernels, project_call(): call(project_kernel, [pltpu.HBM(*o) for o in outs], 12, (0,), [*(pltpu.VM...  4.55 us
    ppermute x3, waiting for transfers between devices, shards(): lax.ppermute(packed, 'tp', [(i, (i + s) % 4) for i in range(4)])  3.94 us
  transfers between devices with their start and end apart: 13, of which 6 were waited for; matrix products, arithmetic and copies ran while one was open for 4% of the time, Pallas kernels for 4%

profile of v2, /device:TPU:8, one launch (start us, length us, event | category | flops | bytes accessed | tf_op | source)
XLA Modules:
  0.0 125.7 jit_solution(8892662730574561214)
XLA Ops:
  0.0 0.8 fusion.13
  0.8 0.7 fusion.15
  1.5 0.2 fusion.17
  1.8 0.6 broadcast_in_dim.24
  2.4 10.3 %all-to-all-start = ((f32[8,20,128]{2,1,0:T(8,128)}), f32[8,20,128]{2,1,0:T(8,128)S(1)}, u32[]{:S(2)}, u32[]{:S(2)}) async-start(f32[8,20,128]{2,1,0:T(8,128)} %broadcast_in_dim.24), calls=%async_computation | async-start | bytes 196608 | tf_op jit(solution)/shard_map/all_to_all | solution.py:420
  12.8 0.8 fusion.14
  13.6 4.6 %collective-permute-start = (bf16[1,2048]{1,0:T(2,128)(2,1)S(1)}, bf16[1,2048]{1,0:T(2,128)(2,1)S(1)}, u32[]{:S(2)}, u32[]{:S(2)}) collective-permute-start(bf16[1,2048]{1,0:T(2,128)(2,1)S(1)} %fusion.14), channel_id=1, source_target_pairs={{6,8},{14,16},{22,24},{30,32},{38,40},{46,48},{54,56},{62,64},{70,... | collective-permute-start | bytes 12296 | tf_op jit(solution)/shard_map/ppermute | solution.py:466
  18.1 1.9 %collective-permute-start.4 = (bf16[1024,512]{1,0:T(8,128)(2,1)}, bf16[1024,512]{1,0:T(8,128)(2,1)}, u32[]{:S(2)}, u32[]{:S(2)}) collective-permute-start(bf16[1024,512]{1,0:T(8,128)(2,1)} %own_x.1), channel_id=1, source_target_pairs={{0,1},{1,0},{2,3},{3,2},{4,5},{5,4},{6,7},{7,6},{8,9},{9,8},{10,11... | collective-permute-start | bytes 3145736 | tf_op jit(solution)/shard_map/ppermute | solution.py:416
  20.0 0.7 slice_bitcast_fusion.1
  20.8 0.2 copy.23
  21.0 0.0 copy-start.17
  21.0 0.1 fusion.1.own_s
  21.1 0.0 copy-start.14
  21.2 2.5 %collective-permute-start.5 = (bf16[1024,384]{1,0:T(8,128)(2,1)S(1)}, bf16[1024,384]{1,0:T(8,128)(2,1)S(1)}, u32[]{:S(2)}, u32[]{:S(2)}) collective-permute-start(bf16[1024,384]{1,0:T(8,128)(2,1)S(1)} %fusion.1.own_s), channel_id=1, source_target_pairs={{0,1},{1,0},{2,3},{3,2},{4,5},{5,4},{6,7},{7,6},{8,9},{9,8},{10,11... | collective-permute-start | bytes 2359304 | tf_op jit(solution)/shard_map/ppermute | solution.py:416
  23.8 0.8 broadcast_in_dim.25
  24.6 7.9 %all-to-all-start.1 = ((f32[32,20,128]{2,1,0:T(8,128)}), f32[32,20,128]{2,1,0:T(8,128)S(1)}, u32[]{:S(2)}, u32[]{:S(2)}) async-start(f32[32,20,128]{2,1,0:T(8,128)} %broadcast_in_dim.25), calls=%async_computation.1 | async-start | bytes 786432 | tf_op jit(solution)/shard_map/all_to_all | solution.py:420
  32.5 0.6 fusion.10
  33.1 0.1 reshape.66
  33.2 3.4 %collective-permute-start.1 = (bf16[40,2048]{1,0:T(8,128)(2,1)S(1)}, bf16[40,2048]{1,0:T(8,128)(2,1)S(1)}, u32[]{:S(2)}, u32[]{:S(2)}) collective-permute-start(bf16[40,2048]{1,0:T(8,128)(2,1)S(1)} %fusion.4.blk0_ref), channel_id=1, source_target_pairs={{0,2},{2,4},{4,6},{6,0},{1,3},{3,5},{5,7},{7,1},{8,10},{10,12},{12... | collective-permute-start | bytes 491528 | tf_op jit(solution)/shard_map/ppermute | solution.py:482
  36.6 4.6 %collective-permute-start.2 = (bf16[40,2048]{1,0:T(8,128)(2,1)S(1)}, bf16[40,2048]{1,0:T(8,128)(2,1)}, u32[]{:S(2)}, u32[]{:S(2)}) collective-permute-start(bf16[40,2048]{1,0:T(8,128)(2,1)S(1)} %fusion.4.blk0_ref), channel_id=1, source_target_pairs={{0,4},{2,6},{4,0},{6,2},{1,5},{3,7},{5,1},{7,3},{8,12},{10,14},{12... | collective-permute-start | bytes 491528 | tf_op jit(solution)/shard_map/ppermute | solution.py:482
  41.2 3.4 %collective-permute-start.3 = (bf16[40,2048]{1,0:T(8,128)(2,1)S(1)}, bf16[40,2048]{1,0:T(8,128)(2,1)}, u32[]{:S(2)}, u32[]{:S(2)}) collective-permute-start(bf16[40,2048]{1,0:T(8,128)(2,1)S(1)} %fusion.4.blk0_ref), channel_id=1, source_target_pairs={{0,6},{2,0},{4,2},{6,4},{1,7},{3,1},{5,3},{7,5},{8,14},{10,8},{12,... | collective-permute-start | bytes 491528 | tf_op jit(solution)/shard_map/ppermute | solution.py:482
  44.6 0.8 select_maximum_fusion.misc_ref
  45.4 0.1 pad_add_fusion.place_ref
  45.5 0.1 collective-permute-done.1.blk1_ref
  45.5 3.5 %collective-permute-done.2.blk2_ref = bf16[40,2048]{1,0:T(8,128)(2,1)} collective-permute-done((bf16[40,2048]{1,0:T(8,128)(2,1)S(1)}, bf16[40,2048]{1,0:T(8,128)(2,1)}, u32[]{:S(2)}, u32[]{:S(2)}) %collective-permute-start.2) | collective-permute-done | bytes 163872 | tf_op jit(solution)/shard_map/ppermute | solution.py:482
  49.0 0.4 collective-permute-done.3.blk3_ref
  49.4 4.5 %shard_map.163 = (bf16[64,32,128]{2,1,0:T(8,128)(2,1)}, bf16[144,2048]{1,0:T(8,128)(2,1)}, bf16[128,640]{1,0:T(8,128)(2,1)}, f32[128,256]{1,0:T(8,128)}, f32[8,2048]{1,0:T(8,128)}) custom-call(s32[3]{0:T(128)S(1)} %pad_add_fusion.place_ref, f32[32,20,128]{2,1,0:T(8,128)S(1)} %all-to-all-done.1.mod_ref, bf16[40,2048]{1,0:T(8,128)(2,1)S(1)} %fusion.4.blk0_ref, ...), custom_call_target="tpu_custom_call" | custom-call | flops 100000000 | bytes 1048576 | tf_op jit(solution)/shard_map/pallas_call | solution.py:367
  54.0 12.5 %all-to-all-start.2 = ((bf16[64,32,128]{2,1,0:T(8,128)(2,1)}), bf16[64,32,128]{2,1,0:T(8,128)(2,1)S(1)}, u32[]{:S(2)}, u32[]{:S(2)}) async-start(bf16[64,32,128]{2,1,0:T(8,128)(2,1)} %get-tuple-element.14), calls=%async_computation.2 | async-start | bytes 1048576 | tf_op jit(solution)/shard_map/all_to_all | solution.py:420
  66.5 1.9 %collective-permute-start.6 = (bf16[1024,512]{1,0:T(8,128)(2,1)S(1)}, bf16[1024,512]{1,0:T(8,128)(2,1)}, u32[]{:S(2)}, u32[]{:S(2)}) collective-permute-start(bf16[1024,512]{1,0:T(8,128)(2,1)S(1)} %copy-done.2), channel_id=1, source_target_pairs={{0,1},{1,0},{2,3},{3,2},{4,5},{5,4},{6,7},{7,6},{8,9},{9,8},{10,11... | collective-permute-start | bytes 3145736 | tf_op jit(solution)/shard_map/ppermute | solution.py:416
  68.5 2.4 %collective-permute-start.7 = (bf16[256,2048]{1,0:T(8,128)(2,1)}, bf16[256,2048]{1,0:T(8,128)(2,1)}, u32[]{:S(2)}, u32[]{:S(2)}) collective-permute-start(bf16[256,2048]{1,0:T(8,128)(2,1)} %own_ref.1), channel_id=1, source_target_pairs={{0,1},{1,0},{2,3},{3,2},{4,5},{5,4},{6,7},{7,6},{8,9},{9,8},{10,11... | collective-permute-start | bytes 3145736 | tf_op jit(solution)/shard_map/ppermute | solution.py:416
  70.9 0.2 dynamic-slice_reduce_fusion.rate_ref
  71.1 0.1 constant_dynamic-slice_fusion
  71.2 14.0 %all-to-all-done.2.recv_ref = bf16[64,32,128]{2,1,0:T(8,128)(2,1)S(1)} async-done(((bf16[64,32,128]{2,1,0:T(8,128)(2,1)}), bf16[64,32,128]{2,1,0:T(8,128)(2,1)S(1)}, u32[]{:S(2)}, u32[]{:S(2)}) %all-to-all-start.2) | async-done | bytes 524320 | tf_op jit(solution)/shard_map/all_to_all | solution.py:420
  85.3 3.0 %shard_map.164 = bf16[64,16,128]{2,1,0:T(8,128)(2,1)} custom-call(f32[2]{0:T(128)S(1)} %dynamic-slice_reduce_fusion.rate_ref, bf16[64,32,128]{2,1,0:T(8,128)(2,1)S(1)} %all-to-all-done.2.recv_ref, f32[3,128]{1,0:T(4,128)S(1)} %convert_element_type.39.tap_b_ref, f32[3,128]{1,0:T(4,128)S(1)} %pad_convert_fusion.tap_x_ref), custom_call_target="tpu_custom_call" | custom-call | flops 100000000 | bytes 1048576 | tf_op jit(solution)/shard_map/pallas_call | solution.py:396
  88.2 5.2 %all-to-all-start.3 = ((bf16[64,16,128]{2,1,0:T(8,128)(2,1)}), bf16[64,16,128]{2,1,0:T(8,128)(2,1)S(1)}, u32[]{:S(2)}, u32[]{:S(2)}) async-start(bf16[64,16,128]{2,1,0:T(8,128)(2,1)} %shard_map.164), calls=%async_computation.3 | async-start | bytes 524288 | tf_op jit(solution)/shard_map/all_to_all | solution.py:420
  93.5 1.1 copy-done.4
  94.6 0.9 copy-done.6
  95.5 2.3 %shard_map.165 = (f32[128,512]{1,0:T(8,128)S(1)}, bf16[128,128]{1,0:T(8,128)(2,1)S(1)}, bf16[128,512]{1,0:T(8,128)(2,1)S(1)}) custom-call(s32[3]{0:T(128)S(1)} %pad_add_fusion.place_ref, bf16[144,2048]{1,0:T(8,128)(2,1)S(1)} %copy-done.4, bf16[1024,512]{1,0:T(8,128)(2,1)S(1)} %copy-done.2, bf16[1024,512]{1,0:T(8,128)(2,1)} %collective-permute-done.6.other_z, ...), custom_call_target="tpu_custom_call" | custom-call | flops 100000000 | bytes 1048576 | tf_op jit(solution)/shard_map/pallas_call | solution.py:382
  97.8 0.6 copy-done.7
  98.4 8.2 %all-to-all-done.3.state_ref = bf16[64,16,128]{2,1,0:T(8,128)(2,1)S(1)} async-done(((bf16[64,16,128]{2,1,0:T(8,128)(2,1)}), bf16[64,16,128]{2,1,0:T(8,128)(2,1)S(1)}, u32[]{:S(2)}, u32[]{:S(2)}) %all-to-all-start.3) | async-done | bytes 262176 | tf_op jit(solution)/shard_map/all_to_all | solution.py:420
  106.6 1.2 copy-done.3
  107.9 0.9 copy-done.8
  108.8 3.0 %shard_map.166 = bf16[128,2048]{1,0:T(8,128)(2,1)} custom-call(s32[3]{0:T(128)S(1)} %pad_add_fusion.place_ref, bf16[64,16,128]{2,1,0:T(8,128)(2,1)S(1)} %all-to-all-done.3.state_ref, bf16[128,128]{1,0:T(8,128)(2,1)S(1)} %get-tuple-element.18.c_ref, f32[128,512]{1,0:T(8,128)S(1)} %get-tuple-element.19.y_ref, f32[128,256]{1,0:T(8,128)S(1)} %copy-done.5, ...), custom_call_target="tpu_custom_call" | custom-call | flops 100000000 | bytes 1048576 | tf_op jit(solution)/shard_map/pallas_call | solution.py:406
  111.7 5.1 %all-to-all-start.4 = ((bf16[4,32,2048]{2,1,0:T(8,128)(2,1)}), bf16[4,32,2048]{2,1,0:T(8,128)(2,1)S(1)}, u32[]{:S(2)}, u32[]{:S(2)}) async-start(bf16[4,32,2048]{2,1,0:T(8,128)(2,1)} %bitcast.16), calls=%async_computation.4 | async-start | bytes 1048576 | tf_op jit(solution)/shard_map/all_to_all | solution.py:420
  116.8 0.8 slice.41
  117.7 7.2 %all-to-all-done.4 = bf16[4,32,2048]{2,1,0:T(8,128)(2,1)S(1)} async-done(((bf16[4,32,2048]{2,1,0:T(8,128)(2,1)}), bf16[4,32,2048]{2,1,0:T(8,128)(2,1)S(1)}, u32[]{:S(2)}, u32[]{:S(2)}) %all-to-all-start.4) | async-done | bytes 524320 | tf_op jit(solution)/shard_map/all_to_all | solution.py:420
  124.9 0.1 convert_reduce_fusion
  125.0 0.7 fusion.3
  (53 shorter events, 0.2 us)
Async XLA Ops:
  0.0 1.5 %copy-start = (bf16[3,32,512]{2,1,0:T(8,128)(2,1)S(1)}, bf16[3,32,512]{2,1,0:T(8,128)(2,1)}, u32[]{:S(2)}) copy-start(bf16[3,32,512]{2,1,0:T(8,128)(2,1)} %param.21) | copy-start | bytes 294916
  0.0 21.0 %copy-start.11 = (bf16[1024,128]{1,0:T(8,128)(2,1)S(1)}, bf16[1024,128]{1,0:T(8,128)(2,1)}, u32[]{:S(2)}) copy-start(bf16[1024,128]{1,0:T(8,128)(2,1)} %param.24) | copy-start | bytes 786436
  0.0 21.0 %copy-start.10 = (bf16[1024,128]{1,0:T(8,128)(2,1)S(1)}, bf16[1024,128]{1,0:T(8,128)(2,1)}, u32[]{:S(2)}) copy-start(bf16[1024,128]{1,0:T(8,128)(2,1)} %param.25) | copy-start | bytes 786436
  2.4 21.3 %all-to-all-start = ((f32[8,20,128]{2,1,0:T(8,128)}), f32[8,20,128]{2,1,0:T(8,128)S(1)}, u32[]{:S(2)}, u32[]{:S(2)}) async-start(f32[8,20,128]{2,1,0:T(8,128)} %broadcast_in_dim.24), calls=%async_computation | async-start | bytes 196608 | tf_op jit(solution)/shard_map/all_to_all | solution.py:420
  13.6 19.7 %collective-permute-start = (bf16[1,2048]{1,0:T(2,128)(2,1)S(1)}, bf16[1,2048]{1,0:T(2,128)(2,1)S(1)}, u32[]{:S(2)}, u32[]{:S(2)}) collective-permute-start(bf16[1,2048]{1,0:T(2,128)(2,1)S(1)} %fusion.14), channel_id=1, source_target_pairs={{6,8},{14,16},{22,24},{30,32},{38,40},{46,48},{54,56},{62,64},{70,... | collective-permute-start | bytes 12296 | tf_op jit(solution)/shard_map/ppermute | solution.py:466
  18.1 31.3 %collective-permute-start.4 = (bf16[1024,512]{1,0:T(8,128)(2,1)}, bf16[1024,512]{1,0:T(8,128)(2,1)}, u32[]{:S(2)}, u32[]{:S(2)}) collective-permute-start(bf16[1024,512]{1,0:T(8,128)(2,1)} %own_x.1), channel_id=1, source_target_pairs={{0,1},{1,0},{2,3},{3,2},{4,5},{5,4},{6,7},{7,6},{8,9},{9,8},{10,11... | collective-permute-start | bytes 3145736 | tf_op jit(solution)/shard_map/ppermute | solution.py:416
  21.0 11.5 %copy-start.13 = (bf16[3,512]{1,0:T(4,128)(2,1)S(1)}, bf16[3,512]{1,0:T(4,128)(2,1)}, u32[]{:S(2)}) copy-start(bf16[3,512]{1,0:T(4,128)(2,1)} %param.28) | copy-start | bytes 9220
  21.0 11.5 %copy-start.15 = (bf16[3,128]{1,0:T(4,128)(2,1)S(1)}, bf16[3,128]{1,0:T(4,128)(2,1)}, u32[]{:S(2)}) copy-start(bf16[3,128]{1,0:T(4,128)(2,1)} %param.29) | copy-start | bytes 2308
  21.0 11.5 %copy-start.17 = (bf16[3,128]{1,0:T(4,128)(2,1)S(1)}, bf16[3,128]{1,0:T(4,128)(2,1)}, u32[]{:S(2)}) copy-start(bf16[3,128]{1,0:T(4,128)(2,1)} %param.30) | copy-start | bytes 2308
  21.1 12.0 %copy-start.14 = (bf16[2048]{0:T(1024)(128)(2,1)S(1)}, bf16[2048]{0:T(1024)(128)(2,1)}, u32[]{:S(2)}) copy-start(bf16[2048]{0:T(1024)(128)(2,1)} %param.22) | copy-start | bytes 12292
  21.2 12.0 %copy-start.19 = (f32[2,8]{1,0:T(2,128)S(1)}, f32[2,8]{1,0:T(2,128)}, u32[]{:S(2)}) copy-start(f32[2,8]{1,0:T(2,128)} %param.31) | copy-start | bytes 196
  21.2 12.0 %copy-start.12 = (bf16[1,32,2048]{2,1,0:T(8,128)(2,1)S(1)}, bf16[1,32,2048]{2,1,0:T(8,128)(2,1)}, u32[]{:S(2)}) copy-start(bf16[1,32,2048]{2,1,0:T(8,128)(2,1)} %param.17) | copy-start | bytes 393220
  21.2 28.2 %copy-start.1 = (bf16[1024,512]{1,0:T(8,128)(2,1)S(1)}, bf16[1024,512]{1,0:T(8,128)(2,1)}, u32[]{:S(2)}) copy-start(bf16[1024,512]{1,0:T(8,128)(2,1)} %own_x.1) | copy-start | bytes 3145732
  21.2 28.2 %copy-start.9 = (bf16[1,8,2048]{2,1,0:T(8,128)(2,1)S(1)}, bf16[1,8,2048]{2,1,0:T(8,128)(2,1)}, u32[]{:S(2)}) copy-start(bf16[1,8,2048]{2,1,0:T(8,128)(2,1)} %param.19) | copy-start | bytes 98308
  21.2 28.2 %collective-permute-start.5 = (bf16[1024,384]{1,0:T(8,128)(2,1)S(1)}, bf16[1024,384]{1,0:T(8,128)(2,1)S(1)}, u32[]{:S(2)}, u32[]{:S(2)}) collective-permute-start(bf16[1024,384]{1,0:T(8,128)(2,1)S(1)} %fusion.1.own_s), channel_id=1, source_target_pairs={{0,1},{1,0},{2,3},{3,2},{4,5},{5,4},{6,7},{7,6},{8,9},{9,8},{10,11... | collective-permute-start | bytes 2359304 | tf_op jit(solution)/shard_map/ppermute | solution.py:416
  24.6 24.8 %all-to-all-start.1 = ((f32[32,20,128]{2,1,0:T(8,128)}), f32[32,20,128]{2,1,0:T(8,128)S(1)}, u32[]{:S(2)}, u32[]{:S(2)}) async-start(f32[32,20,128]{2,1,0:T(8,128)} %broadcast_in_dim.25), calls=%async_computation.1 | async-start | bytes 786432 | tf_op jit(solution)/shard_map/all_to_all | solution.py:420
  33.2 12.3 %collective-permute-start.1 = (bf16[40,2048]{1,0:T(8,128)(2,1)S(1)}, bf16[40,2048]{1,0:T(8,128)(2,1)S(1)}, u32[]{:S(2)}, u32[]{:S(2)}) collective-permute-start(bf16[40,2048]{1,0:T(8,128)(2,1)S(1)} %fusion.4.blk0_ref), channel_id=1, source_target_pairs={{0,2},{2,4},{4,6},{6,0},{1,3},{3,5},{5,7},{7,1},{8,10},{10,12},{12... | collective-permute-start | bytes 491528 | tf_op jit(solution)/shard_map/ppermute | solution.py:482
  36.6 12.4 %collective-permute-start.2 = (bf16[40,2048]{1,0:T(8,128)(2,1)S(1)}, bf16[40,2048]{1,0:T(8,128)(2,1)}, u32[]{:S(2)}, u32[]{:S(2)}) collective-permute-start(bf16[40,2048]{1,0:T(8,128)(2,1)S(1)} %fusion.4.blk0_ref), channel_id=1, source_target_pairs={{0,4},{2,6},{4,0},{6,2},{1,5},{3,7},{5,1},{7,3},{8,12},{10,14},{12... | collective-permute-start | bytes 491528 | tf_op jit(solution)/shard_map/ppermute | solution.py:482
  41.2 8.2 %collective-permute-start.3 = (bf16[40,2048]{1,0:T(8,128)(2,1)S(1)}, bf16[40,2048]{1,0:T(8,128)(2,1)}, u32[]{:S(2)}, u32[]{:S(2)}) collective-permute-start(bf16[40,2048]{1,0:T(8,128)(2,1)S(1)} %fusion.4.blk0_ref), channel_id=1, source_target_pairs={{0,6},{2,0},{4,2},{6,4},{1,7},{3,1},{5,3},{7,5},{8,14},{10,8},{12,... | collective-permute-start | bytes 491528 | tf_op jit(solution)/shard_map/ppermute | solution.py:482
  54.0 12.6 %copy-start.2 = (bf16[1024,512]{1,0:T(8,128)(2,1)S(1)}, bf16[1024,512]{1,0:T(8,128)(2,1)}, u32[]{:S(2)}) copy-start(bf16[1024,512]{1,0:T(8,128)(2,1)} %own_z.1) | copy-start | bytes 3145732
  54.0 16.9 %copy-start.16 = (bf16[3,128]{1,0:T(4,128)(2,1)S(1)}, bf16[3,128]{1,0:T(4,128)(2,1)}, u32[]{:S(2)}) copy-start(bf16[3,128]{1,0:T(4,128)(2,1)} %param.29) | copy-start | bytes 2308
  54.0 16.9 %copy-start.20 = (f32[2,8]{1,0:T(2,128)S(1)}, f32[2,8]{1,0:T(2,128)}, u32[]{:S(2)}) copy-start(f32[2,8]{1,0:T(2,128)} %param.31) | copy-start | bytes 196
  54.0 39.4 %copy-start.18 = (bf16[512]{0:T(512)(128)(2,1)S(1)}, bf16[512]{0:T(512)(128)(2,1)}, u32[]{:S(2)}) copy-start(bf16[512]{0:T(512)(128)(2,1)} %param.32) | copy-start | bytes 3076
  54.0 39.4 %copy-start.5 = (f32[128,256]{1,0:T(8,128)S(1)}, f32[128,256]{1,0:T(8,128)}, u32[]{:S(2)}) copy-start(f32[128,256]{1,0:T(8,128)} %get-tuple-element.17.sr_ref) | copy-start | bytes 393220
  54.0 31.2 %all-to-all-start.2 = ((bf16[64,32,128]{2,1,0:T(8,128)(2,1)}), bf16[64,32,128]{2,1,0:T(8,128)(2,1)S(1)}, u32[]{:S(2)}, u32[]{:S(2)}) async-start(bf16[64,32,128]{2,1,0:T(8,128)(2,1)} %get-tuple-element.14), calls=%async_computation.2 | async-start | bytes 1048576 | tf_op jit(solution)/shard_map/all_to_all | solution.py:420
  66.5 26.9 %collective-permute-start.6 = (bf16[1024,512]{1,0:T(8,128)(2,1)S(1)}, bf16[1024,512]{1,0:T(8,128)(2,1)}, u32[]{:S(2)}, u32[]{:S(2)}) collective-permute-start(bf16[1024,512]{1,0:T(8,128)(2,1)S(1)} %copy-done.2), channel_id=1, source_target_pairs={{0,1},{1,0},{2,3},{3,2},{4,5},{5,4},{6,7},{7,6},{8,9},{9,8},{10,11... | collective-permute-start | bytes 3145736 | tf_op jit(solution)/shard_map/ppermute | solution.py:416
  68.5 29.9 %collective-permute-start.7 = (bf16[256,2048]{1,0:T(8,128)(2,1)}, bf16[256,2048]{1,0:T(8,128)(2,1)}, u32[]{:S(2)}, u32[]{:S(2)}) collective-permute-start(bf16[256,2048]{1,0:T(8,128)(2,1)} %own_ref.1), channel_id=1, source_target_pairs={{0,1},{1,0},{2,3},{3,2},{4,5},{5,4},{6,7},{7,6},{8,9},{9,8},{10,11... | collective-permute-start | bytes 3145736 | tf_op jit(solution)/shard_map/ppermute | solution.py:416
  88.2 18.4 %all-to-all-start.3 = ((bf16[64,16,128]{2,1,0:T(8,128)(2,1)}), bf16[64,16,128]{2,1,0:T(8,128)(2,1)S(1)}, u32[]{:S(2)}, u32[]{:S(2)}) async-start(bf16[64,16,128]{2,1,0:T(8,128)(2,1)} %shard_map.164), calls=%async_computation.3 | async-start | bytes 524288 | tf_op jit(solution)/shard_map/all_to_all | solution.py:420
  93.5 1.1 copy-start.4
  94.6 0.9 copy-start.6
  97.7 0.7 copy-start.7
  106.6 1.2 copy-start.3
  107.9 0.9 copy-start.8
  111.7 13.2 %all-to-all-start.4 = ((bf16[4,32,2048]{2,1,0:T(8,128)(2,1)}), bf16[4,32,2048]{2,1,0:T(8,128)(2,1)S(1)}, u32[]{:S(2)}, u32[]{:S(2)}) async-start(bf16[4,32,2048]{2,1,0:T(8,128)(2,1)} %bitcast.16), calls=%async_computation.4 | async-start | bytes 1048576 | tf_op jit(solution)/shard_map/all_to_all | solution.py:420

commit v3 on v2

--- a/solution.py
+++ b/solution.py
@@ -107,9 +107,9 @@
     is_last = [jnp.where(o == 3, 1.0, 0.0) for o in origin]
     mods = []
     for t in range(4):
-        total = mod_ref[t]
+        total = mod_ref[t].astype(f32)
         for y in range(1, 8):
-            total = total + mod_ref[4 * y + t]
+            total = total + mod_ref[4 * y + t].astype(f32)
         mods.append(total)
 
     def inverse(ref):
@@ -168,39 +168,45 @@
     xb_ref[:, :INNER] = x_in
     stores.append(store(3, xb_ref, xb_hbm))
 
-    states = []
-    for first in (0, HEADS):
-        parts = []
-        for q in range(4):
-            moved = rounded(x_in[:, q * 128 : (q + 1) * 128].astype(f32) * per_channel(step, first, q))
-            parts.append((moved * per_channel(to_end, first, q)).astype(bf16))
-        states.append(
-            lax.dot_general(
-                jnp.concatenate(parts, axis=1), b_in, (((0,), (0,)), ((), ())),
-                preferred_element_type=f32,
-            ).reshape(NSP, 8, STATE)
-        )
-    send_ref[:, 0:16, :] = jnp.concatenate(states, axis=1).astype(bf16)
-
     high = rounded(total)
     low = rounded(total - high)
     lane = lanes((8, 128))
+    turned_b = [
+        pltpu.roll(ctx_b, (64 - 16 * c) % 128, 1) if c != 4 else ctx_b for c in range(8)
+    ]
     for head in range(HEADS):
         misc = jnp.zeros((8, 128), f32)
         for spot, table, col in (
-            (8, ctx_dt, head), (9, ctx_dt, HEADS + head), (10, high, head), (11, low, head),
-            (12, high, HEADS + head), (13, low, HEADS + head),
+            (80, ctx_dt, head), (81, ctx_dt, HEADS + head), (82, high, head), (83, low, head),
+            (84, high, HEADS + head), (85, low, HEADS + head),
         ):
             misc = jnp.where(lane == spot, table[:, col : col + 1], misc)
-        for k in range(8):
-            j = head * 8 + k
-            chunk = ctx_x[:, (j // 16) * 128 : (j // 16 + 1) * 128]
-            shift = (128 - 8 * (j % 16)) % 128
-            if shift:
-                chunk = pltpu.roll(chunk, shift, 1)
-            send_ref[j, 16:32, :] = jnp.concatenate(
-                [ctx_b, jnp.where(lane < 8, chunk, misc)], axis=0
-            ).astype(bf16)
+        chunk = ctx_x[:, (head // 2) * 128 : (head // 2 + 1) * 128]
+        if head % 2:
+            chunk = pltpu.roll(chunk, HD, 1)
+        misc = jnp.where(lane < HD, chunk, misc)
+        for c in range(8):
+            tile = jnp.where((lane >= 64) & (lane < 80), turned_b[c], misc)
+            send_ref[head * 8 + c, 16:24, :] = tile.astype(bf16)
+
+    left = ci < HD
+    for q in range(4):
+        sides = []
+        for first in (0, HEADS):
+            moved = rounded(x_in[:, q * 128 : (q + 1) * 128].astype(f32) * per_channel(step, first, q))
+            ended = (moved * per_channel(to_end, first, q)).astype(bf16)
+            sides.append(
+                lax.dot_general(
+                    b_in, ended, (((0,), (0,)), ((), ())), preferred_element_type=f32
+                )
+            )
+        ahead, behind = sides
+        for k, state in (
+            (0, jnp.where(left, ahead, pltpu.roll(behind, HD, 1))),
+            (1, jnp.where(left, pltpu.roll(ahead, HD, 1), behind)),
+        ):
+            head = 2 * q + k
+            send_ref[head * 8 : head * 8 + 8, 0:16, :] = state.astype(bf16).reshape(8, 16, 128)
     stores.append(store(4, send_ref, send_hbm))
     for copy in stores:
         copy.wait()
@@ -242,89 +248,90 @@
         y_ref[:, cols] = jnp.where(ci < HD, outs[0], outs[1])
 
 
-def owner_kernel(rate_ref, recv_ref, tap_b_ref, tap_x_ref, out_ref, pad_ref, held_ref):
-    def conv(values, tap_ref):
-        pad_ref[0:8, :] = jnp.zeros((8, 128), f32)
-        pad_ref[8 + CTX : 16 + CTX, :] = jnp.zeros((8, 128), f32)
-        pad_ref[8 : 8 + CTX, :] = values
-        summed = (
-            pad_ref[7 : 7 + CTX, :] * tap_ref[0:1, :]
-            + values * tap_ref[1:2, :]
-            + pad_ref[9 : 9 + CTX, :] * tap_ref[2:3, :]
-        )
-        return silu(summed)
-
-    both = recv_ref[:, 16:32, :].astype(f32)
-    raw_b = both[:, 0:8, :].reshape(CTX, 128)
-    misc = both[:, 8:16, :].reshape(CTX, 128)
-    ctx_b = conv(raw_b, tap_b_ref).astype(bf16)
-    ctx_x = rounded(conv(misc, tap_x_ref))
-    step = softplus(misc)
+def owner_kernel(rate_ref, recv_ref, tap_ref, out_ref, pad_ref, held_ref):
+    raw = recv_ref[:, 16:24, :].astype(f32).reshape(CTX, 128)
+    pad_ref[0:8, :] = jnp.zeros((8, 128), f32)
+    pad_ref[8 + CTX : 16 + CTX, :] = jnp.zeros((8, 128), f32)
+    pad_ref[8 : 8 + CTX, :] = raw
+    act = silu(
+        pad_ref[7 : 7 + CTX, :] * tap_ref[0:1, :]
+        + raw * tap_ref[1:2, :]
+        + pad_ref[9 : 9 + CTX, :] * tap_ref[2:3, :]
+    ).astype(bf16)
     lane = lanes((CTX, 128))
-    decay = -jnp.where(lane == 8, rate_ref[0] * step, rate_ref[1] * step)
-    wide = jnp.where(lane < HD, decay[:, 8:9], decay[:, 9:10])
-    high = rounded(wide)
-    mid = rounded(wide - high)
-    low = rounded(wide - high - mid)
+    left = lane < HD
+    step = softplus(jnp.where(left, raw[:, 80:81], raw[:, 81:82]))
+    rate = jnp.where(left, rate_ref[0], rate_ref[1])
+    decay = -(rate * step)
+    high = rounded(decay)
+    mid = rounded(decay - high)
     spot = lane % 4
-    parts = jnp.where(spot == 0, high, jnp.where(spot == 1, mid, jnp.where(spot == 2, low, 0.0)))
-    parts = parts.astype(bf16)
-    ri, ci = rows_of((CTX, CTX)), lanes((CTX, CTX))
-    later = jnp.where(ci > ri, 1.0, 0.0).astype(bf16)
-    earlier = jnp.where(ci < ri, 1.0, 0.0).astype(bf16)
-    fsum = jnp.dot(later, parts, preferred_element_type=f32)
-    bsum = jnp.dot(earlier, parts, preferred_element_type=f32)
-    wf = jnp.exp(fsum[:, 0:1] + fsum[:, 1:2] + fsum[:, 2:3])
-    wb = jnp.exp(bsum[:, 64:65] + bsum[:, 65:66] + bsum[:, 66:67])
-    xf = rounded(ctx_x * step[:, 8:9]) * wf
-    xb = rounded(ctx_x * step[:, 9:10]) * wb
-    x16 = jnp.where(lane < 8, xf, pltpu.roll(xb, 8, 1))
-    x_high = rounded(x16)
-    x_low = x16 - x_high
-    x32 = jnp.where(lane < 16, x_high, jnp.where(lane < 32, pltpu.roll(x_low, 16, 1), 0.0))
-    start = lax.dot_general(
-        x32.astype(bf16), ctx_b, (((0,), (0,)), ((), ())), preferred_element_type=f32
-    )
-    ahead = start[0:8] + start[16:24]
-    behind = start[8:16] + start[24:32]
-    grow_f = jnp.exp(jnp.broadcast_to(misc[:, 10:11] + misc[:, 11:12], (CTX, 128))).reshape(
-        NSP, 8, 128
-    )
-    grow_b = jnp.exp(jnp.broadcast_to(misc[:, 12:13] + misc[:, 13:14], (CTX, 128))).reshape(
-        NSP, 8, 128
-    )
-    fresh = recv_ref[:, 0:16, :].astype(f32)
+    parts = jnp.where(
+        spot == 0, high, jnp.where(spot == 1, mid, jnp.where(spot == 2, decay - high - mid, 0.0))
+    ).astype(bf16)
+    earlier = jnp.where(lanes((CTX, CTX)) < rows_of((CTX, CTX)), 1.0, 0.0).astype(bf16)
+    sums = jnp.dot(earlier, parts, preferred_element_type=f32)
+    before_f = sums[:, 0:1] + sums[:, 1:2] + sums[:, 2:3]
+    before_b = sums[:, 64:65] + sums[:, 65:66] + sums[:, 66:67]
+    upto_f = before_f + decay[:, 0:1]
+    later_f = jnp.minimum(upto_f[CTX - 1 :] - upto_f, 0.0)
+    act_wide = act.astype(f32)
+    moved = rounded(jnp.where(left, act_wide, pltpu.roll(act_wide, HD, 1)) * step)
+    moved = moved * jnp.exp(jnp.where(left, later_f, before_b))
+    top = rounded(moved)
+    dims = (((0,), (0,)), ((), ()))
+    start = lax.dot_general(act, top.astype(bf16), dims, preferred_element_type=f32)
+    start = start + lax.dot_general(
+        act, (moved - top).astype(bf16), dims, preferred_element_type=f32
+    )
+    state = start[64:80]
+    grow = jnp.exp(
+        jnp.where(left, raw[:, 82:83] + raw[:, 83:84], raw[:, 84:85] + raw[:, 85:86])
+    ).reshape(NSP, 8, 128)
+    left8, left16 = lanes((8, 128)) < HD, lanes((16, 128)) < HD
     for k in range(NSP):
         m = NSP - 1 - k
-        held_ref[k, 0:8, :] = ahead
-        held_ref[m, 8:16, :] = behind
-        ahead = ahead * grow_f[k] + fresh[k, 0:8]
-        behind = behind * grow_b[m] + fresh[m, 8:16]
+        held_ref[k, :, 0:HD] = state[:, 0:HD]
+        held_ref[m, :, HD:128] = state[:, HD:128]
+        fresh = jnp.where(left16, recv_ref[k, 0:16, :].astype(f32), recv_ref[m, 0:16, :].astype(f32))
+        growth = jnp.where(left8, grow[k], grow[m])
+        state = state * jnp.concatenate([growth, growth], axis=0) + fresh
     out_ref[...] = held_ref[...].astype(bf16)
 
 
 def output_kernel(
-    place_ref, state_ref, c_ref, y_ref, sr_ref, z_ref, gain_ref, own_ref, other_ref,
-    out_ref, ny_ref,
+    place_ref, state_ref, gain_ref, c_hbm, sr_hbm, y_hbm, z_hbm, own_hbm, other_hbm,
+    out_ref, ny_ref, c_ref, sr_ref, y_ref, z_ref, own_ref, other_ref, sems,
 ):
+    loads = [
+        pltpu.make_async_copy(src, dst, sems.at[i])
+        for i, (src, dst) in enumerate(
+            (
+                (c_hbm, c_ref), (sr_hbm, sr_ref), (y_hbm, y_ref), (z_hbm, z_ref),
+                (own_hbm, own_ref), (other_hbm, other_ref),
+            )
+        )
+    ]
+    for copy in loads:
+        copy.start()
     core = place_ref[0]
-    states = state_ref[...].astype(f32)
+    for copy in loads[:4]:
+        copy.wait()
     growth = jnp.exp(sr_ref[:, 128:256])
     c_in = c_ref[...]
-    ahead = states[:, 0:8, :].reshape(INNER, STATE).astype(bf16)
-    behind = states[:, 8:16, :].reshape(INNER, STATE).astype(bf16)
-    dims = (((1,), (1,)), ((), ()))
-    carried_f = lax.dot_general(c_in, ahead, dims, preferred_element_type=f32)
-    carried_b = lax.dot_general(c_in, behind, dims, preferred_element_type=f32)
+    left = lanes((TOK, 128)) < HD
     squares = jnp.zeros((TOK, 128), f32)
     gated = []
     for q in range(4):
         cols = slice(q * 128, (q + 1) * 128)
-        y = (
-            y_ref[:, cols]
-            + per_channel(growth, 0, q) * carried_f[:, cols]
-            + per_channel(growth, HEADS, q) * carried_b[:, cols]
-        )
+        sums = []
+        for head in (2 * q, 2 * q + 1):
+            state = state_ref[head * 8 : head * 8 + 8].reshape(STATE, 128)
+            both = jnp.dot(c_in, state, preferred_element_type=f32) * jnp.where(
+                left, growth[:, head : head + 1], growth[:, HEADS + head : HEADS + head + 1]
+            )
+            sums.append(both + pltpu.roll(both, HD, 1))
+        y = y_ref[:, cols] + jnp.where(left, sums[0], sums[1])
         g = y * silu(z_ref[:, cols].astype(f32))
         squares = squares + g * g
         gated.append(g)
@@ -335,11 +342,23 @@
     half = INNER // 2
     mine = ny_ref[:, pl.ds(pl.multiple_of(core * half, half), half)]
     theirs = ny_ref[:, pl.ds(pl.multiple_of((1 - core) * half, half), half)]
+    for copy in loads[4:]:
+        copy.wait()
     for n in range(4):
         cols = slice(n * 512, (n + 1) * 512)
         out = jnp.dot(mine, own_ref[:, cols], preferred_element_type=f32)
         out = out + jnp.dot(theirs, other_ref[:, cols], preferred_element_type=f32)
         out_ref[:, cols] = out.astype(bf16)
+
+
+def sum_kernel(tile_ref, gate_ref, out_hbm, out_ref, sem):
+    total = tile_ref[0].astype(f32)
+    for t in range(1, 4):
+        total = total + tile_ref[t].astype(f32)
+    out_ref[...] = (gate_ref[0:1, :] * total).astype(bf16)
+    copy = pltpu.make_async_copy(out_ref, out_hbm, sem)
+    copy.start()
+    copy.wait()
 
 
 def call(kernel, out_shape, n_args, smem, scratch=(), hbm=(), hbm_out=False, flops=10**8):
@@ -361,7 +380,7 @@
 
 def project_call(*args):
     outs = [
-        ((NSP, 32, 128), bf16), ((ROWS, D), bf16), ((TOK, XB), bf16), ((TOK, 256), f32),
+        ((NSP, 24, 128), bf16), ((ROWS, D), bf16), ((TOK, XB), bf16), ((TOK, 256), f32),
         ((8, D), f32),
     ]
     return call(
@@ -396,7 +415,7 @@
     return call(
         owner_kernel,
         jax.ShapeDtypeStruct((NSP, 16, 128), bf16),
-        4,
+        3,
         (0,),
         [pltpu.VMEM((CTX + 16, 128), f32), pltpu.VMEM((NSP, 16, 128), f32)],
     )(*args)
@@ -408,7 +427,28 @@
         jax.ShapeDtypeStruct((TOK, D), bf16),
         9,
         (0,),
-        [pltpu.VMEM((TOK, INNER), bf16)],
+        [
+            pltpu.VMEM((TOK, INNER), bf16),
+            pltpu.VMEM((TOK, STATE), bf16),
+            pltpu.VMEM((TOK, 256), f32),
+            pltpu.VMEM((TOK, INNER), f32),
+            pltpu.VMEM((TOK, INNER), bf16),
+            pltpu.VMEM((INNER // 2, D), bf16),
+            pltpu.VMEM((INNER // 2, D), bf16),
+            pltpu.SemaphoreType.DMA((6,)),
+        ],
+        hbm=range(3, 9),
+    )(*args[:3], *(pltpu.with_memory_space_constraint(a, pltpu.HBM) for a in args[3:]))
+
+
+def sum_call(*args):
+    return call(
+        sum_kernel,
+        pltpu.HBM((OWN, D), bf16),
+        2,
+        (),
+        [pltpu.VMEM((OWN, D), bf16), pltpu.SemaphoreType.DMA(())],
+        hbm_out=True,
     )(*args)
 
 
@@ -444,9 +484,10 @@
 
 
 def owner_taps(conv_x, conv_b, at):
-    own = lax.dynamic_slice_in_dim(conv_x, at * 8, 8, 1)
-    tap_x = jnp.pad(own.astype(f32), ((0, 0), (0, 120)))
-    return conv_b.astype(f32), tap_x
+    of_x = lax.dynamic_slice_in_dim(conv_x, at // 8 * HD, HD, 1)
+    of_b = lax.dynamic_slice_in_dim(conv_b, at % 8 * 16, 16, 1)
+    both = jnp.concatenate([of_x, of_b], axis=1).astype(f32)
+    return jnp.pad(both, ((0, 0), (0, 128 - HD - 16)))
 
 
 def shards(
@@ -474,7 +515,7 @@
     part = part.reshape(20, 128)
     part = sent_to_all(part, 8, "sp_0")
     part = jnp.sum(part, axis=0)
-    mods = sent_to_all(part, 32, ("sp_1", "tp"))
+    mods = sent_to_all(part.astype(bf16), 32, ("sp_1", "tp"))
 
     packed = jnp.concatenate([rows, jnp.pad(halo, ((0, 7), (0, 0)))], axis=0)
     blocks = [packed]
@@ -488,7 +529,7 @@
     other_out = swapped(w_out)
 
     misc = packed_vectors(norm_gain, conv_x, conv_b, conv_c, decay_rate)
-    tap_b, tap_x = owner_taps(conv_x, conv_b, at)
+    own_taps = owner_taps(conv_x, conv_b, at)
     own_rates = lax.dynamic_slice_in_dim(decay_rate, at // 8, 1, 1)[:, 0]
 
     send, h, xb, sr, gate = project_call(
@@ -498,14 +539,13 @@
     y_in, c_in, z_in = inside_call(
         place, h, w_z, other_z, small, other_small, xb, sr, misc
     )
-    entering = owner_call(own_rates, received, tap_b, tap_x)
+    entering = owner_call(own_rates, received, own_taps)
     states = exchanged(entering, SP)
     partial = output_call(
-        place, states, c_in, y_in, sr, z_in, out_gain[None], w_out, other_out
+        place, states, out_gain[None], c_in, sr, y_in, z_in, w_out, other_out
     )
     tiles = exchanged(partial.reshape(4, OWN, D), "tp")
-    mixed = jnp.sum(tiles.astype(f32), axis=0)
-    return (gate[0:1] * mixed).astype(bf16)[None]
+    return sum_call(tiles, gate)[None]
 
 
 def solution(mesh):

time: 127 us -> 119 us (0.937)
  blocking collectives: 0 us -> 10.6 us
  starting transfers between devices: 65.7 us -> 57.4 us
  waiting for transfers between devices: 33.5 us -> 28.1 us
  local copies, waits for them, and re-layouts: 8.44 us -> 5.88 us
  other arithmetic: 4.68 us -> 2.68 us
    all_to_all x0 -> x1, blocking collectives: none -> 10.6 us  [exchanged(): return lax.all_to_all(x, axes, 0, 0, tiled=True)]
    all_to_all x5 -> x4, starting transfers between devices: 41 us -> 35.1 us  [exchanged(): return lax.all_to_all(x, axes, 0, 0, tiled=True)]
    ppermute x3, waiting for transfers between devices: 3.94 us -> 0.01 us  [shards(): lax.ppermute(packed, 'tp', [(i, (i + s) % 4) for i in range(4)])]
    ppermute x3, starting transfers between devices: 11.3 us -> 8.97 us  [shards(): lax.ppermute(packed, 'tp', [(i, (i + s) % 4) for i in range(4)])]
    unnamed x42 -> x44, local copies, waits for them, and re-layouts: 4.84 us -> 3.13 us
    all_to_all x5 -> x4, waiting for transfers between devices: 29.5 us -> 28.1 us  [exchanged(): return lax.all_to_all(x, axes, 0, 0, tiled=True)]
    pallas_call x1 -> x2, Pallas kernels: 2.96 us -> 3.37 us  [the longest x1 2.63 us: owner_call(): call(owner_kernel, jax.ShapeDtypeStruct((NSP, 16, 128), bf16), 3, (0,), [...]
  transfers between devices with their start and end apart: 13 -> 12, of which waited for: 6 -> 3; matrix products, arithmetic and copies ran while one was open for 4% -> 3% of each run, Pallas kernels for 4% -> 4%
where the time goes in v3:
time: 119 us; the launch traced here: 118 us
  starting transfers between devices  57.4 us (48%)
  waiting for transfers between devices  28.1 us (24%)
  Pallas kernels  13 us (11%)
  blocking collectives  10.6 us (9%)
  local copies, waits for them, and re-layouts  5.88 us (5%)
  other arithmetic  2.68 us (2%)
    all_to_all x4, starting transfers between devices, exchanged(): return lax.all_to_all(x, axes, 0, 0, tiled=True)  35.1 us
    all_to_all x4, waiting for transfers between devices, exchanged(): return lax.all_to_all(x, axes, 0, 0, tiled=True)  28.1 us
    all_to_all x1, blocking collectives, exchanged(): return lax.all_to_all(x, axes, 0, 0, tiled=True)  10.6 us
    ppermute x3, starting transfers between devices, shards(): lax.ppermute(packed, 'tp', [(i, (i + s) % 4) for i in range(4)])  8.97 us
    ppermute x4, starting transfers between devices, swapped(): return lax.ppermute(x, 'dp', [(0, 1), (1, 0)])  8.79 us
    ppermute x1, starting transfers between devices, shards(): halo = lax.ppermute(edge, ALL, pairs)  4.55 us
    pallas_call x1, Pallas kernels, project_call(): call(project_kernel, [pltpu.HBM(*o) for o in outs], 12, (0,), [*(pltpu.VM...  4.4 us
    unnamed x44, local copies, waits for them, and re-layouts  3.13 us
  transfers between devices with their start and end apart: 12, of which 3 were waited for; matrix products, arithmetic and copies ran while one was open for 3% of the time, Pallas kernels for 4%

profile of v3, /device:TPU:8, one launch (start us, length us, event | category | flops | bytes accessed | tf_op | source)
XLA Modules:
  0.0 118.4 jit_solution(11461015027757092965)
XLA Ops:
  0.0 0.8 fusion.12
  0.8 0.7 fusion.14
  1.5 0.2 fusion.21
  1.8 0.6 broadcast_in_dim.26
  2.4 10.3 %all-to-all-start = ((f32[8,20,128]{2,1,0:T(8,128)}), f32[8,20,128]{2,1,0:T(8,128)S(1)}, u32[]{:S(2)}, u32[]{:S(2)}) async-start(f32[8,20,128]{2,1,0:T(8,128)} %broadcast_in_dim.26), calls=%async_computation | async-start | bytes 196608 | tf_op jit(solution)/shard_map/all_to_all | solution.py:460
  12.8 0.0 copy-start.16
  12.8 0.0 copy-start.18
  12.8 0.0 copy-start.15
  12.8 0.0 copy-start.20
  12.8 0.8 fusion.13
  13.7 4.6 %collective-permute-start = (bf16[1,2048]{1,0:T(2,128)(2,1)S(1)}, bf16[1,2048]{1,0:T(2,128)(2,1)S(1)}, u32[]{:S(2)}, u32[]{:S(2)}) collective-permute-start(bf16[1,2048]{1,0:T(2,128)(2,1)S(1)} %fusion.13), channel_id=1, source_target_pairs={{6,8},{14,16},{22,24},{30,32},{38,40},{46,48},{54,56},{62,64},{70,... | collective-permute-start | bytes 12296 | tf_op jit(solution)/shard_map/ppermute | solution.py:507
  18.2 1.9 %collective-permute-start.4 = (bf16[1024,512]{1,0:T(8,128)(2,1)}, bf16[1024,512]{1,0:T(8,128)(2,1)}, u32[]{:S(2)}, u32[]{:S(2)}) collective-permute-start(bf16[1024,512]{1,0:T(8,128)(2,1)} %own_x.1), channel_id=1, source_target_pairs={{0,1},{1,0},{2,3},{3,2},{4,5},{5,4},{6,7},{7,6},{8,9},{9,8},{10,11... | collective-permute-start | bytes 3145736 | tf_op jit(solution)/shard_map/ppermute | solution.py:456
  20.2 0.7 slice_bitcast_fusion.1
  20.9 0.2 copy.23
  21.1 0.0 copy-start.9
  21.1 0.1 fusion.1.own_s
  21.3 2.5 %collective-permute-start.5 = (bf16[1024,384]{1,0:T(8,128)(2,1)S(1)}, bf16[1024,384]{1,0:T(8,128)(2,1)S(1)}, u32[]{:S(2)}, u32[]{:S(2)}) collective-permute-start(bf16[1024,384]{1,0:T(8,128)(2,1)S(1)} %fusion.1.own_s), channel_id=1, source_target_pairs={{0,1},{1,0},{2,3},{3,2},{4,5},{5,4},{6,7},{7,6},{8,9},{9,8},{10,11... | collective-permute-start | bytes 2359304 | tf_op jit(solution)/shard_map/ppermute | solution.py:456
  23.9 0.1 reshape.34
  24.0 1.9 %collective-permute-start.1 = (bf16[40,2048]{1,0:T(8,128)(2,1)S(1)}, bf16[40,2048]{1,0:T(8,128)(2,1)S(1)}, u32[]{:S(2)}, u32[]{:S(2)}) collective-permute-start(bf16[40,2048]{1,0:T(8,128)(2,1)S(1)} %fusion.3.blk0_ref), channel_id=1, source_target_pairs={{0,2},{2,4},{4,6},{6,0},{1,3},{3,5},{5,7},{7,1},{8,10},{10,12},{12... | collective-permute-start | bytes 491528 | tf_op jit(solution)/shard_map/ppermute | solution.py:523
  25.9 5.0 %collective-permute-start.2 = (bf16[40,2048]{1,0:T(8,128)(2,1)S(1)}, bf16[40,2048]{1,0:T(8,128)(2,1)S(1)}, u32[]{:S(2)}, u32[]{:S(2)}) collective-permute-start(bf16[40,2048]{1,0:T(8,128)(2,1)S(1)} %fusion.3.blk0_ref), channel_id=1, source_target_pairs={{0,4},{2,6},{4,0},{6,2},{1,5},{3,7},{5,1},{7,3},{8,12},{10,14},{12... | collective-permute-start | bytes 491528 | tf_op jit(solution)/shard_map/ppermute | solution.py:523
  30.9 2.1 %collective-permute-start.3 = (bf16[40,2048]{1,0:T(8,128)(2,1)S(1)}, bf16[40,2048]{1,0:T(8,128)(2,1)}, u32[]{:S(2)}, u32[]{:S(2)}) collective-permute-start(bf16[40,2048]{1,0:T(8,128)(2,1)S(1)} %fusion.3.blk0_ref), channel_id=1, source_target_pairs={{0,6},{2,0},{4,2},{6,4},{1,7},{3,1},{5,3},{7,5},{8,14},{10,8},{12,... | collective-permute-start | bytes 491528 | tf_op jit(solution)/shard_map/ppermute | solution.py:523
  33.0 0.7 broadcast_in_dim.27
  33.7 10.2 %all-to-all-start.1 = ((bf16[32,20,128]{2,1,0:T(8,128)(2,1)}), bf16[32,20,128]{2,1,0:T(8,128)(2,1)S(1)}, u32[]{:S(2)}, u32[]{:S(2)}) async-start(bf16[32,20,128]{2,1,0:T(8,128)(2,1)} %broadcast_in_dim.27), calls=%async_computation.1 | async-start | bytes 393216 | tf_op jit(solution)/shard_map/all_to_all | solution.py:460
  44.0 0.1 pad_add_fusion.place_ref
  44.0 10.1 %all-to-all-done.1.mod_ref = bf16[32,20,128]{2,1,0:T(8,128)(2,1)S(1)} async-done(((bf16[32,20,128]{2,1,0:T(8,128)(2,1)}), bf16[32,20,128]{2,1,0:T(8,128)(2,1)S(1)}, u32[]{:S(2)}, u32[]{:S(2)}) %all-to-all-start.1) | async-done | bytes 163872 | tf_op jit(solution)/shard_map/all_to_all | solution.py:460
  54.1 0.0 copy-start.17
  54.1 4.4 %shard_map.163 = (bf16[64,24,128]{2,1,0:T(8,128)(2,1)}, bf16[144,2048]{1,0:T(8,128)(2,1)}, bf16[128,640]{1,0:T(8,128)(2,1)}, f32[128,256]{1,0:T(8,128)}, f32[8,2048]{1,0:T(8,128)}) custom-call(s32[3]{0:T(128)S(1)} %pad_add_fusion.place_ref, bf16[32,20,128]{2,1,0:T(8,128)(2,1)S(1)} %all-to-all-done.1.mod_ref, bf16[40,2048]{1,0:T(8,128)(2,1)S(1)} %fusion.3.blk0_ref, ...), custom_call_target="tpu_custom_call" | custom-call | flops 100000000 | bytes 1048576 | tf_op jit(solution)/shard_map/pallas_call | solution.py:386
  58.6 0.0 copy-start.2
  58.6 0.0 copy-start.4
  58.6 9.7 %all-to-all-start.2 = ((bf16[64,24,128]{2,1,0:T(8,128)(2,1)}), bf16[64,24,128]{2,1,0:T(8,128)(2,1)S(1)}, u32[]{:S(2)}, u32[]{:S(2)}) async-start(bf16[64,24,128]{2,1,0:T(8,128)(2,1)} %get-tuple-element.13), calls=%async_computation.2 | async-start | bytes 786432 | tf_op jit(solution)/shard_map/all_to_all | solution.py:460
  68.3 1.9 %collective-permute-start.6 = (bf16[1024,512]{1,0:T(8,128)(2,1)}, bf16[1024,512]{1,0:T(8,128)(2,1)}, u32[]{:S(2)}, u32[]{:S(2)}) collective-permute-start(bf16[1024,512]{1,0:T(8,128)(2,1)} %own_z.1), channel_id=1, source_target_pairs={{0,1},{1,0},{2,3},{3,2},{4,5},{5,4},{6,7},{7,6},{8,9},{9,8},{10,11... | collective-permute-start | bytes 3145736 | tf_op jit(solution)/shard_map/ppermute | solution.py:456
  70.2 2.4 %collective-permute-start.7 = (bf16[256,2048]{1,0:T(8,128)(2,1)}, bf16[256,2048]{1,0:T(8,128)(2,1)}, u32[]{:S(2)}, u32[]{:S(2)}) collective-permute-start(bf16[256,2048]{1,0:T(8,128)(2,1)} %own_hbm.1), channel_id=1, source_target_pairs={{0,1},{1,0},{2,3},{3,2},{4,5},{5,4},{6,7},{7,6},{8,9},{9,8},{10,11... | collective-permute-start | bytes 3145736 | tf_op jit(solution)/shard_map/ppermute | solution.py:456
  72.7 0.2 fusion.17.rate_ref
  72.9 0.1 constant_dynamic-slice_fusion
  73.0 0.1 constant_dynamic-slice_fusion.1
  73.0 0.1 fusion.19.tap_ref
  73.1 10.3 %all-to-all-done.2.recv_ref = bf16[64,24,128]{2,1,0:T(8,128)(2,1)S(1)} async-done(((bf16[64,24,128]{2,1,0:T(8,128)(2,1)}), bf16[64,24,128]{2,1,0:T(8,128)(2,1)S(1)}, u32[]{:S(2)}, u32[]{:S(2)}) %all-to-all-start.2) | async-done | bytes 393248 | tf_op jit(solution)/shard_map/all_to_all | solution.py:460
  83.4 2.6 %shard_map.164 = bf16[64,16,128]{2,1,0:T(8,128)(2,1)} custom-call(f32[2]{0:T(128)S(1)} %fusion.17.rate_ref, bf16[64,24,128]{2,1,0:T(8,128)(2,1)S(1)} %all-to-all-done.2.recv_ref, f32[3,128]{1,0:T(4,128)S(1)} %fusion.19.tap_ref), custom_call_target="tpu_custom_call" | custom-call | flops 100000000 | bytes 1048576 | tf_op jit(solution)/shard_map/pallas_call | solution.py:415
  86.0 4.9 %all-to-all-start.3 = ((bf16[64,16,128]{2,1,0:T(8,128)(2,1)}), bf16[64,16,128]{2,1,0:T(8,128)(2,1)S(1)}, u32[]{:S(2)}, u32[]{:S(2)}) async-start(bf16[64,16,128]{2,1,0:T(8,128)(2,1)} %shard_map.164), calls=%async_computation.3 | async-start | bytes 524288 | tf_op jit(solution)/shard_map/all_to_all | solution.py:460
  91.0 1.1 copy-done.3
  92.1 2.3 %shard_map.165 = (f32[128,512]{1,0:T(8,128)S(1)}, bf16[128,128]{1,0:T(8,128)(2,1)S(1)}, bf16[128,512]{1,0:T(8,128)(2,1)S(1)}) custom-call(s32[3]{0:T(128)S(1)} %pad_add_fusion.place_ref, bf16[144,2048]{1,0:T(8,128)(2,1)S(1)} %copy-done.3, bf16[1024,512]{1,0:T(8,128)(2,1)S(1)} %copy-done.2, bf16[1024,512]{1,0:T(8,128)(2,1)} %collective-permute-done.6.other_z, ...), custom_call_target="tpu_custom_call" | custom-call | flops 100000000 | bytes 1048576 | tf_op jit(solution)/shard_map/pallas_call | solution.py:401
  94.4 0.7 copy-done.5
  95.1 0.7 copy-done.7
  95.7 0.6 copy-done.10
  96.3 7.8 %all-to-all-done.3.state_ref = bf16[64,16,128]{2,1,0:T(8,128)(2,1)S(1)} async-done(((bf16[64,16,128]{2,1,0:T(8,128)(2,1)}), bf16[64,16,128]{2,1,0:T(8,128)(2,1)S(1)}, u32[]{:S(2)}, u32[]{:S(2)}) %all-to-all-start.3) | async-done | bytes 262176 | tf_op jit(solution)/shard_map/all_to_all | solution.py:460
  104.1 3.0 %shard_map.166 = bf16[128,2048]{1,0:T(8,128)(2,1)S(1)} custom-call(s32[3]{0:T(128)S(1)} %pad_add_fusion.place_ref, bf16[64,16,128]{2,1,0:T(8,128)(2,1)S(1)} %all-to-all-done.3.state_ref, bf16[1,512]{1,0:T(2,128)(2,1)S(1)} %broadcast_in_dim.30.gain_ref, bf16[128,128]{1,0:T(8,128)(2,1)} %copy-done.10, f32[128,256]{1,0:T(8,128)} %get-tuple-element.16.sr_ref.sr_hbm, ...), custom_call_target="tpu_custom_call" | custom-call | flops 100000000 | bytes 1048576 | tf_op jit(solution)/shard_map/pallas_call | solution.py:425
  107.1 10.6 %all_to_all.25.tile_ref = bf16[4,32,2048]{2,1,0:T(8,128)(2,1)S(1)} all-to-all(bf16[4,32,2048]{2,1,0:T(8,128)(2,1)S(1)} %bitcast.28), channel_id=1, replica_groups=mesh['sp_0'=8,'sp_1'=8,'tp'=4,'dp'=2] {'tp'}, dimensions={0} | all-to-all | bytes 1048576 | tf_op jit(solution)/shard_map/all_to_all | solution.py:460
  117.7 0.7 shard_map.167
  (52 shorter events, 0.2 us)
Async XLA Ops:
  0.0 1.5 %copy-start = (bf16[3,32,512]{2,1,0:T(8,128)(2,1)S(1)}, bf16[3,32,512]{2,1,0:T(8,128)(2,1)}, u32[]{:S(2)}) copy-start(bf16[3,32,512]{2,1,0:T(8,128)(2,1)} %param.21) | copy-start | bytes 294916
  0.0 21.1 %copy-start.12 = (bf16[1024,128]{1,0:T(8,128)(2,1)S(1)}, bf16[1024,128]{1,0:T(8,128)(2,1)}, u32[]{:S(2)}) copy-start(bf16[1024,128]{1,0:T(8,128)(2,1)} %param.24) | copy-start | bytes 786436
  0.0 21.1 %copy-start.11 = (bf16[1024,128]{1,0:T(8,128)(2,1)S(1)}, bf16[1024,128]{1,0:T(8,128)(2,1)}, u32[]{:S(2)}) copy-start(bf16[1024,128]{1,0:T(8,128)(2,1)} %param.25) | copy-start | bytes 786436
  2.4 30.6 %all-to-all-start = ((f32[8,20,128]{2,1,0:T(8,128)}), f32[8,20,128]{2,1,0:T(8,128)S(1)}, u32[]{:S(2)}, u32[]{:S(2)}) async-start(f32[8,20,128]{2,1,0:T(8,128)} %broadcast_in_dim.26), calls=%async_computation | async-start | bytes 196608 | tf_op jit(solution)/shard_map/all_to_all | solution.py:460
  12.8 11.1 %copy-start.14 = (bf16[3,512]{1,0:T(4,128)(2,1)S(1)}, bf16[3,512]{1,0:T(4,128)(2,1)}, u32[]{:S(2)}) copy-start(bf16[3,512]{1,0:T(4,128)(2,1)} %param.28) | copy-start | bytes 9220
  12.8 11.1 %copy-start.16 = (bf16[3,128]{1,0:T(4,128)(2,1)S(1)}, bf16[3,128]{1,0:T(4,128)(2,1)}, u32[]{:S(2)}) copy-start(bf16[3,128]{1,0:T(4,128)(2,1)} %param.29) | copy-start | bytes 2308
  12.8 11.1 %copy-start.18 = (bf16[3,128]{1,0:T(4,128)(2,1)S(1)}, bf16[3,128]{1,0:T(4,128)(2,1)}, u32[]{:S(2)}) copy-start(bf16[3,128]{1,0:T(4,128)(2,1)} %param.30) | copy-start | bytes 2308
  12.8 11.1 %copy-start.15 = (bf16[2048]{0:T(1024)(128)(2,1)S(1)}, bf16[2048]{0:T(1024)(128)(2,1)}, u32[]{:S(2)}) copy-start(bf16[2048]{0:T(1024)(128)(2,1)} %param.22) | copy-start | bytes 12292
  12.8 11.1 %copy-start.20 = (f32[2,8]{1,0:T(2,128)S(1)}, f32[2,8]{1,0:T(2,128)}, u32[]{:S(2)}) copy-start(f32[2,8]{1,0:T(2,128)} %param.31) | copy-start | bytes 196
  12.8 11.2 %copy-start.13 = (bf16[1,32,2048]{2,1,0:T(8,128)(2,1)S(1)}, bf16[1,32,2048]{2,1,0:T(8,128)(2,1)}, u32[]{:S(2)}) copy-start(bf16[1,32,2048]{2,1,0:T(8,128)(2,1)} %param.17) | copy-start | bytes 393220
  13.7 10.3 %collective-permute-start = (bf16[1,2048]{1,0:T(2,128)(2,1)S(1)}, bf16[1,2048]{1,0:T(2,128)(2,1)S(1)}, u32[]{:S(2)}, u32[]{:S(2)}) collective-permute-start(bf16[1,2048]{1,0:T(2,128)(2,1)S(1)} %fusion.13), channel_id=1, source_target_pairs={{6,8},{14,16},{22,24},{30,32},{38,40},{46,48},{54,56},{62,64},{70,... | collective-permute-start | bytes 12296 | tf_op jit(solution)/shard_map/ppermute | solution.py:507
  18.2 35.9 %collective-permute-start.4 = (bf16[1024,512]{1,0:T(8,128)(2,1)}, bf16[1024,512]{1,0:T(8,128)(2,1)}, u32[]{:S(2)}, u32[]{:S(2)}) collective-permute-start(bf16[1024,512]{1,0:T(8,128)(2,1)} %own_x.1), channel_id=1, source_target_pairs={{0,1},{1,0},{2,3},{3,2},{4,5},{5,4},{6,7},{7,6},{8,9},{9,8},{10,11... | collective-permute-start | bytes 3145736 | tf_op jit(solution)/shard_map/ppermute | solution.py:456
  21.1 33.0 %copy-start.1 = (bf16[1024,512]{1,0:T(8,128)(2,1)S(1)}, bf16[1024,512]{1,0:T(8,128)(2,1)}, u32[]{:S(2)}) copy-start(bf16[1024,512]{1,0:T(8,128)(2,1)} %own_x.1) | copy-start | bytes 3145732
  21.1 33.0 %copy-start.9 = (bf16[1,8,2048]{2,1,0:T(8,128)(2,1)S(1)}, bf16[1,8,2048]{2,1,0:T(8,128)(2,1)}, u32[]{:S(2)}) copy-start(bf16[1,8,2048]{2,1,0:T(8,128)(2,1)} %param.19) | copy-start | bytes 98308
  21.3 32.8 %collective-permute-start.5 = (bf16[1024,384]{1,0:T(8,128)(2,1)S(1)}, bf16[1024,384]{1,0:T(8,128)(2,1)S(1)}, u32[]{:S(2)}, u32[]{:S(2)}) collective-permute-start(bf16[1024,384]{1,0:T(8,128)(2,1)S(1)} %fusion.1.own_s), channel_id=1, source_target_pairs={{0,1},{1,0},{2,3},{3,2},{4,5},{5,4},{6,7},{7,6},{8,9},{9,8},{10,11... | collective-permute-start | bytes 2359304 | tf_op jit(solution)/shard_map/ppermute | solution.py:456
  24.0 20.0 %collective-permute-start.1 = (bf16[40,2048]{1,0:T(8,128)(2,1)S(1)}, bf16[40,2048]{1,0:T(8,128)(2,1)S(1)}, u32[]{:S(2)}, u32[]{:S(2)}) collective-permute-start(bf16[40,2048]{1,0:T(8,128)(2,1)S(1)} %fusion.3.blk0_ref), channel_id=1, source_target_pairs={{0,2},{2,4},{4,6},{6,0},{1,3},{3,5},{5,7},{7,1},{8,10},{10,12},{12... | collective-permute-start | bytes 491528 | tf_op jit(solution)/shard_map/ppermute | solution.py:523
  25.9 18.1 %collective-permute-start.2 = (bf16[40,2048]{1,0:T(8,128)(2,1)S(1)}, bf16[40,2048]{1,0:T(8,128)(2,1)S(1)}, u32[]{:S(2)}, u32[]{:S(2)}) collective-permute-start(bf16[40,2048]{1,0:T(8,128)(2,1)S(1)} %fusion.3.blk0_ref), channel_id=1, source_target_pairs={{0,4},{2,6},{4,0},{6,2},{1,5},{3,7},{5,1},{7,3},{8,12},{10,14},{12... | collective-permute-start | bytes 491528 | tf_op jit(solution)/shard_map/ppermute | solution.py:523
  30.9 13.1 %collective-permute-start.3 = (bf16[40,2048]{1,0:T(8,128)(2,1)S(1)}, bf16[40,2048]{1,0:T(8,128)(2,1)}, u32[]{:S(2)}, u32[]{:S(2)}) collective-permute-start(bf16[40,2048]{1,0:T(8,128)(2,1)S(1)} %fusion.3.blk0_ref), channel_id=1, source_target_pairs={{0,6},{2,0},{4,2},{6,4},{1,7},{3,1},{5,3},{7,5},{8,14},{10,8},{12,... | collective-permute-start | bytes 491528 | tf_op jit(solution)/shard_map/ppermute | solution.py:523
  33.7 20.4 %all-to-all-start.1 = ((bf16[32,20,128]{2,1,0:T(8,128)(2,1)}), bf16[32,20,128]{2,1,0:T(8,128)(2,1)S(1)}, u32[]{:S(2)}, u32[]{:S(2)}) async-start(bf16[32,20,128]{2,1,0:T(8,128)(2,1)} %broadcast_in_dim.27), calls=%async_computation.1 | async-start | bytes 393216 | tf_op jit(solution)/shard_map/all_to_all | solution.py:460
  54.1 18.6 %copy-start.21 = (f32[2,8]{1,0:T(2,128)S(1)}, f32[2,8]{1,0:T(2,128)}, u32[]{:S(2)}) copy-start(f32[2,8]{1,0:T(2,128)} %param.31) | copy-start | bytes 196
  54.1 18.8 %copy-start.17 = (bf16[3,128]{1,0:T(4,128)(2,1)S(1)}, bf16[3,128]{1,0:T(4,128)(2,1)}, u32[]{:S(2)}) copy-start(bf16[3,128]{1,0:T(4,128)(2,1)} %param.29) | copy-start | bytes 2308
  58.6 32.4 %copy-start.19 = (bf16[512]{0:T(512)(128)(2,1)S(1)}, bf16[512]{0:T(512)(128)(2,1)}, u32[]{:S(2)}) copy-start(bf16[512]{0:T(512)(128)(2,1)} %param.32) | copy-start | bytes 3076
  58.6 32.4 %copy-start.2 = (bf16[1024,512]{1,0:T(8,128)(2,1)S(1)}, bf16[1024,512]{1,0:T(8,128)(2,1)}, u32[]{:S(2)}) copy-start(bf16[1024,512]{1,0:T(8,128)(2,1)} %own_z.1) | copy-start | bytes 3145732
  58.6 32.4 %copy-start.4 = (f32[128,256]{1,0:T(8,128)S(1)}, f32[128,256]{1,0:T(8,128)}, u32[]{:S(2)}) copy-start(f32[128,256]{1,0:T(8,128)} %get-tuple-element.16.sr_ref.sr_hbm) | copy-start | bytes 393220
  58.6 32.4 %copy-start.6 = (bf16[128,640]{1,0:T(8,128)(2,1)S(1)}, bf16[128,640]{1,0:T(8,128)(2,1)}, u32[]{:S(2)}) copy-start(bf16[128,640]{1,0:T(8,128)(2,1)} %get-tuple-element.15.xb_ref) | copy-start | bytes 491524
  58.6 24.8 %all-to-all-start.2 = ((bf16[64,24,128]{2,1,0:T(8,128)(2,1)}), bf16[64,24,128]{2,1,0:T(8,128)(2,1)S(1)}, u32[]{:S(2)}, u32[]{:S(2)}) async-start(bf16[64,24,128]{2,1,0:T(8,128)(2,1)} %get-tuple-element.13), calls=%async_computation.2 | async-start | bytes 786432 | tf_op jit(solution)/shard_map/all_to_all | solution.py:460
  68.3 22.7 %collective-permute-start.6 = (bf16[1024,512]{1,0:T(8,128)(2,1)}, bf16[1024,512]{1,0:T(8,128)(2,1)}, u32[]{:S(2)}, u32[]{:S(2)}) collective-permute-start(bf16[1024,512]{1,0:T(8,128)(2,1)} %own_z.1), channel_id=1, source_target_pairs={{0,1},{1,0},{2,3},{3,2},{4,5},{5,4},{6,7},{7,6},{8,9},{9,8},{10,11... | collective-permute-start | bytes 3145736 | tf_op jit(solution)/shard_map/ppermute | solution.py:456
  70.2 26.1 %collective-permute-start.7 = (bf16[256,2048]{1,0:T(8,128)(2,1)}, bf16[256,2048]{1,0:T(8,128)(2,1)}, u32[]{:S(2)}, u32[]{:S(2)}) collective-permute-start(bf16[256,2048]{1,0:T(8,128)(2,1)} %own_hbm.1), channel_id=1, source_target_pairs={{0,1},{1,0},{2,3},{3,2},{4,5},{5,4},{6,7},{7,6},{8,9},{9,8},{10,11... | collective-permute-start | bytes 3145736 | tf_op jit(solution)/shard_map/ppermute | solution.py:456
  86.0 18.1 %all-to-all-start.3 = ((bf16[64,16,128]{2,1,0:T(8,128)(2,1)}), bf16[64,16,128]{2,1,0:T(8,128)(2,1)S(1)}, u32[]{:S(2)}, u32[]{:S(2)}) async-start(bf16[64,16,128]{2,1,0:T(8,128)(2,1)} %shard_map.164), calls=%async_computation.3 | async-start | bytes 524288 | tf_op jit(solution)/shard_map/all_to_all | solution.py:460
  91.0 1.1 copy-start.3
  94.3 0.7 copy-start.5
  95.1 0.7 copy-start.7
  95.7 0.6 copy-start.10
  107.1 10.6 %copy-start.8 = (f32[8,2048]{1,0:T(8,128)S(1)}, f32[8,2048]{1,0:T(8,128)}, u32[]{:S(2)}) copy-start(f32[8,2048]{1,0:T(8,128)} %get-tuple-element.20.gate_ref) | copy-start | bytes 196612

commit v4 on v3

--- a/solution.py
+++ b/solution.py
@@ -89,9 +89,38 @@
     )
 
 
+def pack_kernel(part_ref, rows_ref, halo_ref, out_hbm, tail_ref, sems):
+    copies = [
+        pltpu.make_async_copy(rows_ref, out_hbm.at[t, pl.ds(0, OWN)], sems.at[t]) for t in range(4)
+    ]
+    for copy in copies:
+        copy.start()
+    total = part_ref[0]
+    for y in range(1, 8):
+        total = total + part_ref[y]
+    high = rounded(total)
+    mid = rounded(total - high)
+    parts = [high, mid, total - high - mid]
+    zero = jnp.zeros((1, 128), f32)
+    for m in range(16):
+        cols = slice(m * 128, (m + 1) * 128)
+        rows = [halo_ref[0:1, cols].astype(f32)]
+        for r in range(7):
+            k = r * 16 + m
+            rows.append(parts[k // 20][k % 20 : k % 20 + 1] if k < 60 else zero)
+        tail_ref[:, cols] = jnp.concatenate(rows, axis=0).astype(bf16)
+    more = [
+        pltpu.make_async_copy(tail_ref, out_hbm.at[t, pl.ds(OWN, 8)], sems.at[4 + t])
+        for t in range(4)
+    ]
+    for copy in more:
+        copy.start()
+    for copy in copies + more:
+        copy.wait()
+
+
 def project_kernel(
-    place_ref, mod_ref, blk0_ref, blk1_ref, blk2_ref, blk3_ref, ctx_ref, misc_ref,
-    own_x, other_x, own_s, other_s,
+    place_ref, blk_ref, ctx_ref, misc_ref, own_x, other_x, own_s, other_s,
     send_hbm, h_hbm, xb_hbm, sr_hbm, gate_hbm,
     send_ref, h_ref, xb_ref, sr_ref, gate_ref, conv_ref, sems,
 ):
@@ -100,44 +129,45 @@
         copy.start()
         return copy
 
-    core, at, tp = place_ref[0], place_ref[1], place_ref[2]
-    blocks = (blk0_ref, blk1_ref, blk2_ref, blk3_ref)
-    origin = [lax.rem(tp + 4 - s, 4) for s in range(4)]
-    is_first = [jnp.where(o == 0, 1.0, 0.0) for o in origin]
-    is_last = [jnp.where(o == 3, 1.0, 0.0) for o in origin]
-    mods = []
+    core, at = place_ref[0], place_ref[1]
+    mods, tails = [], []
     for t in range(4):
-        total = mod_ref[t].astype(f32)
-        for y in range(1, 8):
-            total = total + mod_ref[4 * y + t].astype(f32)
-        mods.append(total)
-
-    def inverse(ref):
-        squares = jnp.zeros((ref.shape[0], 128), f32)
+        tail = blk_ref[t, OWN:, :].astype(f32)
+        tails.append(tail)
+
+        def row(k, tail=tail):
+            return tail[1 + k // 16 : 2 + k // 16, (k % 16) * 128 : (k % 16 + 1) * 128]
+
+        mods.append([row(i) + row(20 + i) + row(40 + i) for i in range(20)])
+
+    def inverse(rows, read):
+        squares = jnp.zeros((rows, 128), f32)
         for c in range(16):
-            v = ref[:, c * 128 : (c + 1) * 128].astype(f32)
+            v = read(slice(c * 128, (c + 1) * 128))
             squares = squares + v * v
         return lax.rsqrt(jnp.sum(squares, axis=1, keepdims=True) * (1.0 / D) + EPSILON)
 
-    inv = [inverse(ref) for ref in blocks]
-    inv_ctx = inverse(ctx_ref)
     row8 = rows_of((8, 128))
+
+    def neighbours(cols):
+        last = pltpu.roll(tails[3][:, cols], 1, 0)
+        return jnp.where(row8 == 0, tails[0][:, cols], jnp.where(row8 == 1, last, 0.0))
+
+    inv = [inverse(OWN, lambda cols, t=t: blk_ref[t, :OWN, cols].astype(f32)) for t in range(4)]
+    inv_halo = inverse(8, neighbours)
+    inv_ctx = inverse(8, lambda cols: ctx_ref[:, cols].astype(f32))
     for c in range(16):
         t, q = c // 4, c % 4
         cols = slice(c * 128, (c + 1) * 128)
         gain = misc_ref[0:1, cols]
-        shift, scale = mods[t][q : q + 1], mods[t][4 + q : 5 + q]
-        cshift, cscale = mods[t][8 + q : 9 + q], mods[t][12 + q : 13 + q]
-        gate_ref[:, cols] = jnp.broadcast_to(mods[t][16 + q : 17 + q], (8, 128))
-        before = jnp.zeros((8, 128), f32)
-        after = jnp.zeros((8, 128), f32)
+        shift, scale = mods[t][q], 1.0 + mods[t][4 + q]
+        cshift, cscale = mods[t][8 + q], 1.0 + mods[t][12 + q]
+        gate_ref[:, cols] = jnp.broadcast_to(mods[t][16 + q], (8, 128))
         for s in range(4):
-            h = blocks[s][:, cols].astype(f32) * inv[s] * gain * (1.0 + scale) + shift
-            h_ref[pl.ds(pl.multiple_of(origin[s] * OWN, OWN), OWN), cols] = h[:OWN].astype(bf16)
-            before = before + h[OWN:] * is_first[s]
-            after = after + h[OWN:] * is_last[s]
-        halo = jnp.where(row8 == 0, before, pltpu.roll(after, 1, 0))
-        ctx = ctx_ref[:, cols].astype(f32) * inv_ctx * gain * (1.0 + cscale) + cshift
+            h = blk_ref[s, :OWN, cols].astype(f32) * inv[s] * gain * scale + shift
+            h_ref[s * OWN : (s + 1) * OWN, cols] = h.astype(bf16)
+        halo = neighbours(cols) * inv_halo * gain * scale + shift
+        ctx = ctx_ref[:, cols].astype(f32) * inv_ctx * gain * cscale + cshift
         h_ref[TOK:ROWS, cols] = jnp.concatenate([halo, ctx], axis=0).astype(bf16)
     stores = [store(0, h_ref, h_hbm), store(1, gate_ref, gate_hbm)]
 
@@ -300,23 +330,18 @@
 
 
 def output_kernel(
-    place_ref, state_ref, gain_ref, c_hbm, sr_hbm, y_hbm, z_hbm, own_hbm, other_hbm,
-    out_ref, ny_ref, c_ref, sr_ref, y_ref, z_ref, own_ref, other_ref, sems,
+    place_ref, state_ref, gain_ref, c_ref, sr_ref, z_ref, y_hbm, own_hbm, other_hbm,
+    out_ref, ny_ref, y_ref, own_ref, other_ref, sems,
 ):
     loads = [
         pltpu.make_async_copy(src, dst, sems.at[i])
         for i, (src, dst) in enumerate(
-            (
-                (c_hbm, c_ref), (sr_hbm, sr_ref), (y_hbm, y_ref), (z_hbm, z_ref),
-                (own_hbm, own_ref), (other_hbm, other_ref),
-            )
+            ((y_hbm, y_ref), (own_hbm, own_ref), (other_hbm, other_ref))
         )
     ]
     for copy in loads:
         copy.start()
     core = place_ref[0]
-    for copy in loads[:4]:
-        copy.wait()
     growth = jnp.exp(sr_ref[:, 128:256])
     c_in = c_ref[...]
     left = lanes((TOK, 128)) < HD
@@ -331,6 +356,8 @@
                 left, growth[:, head : head + 1], growth[:, HEADS + head : HEADS + head + 1]
             )
             sums.append(both + pltpu.roll(both, HD, 1))
+        if q == 0:
+            loads[0].wait()
         y = y_ref[:, cols] + jnp.where(left, sums[0], sums[1])
         g = y * silu(z_ref[:, cols].astype(f32))
         squares = squares + g * g
@@ -342,7 +369,7 @@
     half = INNER // 2
     mine = ny_ref[:, pl.ds(pl.multiple_of(core * half, half), half)]
     theirs = ny_ref[:, pl.ds(pl.multiple_of((1 - core) * half, half), half)]
-    for copy in loads[4:]:
+    for copy in loads[1:]:
         copy.wait()
     for n in range(4):
         cols = slice(n * 512, (n + 1) * 512)
@@ -378,6 +405,17 @@
     )
 
 
+def pack_call(*args):
+    return call(
+        pack_kernel,
+        pltpu.HBM((4, OWN + 8, D), bf16),
+        3,
+        (),
+        [pltpu.VMEM((8, D), bf16), pltpu.SemaphoreType.DMA((8,))],
+        hbm_out=True,
+    )(*args)
+
+
 def project_call(*args):
     outs = [
         ((NSP, 24, 128), bf16), ((ROWS, D), bf16), ((TOK, XB), bf16), ((TOK, 256), f32),
@@ -386,7 +424,7 @@
     return call(
         project_kernel,
         [pltpu.HBM(*o) for o in outs],
-        12,
+        8,
         (0,),
         [
             *(pltpu.VMEM(*o) for o in outs),
@@ -429,16 +467,13 @@
         (0,),
         [
             pltpu.VMEM((TOK, INNER), bf16),
-            pltpu.VMEM((TOK, STATE), bf16),
-            pltpu.VMEM((TOK, 256), f32),
             pltpu.VMEM((TOK, INNER), f32),
-            pltpu.VMEM((TOK, INNER), bf16),
             pltpu.VMEM((INNER // 2, D), bf16),
             pltpu.VMEM((INNER // 2, D), bf16),
-            pltpu.SemaphoreType.DMA((6,)),
+            pltpu.SemaphoreType.DMA((3,)),
         ],
-        hbm=range(3, 9),
-    )(*args[:3], *(pltpu.with_memory_space_constraint(a, pltpu.HBM) for a in args[3:]))
+        hbm=(6, 7, 8),
+    )(*args[:6], *(pltpu.with_memory_space_constraint(a, pltpu.HBM) for a in args[6:]))
 
 
 def sum_call(*args):
@@ -497,7 +532,7 @@
     at = lax.axis_index(SP)
     core = lax.axis_index("dp")
     tp = lax.axis_index("tp")
-    place = jnp.stack([core, at, tp]).astype(jnp.int32)
+    place = jnp.stack([core, at]).astype(jnp.int32)
     row_count = mod_weight.shape[1]
 
     rows = latent[0]
@@ -515,12 +550,9 @@
     part = part.reshape(20, 128)
     part = sent_to_all(part, 8, "sp_0")
     part = jnp.sum(part, axis=0)
-    mods = sent_to_all(part.astype(bf16), 32, ("sp_1", "tp"))
-
-    packed = jnp.concatenate([rows, jnp.pad(halo, ((0, 7), (0, 0)))], axis=0)
-    blocks = [packed]
-    for s in (1, 2, 3):
-        blocks.append(lax.ppermute(packed, "tp", [(i, (i + s) % 4) for i in range(4)]))
+    part = sent_to_all(part, 8, "sp_1")
+    packed = pack_call(part, rows, halo)
+    block = exchanged(packed, "tp")
 
     small = small_weights(w_b, w_c, w_dt)
     other_x = swapped(w_x)
@@ -533,7 +565,7 @@
     own_rates = lax.dynamic_slice_in_dim(decay_rate, at // 8, 1, 1)[:, 0]
 
     send, h, xb, sr, gate = project_call(
-        place, mods, *blocks, context[0], misc, w_x, other_x, small, other_small
+        place, block, context[0], misc, w_x, other_x, small, other_small
     )
     received = exchanged(send, SP)
     y_in, c_in, z_in = inside_call(
@@ -542,7 +574,7 @@
     entering = owner_call(own_rates, received, own_taps)
     states = exchanged(entering, SP)
     partial = output_call(
-        place, states, out_gain[None], c_in, sr, y_in, z_in, w_out, other_out
+        place, states, out_gain[None], c_in, sr, z_in, y_in, w_out, other_out
     )
     tiles = exchanged(partial.reshape(4, OWN, D), "tp")
     return sum_call(tiles, gate)[None]

time: 119 us -> 117 us (0.983)
  starting transfers between devices: 57.4 us -> 50.9 us
  waiting for transfers between devices: 28.1 us -> 33.3 us
    ppermute x3 -> x0, starting transfers between devices: 8.97 us -> none  [shards(): lax.ppermute(packed, 'tp', [(i, (i + s) % 4) for i in range(4)])]
    ppermute x1, waiting for transfers between devices: 0.01 us -> 3.63 us  [shards(): halo = lax.ppermute(edge, ALL, pairs)]
    all_to_all x4 -> x5, starting transfers between devices: 35.1 us -> 38.1 us  [exchanged(): return lax.all_to_all(x, axes, 0, 0, tiled=True)]
    all_to_all x4 -> x5, waiting for transfers between devices: 28.1 us -> 29.6 us  [exchanged(): return lax.all_to_all(x, axes, 0, 0, tiled=True)]
    pallas_call x1 -> x2, Pallas kernels: 4.4 us -> 5.34 us  [the longest x1 4.42 us: project_call(): call(project_kernel, [pltpu.HBM(*o) for o in outs], 8, (0,), [*(pltpu.VME...]
    unnamed x44 -> x36, local copies, waits for them, and re-layouts: 3.13 us -> 2.74 us
  transfers between devices with their start and end apart: 12 -> 10, of which waited for: 3 -> 5; matrix products, arithmetic and copies ran while one was open for 3% -> 2% of each run, Pallas kernels for 4% -> 5%
where the time goes in v4:
time: 117 us; the launch traced here: 116 us
  starting transfers between devices  50.9 us (44%)
  waiting for transfers between devices  33.3 us (28%)
  Pallas kernels  13.5 us (12%)
  blocking collectives  10.6 us (9%)
  local copies, waits for them, and re-layouts  5.43 us (5%)
  other arithmetic  1.82 us (2%)
    all_to_all x5, starting transfers between devices, exchanged(): return lax.all_to_all(x, axes, 0, 0, tiled=True)  38.1 us
    all_to_all x5, waiting for transfers between devices, exchanged(): return lax.all_to_all(x, axes, 0, 0, tiled=True)  29.6 us
    all_to_all x1, blocking collectives, exchanged(): return lax.all_to_all(x, axes, 0, 0, tiled=True)  10.6 us
    ppermute x4, starting transfers between devices, swapped(): return lax.ppermute(x, 'dp', [(0, 1), (1, 0)])  8.65 us
    pallas_call x1, Pallas kernels, project_call(): call(project_kernel, [pltpu.HBM(*o) for o in outs], 8, (0,), [*(pltpu.VME...  4.42 us
    ppermute x1, starting transfers between devices, shards(): halo = lax.ppermute(edge, ALL, pairs)  4.12 us
    ppermute x1, waiting for transfers between devices, shards(): halo = lax.ppermute(edge, ALL, pairs)  3.63 us
    unnamed x36, local copies, waits for them, and re-layouts  2.74 us
  transfers between devices with their start and end apart: 10, of which 5 were waited for; matrix products, arithmetic and copies ran while one was open for 2% of the time, Pallas kernels for 5%

profile of v4, /device:TPU:8, one launch (start us, length us, event | category | flops | bytes accessed | tf_op | source)
XLA Modules:
  0.0 116.2 jit_solution(9527447589587921396)
XLA Ops:
  0.0 0.8 fusion.10
  0.8 0.7 fusion.12
  1.5 0.2 fusion.19
  1.8 0.6 broadcast_in_dim.26
  2.4 10.3 %all-to-all-start = ((f32[8,20,128]{2,1,0:T(8,128)}), f32[8,20,128]{2,1,0:T(8,128)S(1)}, u32[]{:S(2)}, u32[]{:S(2)}) async-start(f32[8,20,128]{2,1,0:T(8,128)} %broadcast_in_dim.26), calls=%async_computation | async-start | bytes 196608 | tf_op jit(solution)/shard_map/all_to_all | solution.py:495
  12.8 1.9 %collective-permute-start.1 = (bf16[1024,512]{1,0:T(8,128)(2,1)}, bf16[1024,512]{1,0:T(8,128)(2,1)}, u32[]{:S(2)}, u32[]{:S(2)}) collective-permute-start(bf16[1024,512]{1,0:T(8,128)(2,1)} %own_x.1), channel_id=1, source_target_pairs={{0,1},{1,0},{2,3},{3,2},{4,5},{5,4},{6,7},{7,6},{8,9},{9,8},{10,11... | collective-permute-start | bytes 3145736 | tf_op jit(solution)/shard_map/ppermute | solution.py:491
  14.7 0.7 slice_bitcast_fusion.1
  15.4 0.2 copy.23
  15.6 0.0 copy-start.6
  15.6 0.1 fusion.1.own_s
  15.8 2.4 %collective-permute-start.2 = (bf16[1024,384]{1,0:T(8,128)(2,1)S(1)}, bf16[1024,384]{1,0:T(8,128)(2,1)S(1)}, u32[]{:S(2)}, u32[]{:S(2)}) collective-permute-start(bf16[1024,384]{1,0:T(8,128)(2,1)S(1)} %fusion.1.own_s), channel_id=1, source_target_pairs={{0,1},{1,0},{2,3},{3,2},{4,5},{5,4},{6,7},{7,6},{8,9},{9,8},{10,11... | collective-permute-start | bytes 2359304 | tf_op jit(solution)/shard_map/ppermute | solution.py:491
  18.2 3.3 %all-to-all-done = f32[8,20,128]{2,1,0:T(8,128)S(1)} async-done(((f32[8,20,128]{2,1,0:T(8,128)}), f32[8,20,128]{2,1,0:T(8,128)S(1)}, u32[]{:S(2)}, u32[]{:S(2)}) %all-to-all-start) | async-done | bytes 81952 | tf_op jit(solution)/shard_map/all_to_all | solution.py:495
  21.5 0.6 broadcast_in_dim.27
  22.2 7.5 %all-to-all-start.1 = ((f32[8,20,128]{2,1,0:T(8,128)}), f32[8,20,128]{2,1,0:T(8,128)S(1)}, u32[]{:S(2)}, u32[]{:S(2)}) async-start(f32[8,20,128]{2,1,0:T(8,128)} %broadcast_in_dim.27), calls=%async_computation.1 | async-start | bytes 196608 | tf_op jit(solution)/shard_map/all_to_all | solution.py:495
  29.7 4.1 %collective-permute-start = (bf16[1,2048]{1,0:T(2,128)(2,1)S(1)}, bf16[1,2048]{1,0:T(2,128)(2,1)S(1)}, u32[]{:S(2)}, u32[]{:S(2)}) collective-permute-start(bf16[1,2048]{1,0:T(2,128)(2,1)S(1)} %fusion.11), channel_id=1, source_target_pairs={{6,8},{14,16},{22,24},{30,32},{38,40},{46,48},{54,56},{62,64},{70,... | collective-permute-start | bytes 12296 | tf_op jit(solution)/shard_map/ppermute | solution.py:542
  33.9 3.6 %collective-permute-done.halo_ref = bf16[1,2048]{1,0:T(2,128)(2,1)S(1)} collective-permute-done((bf16[1,2048]{1,0:T(2,128)(2,1)S(1)}, bf16[1,2048]{1,0:T(2,128)(2,1)S(1)}, u32[]{:S(2)}, u32[]{:S(2)}) %collective-permute-start) | collective-permute-done | bytes 4128 | tf_op jit(solution)/shard_map/ppermute | solution.py:542
  37.5 0.0 copy-start.14
  37.5 0.0 copy-start.15
  37.5 0.0 copy-start.1
  37.5 0.0 copy-start.9
  37.5 0.9 shard_map.163
  38.5 3.9 %all-to-all-start.2 = ((bf16[4,40,2048]{2,1,0:T(8,128)(2,1)}), bf16[4,40,2048]{2,1,0:T(8,128)(2,1)S(1)}, u32[]{:S(2)}, u32[]{:S(2)}) async-start(bf16[4,40,2048]{2,1,0:T(8,128)(2,1)} %shard_map.163), calls=%async_computation.2 | async-start | bytes 1310720 | tf_op jit(solution)/shard_map/all_to_all | solution.py:495
  42.4 0.1 pad_add_fusion.place_ref
  42.5 0.1 reshape.32
  42.6 8.6 %all-to-all-done.2.blk_ref = bf16[4,40,2048]{2,1,0:T(8,128)(2,1)S(1)} async-done(((bf16[4,40,2048]{2,1,0:T(8,128)(2,1)}), bf16[4,40,2048]{2,1,0:T(8,128)(2,1)S(1)}, u32[]{:S(2)}, u32[]{:S(2)}) %all-to-all-start.2) | async-done | bytes 655392 | tf_op jit(solution)/shard_map/all_to_all | solution.py:495
  51.2 0.0 collective-permute-done.2.other_s
  51.2 4.4 %shard_map.164 = (bf16[64,24,128]{2,1,0:T(8,128)(2,1)}, bf16[144,2048]{1,0:T(8,128)(2,1)}, bf16[128,640]{1,0:T(8,128)(2,1)}, f32[128,256]{1,0:T(8,128)}, f32[8,2048]{1,0:T(8,128)}) custom-call(s32[2]{0:T(128)S(1)} %pad_add_fusion.place_ref, bf16[4,40,2048]{2,1,0:T(8,128)(2,1)S(1)} %all-to-all-done.2.blk_ref, bf16[8,2048]{1,0:T(8,128)(2,1)S(1)} %bitcast.29, ...), custom_call_target="tpu_custom_call" | custom-call | flops 100000000 | bytes 1048576 | tf_op jit(solution)/shard_map/pallas_call | solution.py:424
  55.6 0.0 copy-start.16
  55.7 0.0 copy-start.2
  55.7 0.0 copy-start.4
  55.7 11.5 %all-to-all-start.3 = ((bf16[64,24,128]{2,1,0:T(8,128)(2,1)}), bf16[64,24,128]{2,1,0:T(8,128)(2,1)S(1)}, u32[]{:S(2)}, u32[]{:S(2)}) async-start(bf16[64,24,128]{2,1,0:T(8,128)(2,1)} %get-tuple-element.13), calls=%async_computation.3 | async-start | bytes 786432 | tf_op jit(solution)/shard_map/all_to_all | solution.py:495
  67.1 1.9 %collective-permute-start.3 = (bf16[1024,512]{1,0:T(8,128)(2,1)}, bf16[1024,512]{1,0:T(8,128)(2,1)}, u32[]{:S(2)}, u32[]{:S(2)}) collective-permute-start(bf16[1024,512]{1,0:T(8,128)(2,1)} %own_z.1), channel_id=1, source_target_pairs={{0,1},{1,0},{2,3},{3,2},{4,5},{5,4},{6,7},{7,6},{8,9},{9,8},{10,11... | collective-permute-start | bytes 3145736 | tf_op jit(solution)/shard_map/ppermute | solution.py:491
  69.1 2.4 %collective-permute-start.4 = (bf16[256,2048]{1,0:T(8,128)(2,1)}, bf16[256,2048]{1,0:T(8,128)(2,1)}, u32[]{:S(2)}, u32[]{:S(2)}) collective-permute-start(bf16[256,2048]{1,0:T(8,128)(2,1)} %own_hbm.1), channel_id=1, source_target_pairs={{0,1},{1,0},{2,3},{3,2},{4,5},{5,4},{6,7},{7,6},{8,9},{9,8},{10,11... | collective-permute-start | bytes 3145736 | tf_op jit(solution)/shard_map/ppermute | solution.py:491
  71.5 0.2 fusion.15.rate_ref
  71.7 0.1 constant_dynamic-slice_fusion
  71.8 0.1 constant_dynamic-slice_fusion.1
  71.9 0.1 fusion.17.tap_ref
  71.9 9.5 %all-to-all-done.3.recv_ref = bf16[64,24,128]{2,1,0:T(8,128)(2,1)S(1)} async-done(((bf16[64,24,128]{2,1,0:T(8,128)(2,1)}), bf16[64,24,128]{2,1,0:T(8,128)(2,1)S(1)}, u32[]{:S(2)}, u32[]{:S(2)}) %all-to-all-start.3) | async-done | bytes 393248 | tf_op jit(solution)/shard_map/all_to_all | solution.py:495
  81.5 2.6 %shard_map.165 = bf16[64,16,128]{2,1,0:T(8,128)(2,1)} custom-call(f32[2]{0:T(128)S(1)} %fusion.15.rate_ref, bf16[64,24,128]{2,1,0:T(8,128)(2,1)S(1)} %all-to-all-done.3.recv_ref, f32[3,128]{1,0:T(4,128)S(1)} %fusion.17.tap_ref), custom_call_target="tpu_custom_call" | custom-call | flops 100000000 | bytes 1048576 | tf_op jit(solution)/shard_map/pallas_call | solution.py:453
  84.1 4.9 %all-to-all-start.4 = ((bf16[64,16,128]{2,1,0:T(8,128)(2,1)}), bf16[64,16,128]{2,1,0:T(8,128)(2,1)S(1)}, u32[]{:S(2)}, u32[]{:S(2)}) async-start(bf16[64,16,128]{2,1,0:T(8,128)(2,1)} %shard_map.165), calls=%async_computation.4 | async-start | bytes 524288 | tf_op jit(solution)/shard_map/all_to_all | solution.py:495
  89.1 1.1 copy-done.3
  90.1 0.9 copy-done.7
  91.0 2.2 %shard_map.166 = (f32[128,512]{1,0:T(8,128)S(1)}, bf16[128,128]{1,0:T(8,128)(2,1)S(1)}, bf16[128,512]{1,0:T(8,128)(2,1)S(1)}) custom-call(s32[2]{0:T(128)S(1)} %pad_add_fusion.place_ref, bf16[144,2048]{1,0:T(8,128)(2,1)S(1)} %copy-done.3, bf16[1024,512]{1,0:T(8,128)(2,1)S(1)} %copy-done.2, bf16[1024,512]{1,0:T(8,128)(2,1)} %collective-permute-done.3.other_z, ...), custom_call_target="tpu_custom_call" | custom-call | flops 100000000 | bytes 1048576 | tf_op jit(solution)/shard_map/pallas_call | solution.py:439
  93.2 0.7 copy-done.5
  93.9 8.2 %all-to-all-done.4.state_ref = bf16[64,16,128]{2,1,0:T(8,128)(2,1)S(1)} async-done(((bf16[64,16,128]{2,1,0:T(8,128)(2,1)}), bf16[64,16,128]{2,1,0:T(8,128)(2,1)S(1)}, u32[]{:S(2)}, u32[]{:S(2)}) %all-to-all-start.4) | async-done | bytes 262176 | tf_op jit(solution)/shard_map/all_to_all | solution.py:495
  102.1 2.7 %shard_map.167 = bf16[128,2048]{1,0:T(8,128)(2,1)S(1)} custom-call(s32[2]{0:T(128)S(1)} %pad_add_fusion.place_ref, bf16[64,16,128]{2,1,0:T(8,128)(2,1)S(1)} %all-to-all-done.4.state_ref, bf16[1,512]{1,0:T(2,128)(2,1)S(1)} %broadcast_in_dim.30.gain_ref, bf16[128,128]{1,0:T(8,128)(2,1)S(1)} %get-tuple-element.17.c_ref, f32[128,256]{1,0:T(8,128)S(1)} %copy-done.4, ...), custom_call_target="tpu_custom_call" | custom-call | flops 100000000 | bytes 1048576 | tf_op jit(solution)/shard_map/pallas_call | solution.py:463
  104.8 10.6 %all_to_all.30.tile_ref = bf16[4,32,2048]{2,1,0:T(8,128)(2,1)S(1)} all-to-all(bf16[4,32,2048]{2,1,0:T(8,128)(2,1)S(1)} %bitcast.27), channel_id=1, replica_groups=mesh['sp_0'=8,'sp_1'=8,'tp'=4,'dp'=2] {'tp'}, dimensions={0} | all-to-all | bytes 1048576 | tf_op jit(solution)/shard_map/all_to_all | solution.py:495
  115.4 0.7 shard_map.168
  (40 shorter events, 0.2 us)
Async XLA Ops:
  0.0 1.5 %copy-start = (bf16[3,32,512]{2,1,0:T(8,128)(2,1)S(1)}, bf16[3,32,512]{2,1,0:T(8,128)(2,1)}, u32[]{:S(2)}) copy-start(bf16[3,32,512]{2,1,0:T(8,128)(2,1)} %param.21) | copy-start | bytes 294916
  0.0 15.6 %copy-start.11 = (bf16[1024,128]{1,0:T(8,128)(2,1)S(1)}, bf16[1024,128]{1,0:T(8,128)(2,1)}, u32[]{:S(2)}) copy-start(bf16[1024,128]{1,0:T(8,128)(2,1)} %param.24) | copy-start | bytes 786436
  0.0 15.6 %copy-start.10 = (bf16[1024,128]{1,0:T(8,128)(2,1)S(1)}, bf16[1024,128]{1,0:T(8,128)(2,1)}, u32[]{:S(2)}) copy-start(bf16[1024,128]{1,0:T(8,128)(2,1)} %param.25) | copy-start | bytes 786436
  2.4 19.0 %all-to-all-start = ((f32[8,20,128]{2,1,0:T(8,128)}), f32[8,20,128]{2,1,0:T(8,128)S(1)}, u32[]{:S(2)}, u32[]{:S(2)}) async-start(f32[8,20,128]{2,1,0:T(8,128)} %broadcast_in_dim.26), calls=%async_computation | async-start | bytes 196608 | tf_op jit(solution)/shard_map/all_to_all | solution.py:495
  12.8 38.4 %collective-permute-start.1 = (bf16[1024,512]{1,0:T(8,128)(2,1)}, bf16[1024,512]{1,0:T(8,128)(2,1)}, u32[]{:S(2)}, u32[]{:S(2)}) collective-permute-start(bf16[1024,512]{1,0:T(8,128)(2,1)} %own_x.1), channel_id=1, source_target_pairs={{0,1},{1,0},{2,3},{3,2},{4,5},{5,4},{6,7},{7,6},{8,9},{9,8},{10,11... | collective-permute-start | bytes 3145736 | tf_op jit(solution)/shard_map/ppermute | solution.py:491
  15.6 14.1 %copy-start.6 = (bf16[1,32,2048]{2,1,0:T(8,128)(2,1)S(1)}, bf16[1,32,2048]{2,1,0:T(8,128)(2,1)}, u32[]{:S(2)}) copy-start(bf16[1,32,2048]{2,1,0:T(8,128)(2,1)} %param.17) | copy-start | bytes 393220
  15.8 35.4 %collective-permute-start.2 = (bf16[1024,384]{1,0:T(8,128)(2,1)S(1)}, bf16[1024,384]{1,0:T(8,128)(2,1)S(1)}, u32[]{:S(2)}, u32[]{:S(2)}) collective-permute-start(bf16[1024,384]{1,0:T(8,128)(2,1)S(1)} %fusion.1.own_s), channel_id=1, source_target_pairs={{0,1},{1,0},{2,3},{3,2},{4,5},{5,4},{6,7},{7,6},{8,9},{9,8},{10,11... | collective-permute-start | bytes 2359304 | tf_op jit(solution)/shard_map/ppermute | solution.py:491
  22.2 15.3 %all-to-all-start.1 = ((f32[8,20,128]{2,1,0:T(8,128)}), f32[8,20,128]{2,1,0:T(8,128)S(1)}, u32[]{:S(2)}, u32[]{:S(2)}) async-start(f32[8,20,128]{2,1,0:T(8,128)} %broadcast_in_dim.27), calls=%async_computation.1 | async-start | bytes 196608 | tf_op jit(solution)/shard_map/all_to_all | solution.py:495
  29.7 7.8 %collective-permute-start = (bf16[1,2048]{1,0:T(2,128)(2,1)S(1)}, bf16[1,2048]{1,0:T(2,128)(2,1)S(1)}, u32[]{:S(2)}, u32[]{:S(2)}) collective-permute-start(bf16[1,2048]{1,0:T(2,128)(2,1)S(1)} %fusion.11), channel_id=1, source_target_pairs={{6,8},{14,16},{22,24},{30,32},{38,40},{46,48},{54,56},{62,64},{70,... | collective-permute-start | bytes 12296 | tf_op jit(solution)/shard_map/ppermute | solution.py:542
  37.5 5.0 %copy-start.13 = (bf16[2048]{0:T(1024)(128)(2,1)S(1)}, bf16[2048]{0:T(1024)(128)(2,1)}, u32[]{:S(2)}) copy-start(bf16[2048]{0:T(1024)(128)(2,1)} %param.22) | copy-start | bytes 12292
  37.5 5.0 %copy-start.17 = (f32[2,8]{1,0:T(2,128)S(1)}, f32[2,8]{1,0:T(2,128)}, u32[]{:S(2)}) copy-start(f32[2,8]{1,0:T(2,128)} %param.31) | copy-start | bytes 196
  37.5 5.1 %copy-start.12 = (bf16[3,512]{1,0:T(4,128)(2,1)S(1)}, bf16[3,512]{1,0:T(4,128)(2,1)}, u32[]{:S(2)}) copy-start(bf16[3,512]{1,0:T(4,128)(2,1)} %param.28) | copy-start | bytes 9220
  37.5 5.1 %copy-start.14 = (bf16[3,128]{1,0:T(4,128)(2,1)S(1)}, bf16[3,128]{1,0:T(4,128)(2,1)}, u32[]{:S(2)}) copy-start(bf16[3,128]{1,0:T(4,128)(2,1)} %param.29) | copy-start | bytes 2308
  37.5 5.1 %copy-start.15 = (bf16[3,128]{1,0:T(4,128)(2,1)S(1)}, bf16[3,128]{1,0:T(4,128)(2,1)}, u32[]{:S(2)}) copy-start(bf16[3,128]{1,0:T(4,128)(2,1)} %param.30) | copy-start | bytes 2308
  37.5 13.7 %copy-start.1 = (bf16[1024,512]{1,0:T(8,128)(2,1)S(1)}, bf16[1024,512]{1,0:T(8,128)(2,1)}, u32[]{:S(2)}) copy-start(bf16[1024,512]{1,0:T(8,128)(2,1)} %own_x.1) | copy-start | bytes 3145732
  37.5 13.7 %copy-start.9 = (bf16[1,8,2048]{2,1,0:T(8,128)(2,1)S(1)}, bf16[1,8,2048]{2,1,0:T(8,128)(2,1)}, u32[]{:S(2)}) copy-start(bf16[1,8,2048]{2,1,0:T(8,128)(2,1)} %param.19) | copy-start | bytes 98308
  38.5 12.7 %all-to-all-start.2 = ((bf16[4,40,2048]{2,1,0:T(8,128)(2,1)}), bf16[4,40,2048]{2,1,0:T(8,128)(2,1)S(1)}, u32[]{:S(2)}, u32[]{:S(2)}) async-start(bf16[4,40,2048]{2,1,0:T(8,128)(2,1)} %shard_map.163), calls=%async_computation.2 | async-start | bytes 1310720 | tf_op jit(solution)/shard_map/all_to_all | solution.py:495
  55.6 33.4 %copy-start.16 = (bf16[512]{0:T(512)(128)(2,1)S(1)}, bf16[512]{0:T(512)(128)(2,1)}, u32[]{:S(2)}) copy-start(bf16[512]{0:T(512)(128)(2,1)} %param.32) | copy-start | bytes 3076
  55.7 33.4 %copy-start.2 = (bf16[1024,512]{1,0:T(8,128)(2,1)S(1)}, bf16[1024,512]{1,0:T(8,128)(2,1)}, u32[]{:S(2)}) copy-start(bf16[1024,512]{1,0:T(8,128)(2,1)} %own_z.1) | copy-start | bytes 3145732
  55.7 33.4 %copy-start.4 = (f32[128,256]{1,0:T(8,128)S(1)}, f32[128,256]{1,0:T(8,128)}, u32[]{:S(2)}) copy-start(f32[128,256]{1,0:T(8,128)} %get-tuple-element.16.sr_ref) | copy-start | bytes 393220
  55.7 25.8 %all-to-all-start.3 = ((bf16[64,24,128]{2,1,0:T(8,128)(2,1)}), bf16[64,24,128]{2,1,0:T(8,128)(2,1)S(1)}, u32[]{:S(2)}, u32[]{:S(2)}) async-start(bf16[64,24,128]{2,1,0:T(8,128)(2,1)} %get-tuple-element.13), calls=%async_computation.3 | async-start | bytes 786432 | tf_op jit(solution)/shard_map/all_to_all | solution.py:495
  67.1 21.9 %collective-permute-start.3 = (bf16[1024,512]{1,0:T(8,128)(2,1)}, bf16[1024,512]{1,0:T(8,128)(2,1)}, u32[]{:S(2)}, u32[]{:S(2)}) collective-permute-start(bf16[1024,512]{1,0:T(8,128)(2,1)} %own_z.1), channel_id=1, source_target_pairs={{0,1},{1,0},{2,3},{3,2},{4,5},{5,4},{6,7},{7,6},{8,9},{9,8},{10,11... | collective-permute-start | bytes 3145736 | tf_op jit(solution)/shard_map/ppermute | solution.py:491
  69.1 24.9 %collective-permute-start.4 = (bf16[256,2048]{1,0:T(8,128)(2,1)}, bf16[256,2048]{1,0:T(8,128)(2,1)}, u32[]{:S(2)}, u32[]{:S(2)}) collective-permute-start(bf16[256,2048]{1,0:T(8,128)(2,1)} %own_hbm.1), channel_id=1, source_target_pairs={{0,1},{1,0},{2,3},{3,2},{4,5},{5,4},{6,7},{7,6},{8,9},{9,8},{10,11... | collective-permute-start | bytes 3145736 | tf_op jit(solution)/shard_map/ppermute | solution.py:491
  84.1 18.0 %all-to-all-start.4 = ((bf16[64,16,128]{2,1,0:T(8,128)(2,1)}), bf16[64,16,128]{2,1,0:T(8,128)(2,1)S(1)}, u32[]{:S(2)}, u32[]{:S(2)}) async-start(bf16[64,16,128]{2,1,0:T(8,128)(2,1)} %shard_map.165), calls=%async_computation.4 | async-start | bytes 524288 | tf_op jit(solution)/shard_map/all_to_all | solution.py:495
  89.0 1.1 copy-start.3
  90.1 0.9 copy-start.7
  93.2 0.7 copy-start.5
  104.8 10.6 %copy-start.8 = (f32[8,2048]{1,0:T(8,128)S(1)}, f32[8,2048]{1,0:T(8,128)}, u32[]{:S(2)}) copy-start(f32[8,2048]{1,0:T(8,128)} %get-tuple-element.20.gate_ref) | copy-start | bytes 196612

commit v5 on v3

--- a/solution.py
+++ b/solution.py
@@ -8,7 +8,6 @@
 
 
 SP = ("sp_0", "sp_1")
-ALL = ("sp_0", "sp_1", "tp")
 EPSILON = 1e-06
 INTERPRET = False
 
@@ -24,7 +23,6 @@
 CTX_DEV = 8
 CTX = NSP * CTX_DEV
 XB = INNER + STATE
-XBC = INNER + 2 * STATE
 ROWS = TOK + 16
 
 f32 = jnp.float32
@@ -89,12 +87,39 @@
     )
 
 
+def start_kernel(place_ref, cond_ref, source_ref, weight_ref, out_hbm, out_ref, sem):
+    at = place_ref[1]
+    both = jnp.concatenate(
+        [
+            ref[0:1, pl.ds(pl.multiple_of(at // 4 * 128, 128), 128)].astype(f32)
+            for ref in (cond_ref, source_ref)
+        ]
+        + [jnp.zeros((6, 128), f32)],
+        axis=0,
+    )
+    both = pltpu.roll(both, (128 - at % 4 * 32) % 128, 1)
+    act = silu(both)[:, 0:32].astype(bf16)
+    rows = []
+    sums = [jnp.dot(act, weight_ref[k], preferred_element_type=f32) for k in range(3)]
+    for k, which in ((0, 0), (1, 0), (0, 1), (1, 1), (2, 0)):
+        rows += [sums[k][which : which + 1, q * 128 : (q + 1) * 128] for q in range(4)]
+    out = jnp.concatenate(rows, axis=0)
+    for peer in range(8):
+        out_ref[peer] = out
+    copy = pltpu.make_async_copy(out_ref, out_hbm, sem)
+    copy.start()
+    copy.wait()
+
+
 def project_kernel(
-    place_ref, mod_ref, blk0_ref, blk1_ref, blk2_ref, blk3_ref, ctx_ref, misc_ref,
-    own_x, other_x, own_s, other_s,
+    place_ref, mod_ref, blk0_ref, blk1_ref, blk2_ref, blk3_ref, edge_ref, ctx_ref, misc_ref,
+    own_x, own_s, other_s, other_x_hbm,
     send_hbm, h_hbm, xb_hbm, sr_hbm, gate_hbm,
-    send_ref, h_ref, xb_ref, sr_ref, gate_ref, conv_ref, sems,
+    send_ref, h_ref, xb_ref, sr_ref, gate_ref, conv_ref, other_x, sems,
 ):
+    load = pltpu.make_async_copy(other_x_hbm, other_x, sems.at[5])
+    load.start()
+
     def store(i, src, dst):
         copy = pltpu.make_async_copy(src, dst, sems.at[i])
         copy.start()
@@ -103,13 +128,11 @@
     core, at, tp = place_ref[0], place_ref[1], place_ref[2]
     blocks = (blk0_ref, blk1_ref, blk2_ref, blk3_ref)
     origin = [lax.rem(tp + 4 - s, 4) for s in range(4)]
-    is_first = [jnp.where(o == 0, 1.0, 0.0) for o in origin]
-    is_last = [jnp.where(o == 3, 1.0, 0.0) for o in origin]
     mods = []
     for t in range(4):
-        total = mod_ref[t].astype(f32)
+        total = mod_ref[t]
         for y in range(1, 8):
-            total = total + mod_ref[4 * y + t].astype(f32)
+            total = total + mod_ref[4 * y + t]
         mods.append(total)
 
     def inverse(ref):
@@ -120,31 +143,28 @@
         return lax.rsqrt(jnp.sum(squares, axis=1, keepdims=True) * (1.0 / D) + EPSILON)
 
     inv = [inverse(ref) for ref in blocks]
+    inv_edge = inverse(edge_ref)
     inv_ctx = inverse(ctx_ref)
-    row8 = rows_of((8, 128))
     for c in range(16):
         t, q = c // 4, c % 4
         cols = slice(c * 128, (c + 1) * 128)
         gain = misc_ref[0:1, cols]
-        shift, scale = mods[t][q : q + 1], mods[t][4 + q : 5 + q]
-        cshift, cscale = mods[t][8 + q : 9 + q], mods[t][12 + q : 13 + q]
+        shift, scale = mods[t][q : q + 1], 1.0 + mods[t][4 + q : 5 + q]
+        cshift, cscale = mods[t][8 + q : 9 + q], 1.0 + mods[t][12 + q : 13 + q]
         gate_ref[:, cols] = jnp.broadcast_to(mods[t][16 + q : 17 + q], (8, 128))
-        before = jnp.zeros((8, 128), f32)
-        after = jnp.zeros((8, 128), f32)
         for s in range(4):
-            h = blocks[s][:, cols].astype(f32) * inv[s] * gain * (1.0 + scale) + shift
-            h_ref[pl.ds(pl.multiple_of(origin[s] * OWN, OWN), OWN), cols] = h[:OWN].astype(bf16)
-            before = before + h[OWN:] * is_first[s]
-            after = after + h[OWN:] * is_last[s]
-        halo = jnp.where(row8 == 0, before, pltpu.roll(after, 1, 0))
-        ctx = ctx_ref[:, cols].astype(f32) * inv_ctx * gain * (1.0 + cscale) + cshift
-        h_ref[TOK:ROWS, cols] = jnp.concatenate([halo, ctx], axis=0).astype(bf16)
+            h = blocks[s][:, cols].astype(f32) * inv[s] * gain * scale + shift
+            h_ref[pl.ds(pl.multiple_of(origin[s] * OWN, OWN), OWN), cols] = h.astype(bf16)
+        edge = edge_ref[:, cols].astype(f32) * inv_edge * gain * scale + shift
+        ctx = ctx_ref[:, cols].astype(f32) * inv_ctx * gain * cscale + cshift
+        h_ref[TOK:ROWS, cols] = jnp.concatenate([edge, ctx], axis=0).astype(bf16)
     stores = [store(0, h_ref, h_hbm), store(1, gate_ref, gate_hbm)]
 
     p = projected(h_ref, core, own_s, other_s, slice(2 * STATE, 2 * STATE + 128))
     step = softplus(p[:TOK])
     ctx_dt = p[TOK + 8 :]
-    log_decay = -(misc_ref[4:5, 0:128] * step)
+    rate = misc_ref[4:5, 0:128] + pltpu.roll(misc_ref[4:8, 0:128], HEADS, 1)[1:2]
+    log_decay = -(rate * step)
     ri, ci = rows_of((TOK, TOK)), lanes((TOK, TOK))
     lower = jnp.where(ri >= ci, 1.0, 0.0).astype(f32)
     upper = jnp.where(ri <= ci, 1.0, 0.0).astype(f32)
@@ -162,6 +182,7 @@
     ctx_b = p[TOK + 8 :]
     b_in = softened(p, misc_ref, INNER, conv_ref, before_ok, after_ok)
     xb_ref[:, INNER:] = b_in
+    load.wait()
     p = projected(h_ref, core, own_x, other_x, slice(0, INNER))
     ctx_x = p[TOK + 8 :]
     x_in = softened(p, misc_ref, 0, conv_ref, before_ok, after_ok)
@@ -300,23 +321,18 @@
 
 
 def output_kernel(
-    place_ref, state_ref, gain_ref, c_hbm, sr_hbm, y_hbm, z_hbm, own_hbm, other_hbm,
-    out_ref, ny_ref, c_ref, sr_ref, y_ref, z_ref, own_ref, other_ref, sems,
+    place_ref, state_ref, gain_ref, c_ref, sr_ref, z_ref, y_hbm, own_hbm, other_hbm,
+    out_ref, ny_ref, y_ref, own_ref, other_ref, sems,
 ):
     loads = [
         pltpu.make_async_copy(src, dst, sems.at[i])
         for i, (src, dst) in enumerate(
-            (
-                (c_hbm, c_ref), (sr_hbm, sr_ref), (y_hbm, y_ref), (z_hbm, z_ref),
-                (own_hbm, own_ref), (other_hbm, other_ref),
-            )
+            ((y_hbm, y_ref), (own_hbm, own_ref), (other_hbm, other_ref))
         )
     ]
     for copy in loads:
         copy.start()
     core = place_ref[0]
-    for copy in loads[:4]:
-        copy.wait()
     growth = jnp.exp(sr_ref[:, 128:256])
     c_in = c_ref[...]
     left = lanes((TOK, 128)) < HD
@@ -331,6 +347,8 @@
                 left, growth[:, head : head + 1], growth[:, HEADS + head : HEADS + head + 1]
             )
             sums.append(both + pltpu.roll(both, HD, 1))
+        if q == 0:
+            loads[0].wait()
         y = y_ref[:, cols] + jnp.where(left, sums[0], sums[1])
         g = y * silu(z_ref[:, cols].astype(f32))
         squares = squares + g * g
@@ -342,7 +360,7 @@
     half = INNER // 2
     mine = ny_ref[:, pl.ds(pl.multiple_of(core * half, half), half)]
     theirs = ny_ref[:, pl.ds(pl.multiple_of((1 - core) * half, half), half)]
-    for copy in loads[4:]:
+    for copy in loads[1:]:
         copy.wait()
     for n in range(4):
         cols = slice(n * 512, (n + 1) * 512)
@@ -378,6 +396,17 @@
     )
 
 
+def start_call(*args):
+    return call(
+        start_kernel,
+        pltpu.HBM((8, 20, 128), f32),
+        4,
+        (0,),
+        [pltpu.VMEM((8, 20, 128), f32), pltpu.SemaphoreType.DMA(())],
+        hbm_out=True,
+    )(*args)
+
+
 def project_call(*args):
     outs = [
         ((NSP, 24, 128), bf16), ((ROWS, D), bf16), ((TOK, XB), bf16), ((TOK, 256), f32),
@@ -386,15 +415,17 @@
     return call(
         project_kernel,
         [pltpu.HBM(*o) for o in outs],
-        12,
+        13,
         (0,),
         [
             *(pltpu.VMEM(*o) for o in outs),
             pltpu.VMEM((TOK + 16, INNER), f32),
-            pltpu.SemaphoreType.DMA((5,)),
+            pltpu.VMEM((HALF, INNER), bf16),
+            pltpu.SemaphoreType.DMA((6,)),
         ],
+        hbm=(12,),
         hbm_out=True,
-    )(*args)
+    )(*args[:12], pltpu.with_memory_space_constraint(args[12], pltpu.HBM))
 
 
 def inside_call(*args):
@@ -429,16 +460,13 @@
         (0,),
         [
             pltpu.VMEM((TOK, INNER), bf16),
-            pltpu.VMEM((TOK, STATE), bf16),
-            pltpu.VMEM((TOK, 256), f32),
             pltpu.VMEM((TOK, INNER), f32),
-            pltpu.VMEM((TOK, INNER), bf16),
             pltpu.VMEM((INNER // 2, D), bf16),
             pltpu.VMEM((INNER // 2, D), bf16),
-            pltpu.SemaphoreType.DMA((6,)),
+            pltpu.SemaphoreType.DMA((3,)),
         ],
-        hbm=range(3, 9),
-    )(*args[:3], *(pltpu.with_memory_space_constraint(a, pltpu.HBM) for a in args[3:]))
+        hbm=(6, 7, 8),
+    )(*args[:6], *(pltpu.with_memory_space_constraint(a, pltpu.HBM) for a in args[6:]))
 
 
 def sum_call(*args):
@@ -471,15 +499,16 @@
 
 
 def packed_vectors(norm_gain, conv_x, conv_b, conv_c, decay_rate):
-    taps = jnp.concatenate([conv_x, conv_b, conv_c], axis=1).astype(f32)
-    rates = decay_rate.reshape(1, 2 * HEADS)
-    return jnp.concatenate(
-        [
-            norm_gain.astype(f32)[None],
-            jnp.pad(taps, ((0, 0), (0, D - XBC))),
-            jnp.pad(rates, ((0, 3), (0, D - 2 * HEADS))),
-        ],
-        axis=0,
+    def placed(v, row, col):
+        v = v.astype(f32)
+        return jnp.pad(v, ((row, 8 - row - v.shape[0]), (col, D - col - v.shape[1])))
+
+    return (
+        placed(norm_gain[None], 0, 0)
+        + placed(conv_x, 1, 0)
+        + placed(conv_b, 1, INNER)
+        + placed(conv_c, 1, XB)
+        + placed(decay_rate, 4, 0)
     )
 
 
@@ -498,29 +527,25 @@
     core = lax.axis_index("dp")
     tp = lax.axis_index("tp")
     place = jnp.stack([core, at, tp]).astype(jnp.int32)
-    row_count = mod_weight.shape[1]
+
+    part = start_call(place, condition, context_source[None], mod_weight)
+    part = exchanged(part, "sp_0")
+    part = jnp.sum(part, axis=0)
+    mods = sent_to_all(part, 32, ("sp_1", "tp"))
 
     rows = latent[0]
-    edge = jnp.where(tp == 3, rows[OWN - 1 :], rows[:1])
-    pairs = [(4 * i + 3, 4 * i + 4) for i in range(NSP - 1)]
-    pairs += [(j, i) for i, j in pairs]
-    halo = lax.ppermute(edge, ALL, pairs)
-
-    act = jnp.stack(
-        [silu(condition[0].astype(f32)), silu(context_source.astype(f32))]
-    ).astype(bf16)
-    act = lax.dynamic_slice_in_dim(act, at * row_count, row_count, 1)
-    part = jnp.einsum("ar,krc->akc", act, mod_weight, preferred_element_type=f32)
-    part = jnp.stack([part[0, 0], part[0, 1], part[1, 0], part[1, 1], part[0, 2]])
-    part = part.reshape(20, 128)
-    part = sent_to_all(part, 8, "sp_0")
-    part = jnp.sum(part, axis=0)
-    mods = sent_to_all(part.astype(bf16), 32, ("sp_1", "tp"))
-
-    packed = jnp.concatenate([rows, jnp.pad(halo, ((0, 7), (0, 0)))], axis=0)
-    blocks = [packed]
+    blocks = [rows]
     for s in (1, 2, 3):
-        blocks.append(lax.ppermute(packed, "tp", [(i, (i + s) % 4) for i in range(4)]))
+        blocks.append(lax.ppermute(rows, "tp", [(i, (i + s) % 4) for i in range(4)]))
+    last, first = rows[OWN - 1 :], rows[:1]
+    for s in (1, 2, 3):
+        origin = (tp + 4 - s) % 4
+        last = jnp.where(origin == 3, blocks[s][OWN - 1 :], last)
+        first = jnp.where(origin == 0, blocks[s][:1], first)
+    up = [(i, i + 1) for i in range(NSP - 1)]
+    before = lax.ppermute(last, SP, up)
+    after = lax.ppermute(first, SP, [(j, i) for i, j in up])
+    edges = jnp.concatenate([before, after, jnp.zeros((6, D), bf16)], axis=0)
 
     small = small_weights(w_b, w_c, w_dt)
     other_x = swapped(w_x)
@@ -533,7 +558,7 @@
     own_rates = lax.dynamic_slice_in_dim(decay_rate, at // 8, 1, 1)[:, 0]
 
     send, h, xb, sr, gate = project_call(
-        place, mods, *blocks, context[0], misc, w_x, other_x, small, other_small
+        place, mods, *blocks, edges, context[0], misc, w_x, small, other_small, other_x
     )
     received = exchanged(send, SP)
     y_in, c_in, z_in = inside_call(
@@ -542,7 +567,7 @@
     entering = owner_call(own_rates, received, own_taps)
     states = exchanged(entering, SP)
     partial = output_call(
-        place, states, out_gain[None], c_in, sr, y_in, z_in, w_out, other_out
+        place, states, out_gain[None], c_in, sr, z_in, y_in, w_out, other_out
     )
     tiles = exchanged(partial.reshape(4, OWN, D), "tp")
     return sum_call(tiles, gate)[None]

time: 119 us -> 131 us (1.10)
  waiting for transfers between devices: 28.1 us -> 32.2 us
  starting transfers between devices: 57.4 us -> 60 us
  blocking collectives: 10.6 us -> 12.1 us
  local copies, waits for them, and re-layouts: 5.88 us -> 7.22 us
    all_to_all x4, waiting for transfers between devices: 28.1 us -> 32.2 us  [exchanged(): return lax.all_to_all(x, axes, 0, 0, tiled=True)]
    ppermute x4 -> x5, starting transfers between devices: 13.5 us -> 17.2 us  [the longest x3 11.4 us: shards(): lax.ppermute(rows, 'tp', [(i, (i + s) % 4) for i in range(4)])]
    another operation x2 -> x0, other arithmetic: 1.49 us -> none
    all_to_all x1, blocking collectives: 10.6 us -> 12.1 us  [exchanged(): return lax.all_to_all(x, axes, 0, 0, tiled=True)]
    pallas_call x1 -> x2, Pallas kernels: 4.4 us -> 5.88 us  [the longest x1 4.48 us: project_call(): call(project_kernel, [pltpu.HBM(*o) for o in outs], 13, (0,), [*(pltpu.VM...]
    unnamed x44 -> x42, local copies, waits for them, and re-layouts: 3.13 us -> 4.32 us
  transfers between devices with their start and end apart: 12 -> 13, of which waited for: 3 -> 3; matrix products, arithmetic and copies ran while one was open for 3% -> 5% of each run, Pallas kernels for 4% -> 5%
where the time goes in v5:
time: 131 us; the launch traced here: 129 us
  starting transfers between devices  60 us (46%)
  waiting for transfers between devices  32.2 us (25%)
  Pallas kernels  14.1 us (11%)
  blocking collectives  12.1 us (9%)
  local copies, waits for them, and re-layouts  7.22 us (6%)
  other arithmetic  3.31 us (3%)
    all_to_all x4, starting transfers between devices, exchanged(): return lax.all_to_all(x, axes, 0, 0, tiled=True)  34 us
    all_to_all x4, waiting for transfers between devices, exchanged(): return lax.all_to_all(x, axes, 0, 0, tiled=True)  32.2 us
    all_to_all x1, blocking collectives, exchanged(): return lax.all_to_all(x, axes, 0, 0, tiled=True)  12.1 us
    ppermute x3, starting transfers between devices, shards(): lax.ppermute(rows, 'tp', [(i, (i + s) % 4) for i in range(4)])  11.4 us
    ppermute x4, starting transfers between devices, swapped(): return lax.ppermute(x, 'dp', [(0, 1), (1, 0)])  8.79 us
    pallas_call x1, Pallas kernels, project_call(): call(project_kernel, [pltpu.HBM(*o) for o in outs], 13, (0,), [*(pltpu.VM...  4.48 us
    unnamed x42, local copies, waits for them, and re-layouts  4.32 us
    ppermute x1, starting transfers between devices, shards(): before = lax.ppermute(last, SP, up)  3.47 us
  transfers between devices with their start and end apart: 13, of which 3 were waited for; matrix products, arithmetic and copies ran while one was open for 5% of the time, Pallas kernels for 5%

profile of v5, /device:TPU:8, one launch (start us, length us, event | category | flops | bytes accessed | tf_op | source)
XLA Modules:
  0.0 129.5 jit_solution(11684158083060012748)
XLA Ops:
  0.0 3.4 %collective-permute-start = (bf16[32,2048]{1,0:T(8,128)(2,1)}, bf16[32,2048]{1,0:T(8,128)(2,1)S(1)}, u32[]{:S(2)}, u32[]{:S(2)}) collective-permute-start(bf16[32,2048]{1,0:T(8,128)(2,1)} %bitcast.16), channel_id=1, source_target_pairs={{0,2},{2,4},{4,6},{6,0},{1,3},{3,5},{5,7},{7,1},{8,10},{10,12},{12... | collective-permute-start | bytes 393224 | tf_op jit(solution)/shard_map/ppermute | solution.py:539
  3.4 4.6 %collective-permute-start.1 = (bf16[32,2048]{1,0:T(8,128)(2,1)}, bf16[32,2048]{1,0:T(8,128)(2,1)S(1)}, u32[]{:S(2)}, u32[]{:S(2)}) collective-permute-start(bf16[32,2048]{1,0:T(8,128)(2,1)} %bitcast.17), channel_id=1, source_target_pairs={{0,4},{2,6},{4,0},{6,2},{1,5},{3,7},{5,1},{7,3},{8,12},{10,14},{12... | collective-permute-start | bytes 393224 | tf_op jit(solution)/shard_map/ppermute | solution.py:539
  8.0 3.3 %collective-permute-start.2 = (bf16[32,2048]{1,0:T(8,128)(2,1)}, bf16[32,2048]{1,0:T(8,128)(2,1)S(1)}, u32[]{:S(2)}, u32[]{:S(2)}) collective-permute-start(bf16[32,2048]{1,0:T(8,128)(2,1)} %bitcast.18), channel_id=1, source_target_pairs={{0,6},{2,0},{4,2},{6,4},{1,7},{3,1},{5,3},{7,5},{8,14},{10,8},{12,... | collective-permute-start | bytes 393224 | tf_op jit(solution)/shard_map/ppermute | solution.py:539
  11.4 0.7 broadcast_in_dim.19.source_ref
  12.1 0.1 pad_add_fusion.1.place_ref
  12.2 0.9 copy-done.11
  13.1 0.7 copy-done.12
  13.8 1.4 %shard_map.163 = f32[8,20,128]{2,1,0:T(8,128)} custom-call(s32[3]{0:T(128)S(1)} %pad_add_fusion.1.place_ref, bf16[1,2048]{1,0:T(2,128)(2,1)S(1)} %copy-done.12, bf16[1,2048]{1,0:T(2,128)(2,1)S(1)} %broadcast_in_dim.19.source_ref, bf16[3,32,512]{2,1,0:T(8,128)(2,1)S(1)} %copy-done.11), custom_call_target="tpu_custom_call" | custom-call | flops 100000000 | bytes 1048576 | tf_op jit(solution)/shard_map/pallas_call | solution.py:400
  15.2 10.3 %all-to-all-start = ((f32[8,20,128]{2,1,0:T(8,128)}), f32[8,20,128]{2,1,0:T(8,128)}, u32[]{:S(2)}, u32[]{:S(2)}) async-start(f32[8,20,128]{2,1,0:T(8,128)} %shard_map.163), calls=%async_computation | async-start | bytes 196608 | tf_op jit(solution)/shard_map/all_to_all | solution.py:488
  25.5 0.0 copy-start.5
  25.5 0.8 slice_bitcast_fusion.1
  26.4 0.2 copy.20
  26.6 0.1 fusion.1.own_s
  26.7 0.0 copy-start.16
  26.7 0.0 copy-start.10
  26.7 2.1 %collective-permute-start.5 = (bf16[1024,384]{1,0:T(8,128)(2,1)S(1)}, bf16[1024,384]{1,0:T(8,128)(2,1)S(1)}, u32[]{:S(2)}, u32[]{:S(2)}) collective-permute-start(bf16[1024,384]{1,0:T(8,128)(2,1)S(1)} %fusion.1.own_s), channel_id=1, source_target_pairs={{0,1},{1,0},{2,3},{3,2},{4,5},{5,4},{6,7},{7,6},{8,9},{9,8},{10,11... | collective-permute-start | bytes 2359304 | tf_op jit(solution)/shard_map/ppermute | solution.py:484
  28.8 2.4 %collective-permute-start.6 = (bf16[1024,512]{1,0:T(8,128)(2,1)S(1)}, bf16[1024,512]{1,0:T(8,128)(2,1)}, u32[]{:S(2)}, u32[]{:S(2)}) collective-permute-start(bf16[1024,512]{1,0:T(8,128)(2,1)S(1)} %copy-done), channel_id=1, source_target_pairs={{0,1},{1,0},{2,3},{3,2},{4,5},{5,4},{6,7},{7,6},{8,9},{9,8},{10,11... | collective-permute-start | bytes 3145736 | tf_op jit(solution)/shard_map/ppermute | solution.py:484
  31.3 0.7 broadcast_select_fusion.5
  32.0 3.5 %collective-permute-start.3 = (bf16[1,2048]{1,0:T(2,128)(2,1)}, bf16[1,2048]{1,0:T(2,128)(2,1)S(1)}, u32[]{:S(2)}, u32[]{:S(2)}) collective-permute-start(bf16[1,2048]{1,0:T(2,128)(2,1)} %get-tuple-element.21), channel_id=1, source_target_pairs={{0,8},{8,16},{16,24},{24,32},{32,40},{40,48},{48,56},{56,64},{64,7... | collective-permute-start | bytes 12296 | tf_op jit(solution)/shard_map/ppermute | solution.py:546
  35.5 2.4 %collective-permute-start.4 = (bf16[1,2048]{1,0:T(2,128)(2,1)S(1)}, bf16[1,2048]{1,0:T(2,128)(2,1)}, u32[]{:S(2)}, u32[]{:S(2)}) collective-permute-start(bf16[1,2048]{1,0:T(2,128)(2,1)S(1)} %get-tuple-element.22), channel_id=1, source_target_pairs={{8,0},{16,8},{24,16},{32,24},{40,32},{48,40},{56,48},{64,56},{72,6... | collective-permute-start | bytes 12296 | tf_op jit(solution)/shard_map/ppermute | solution.py:547
  37.8 0.9 reduce_sum.9
  38.8 0.8 broadcast_in_dim.20
  39.5 8.9 %all-to-all-start.1 = ((f32[32,20,128]{2,1,0:T(8,128)}), f32[32,20,128]{2,1,0:T(8,128)S(1)}, u32[]{:S(2)}, u32[]{:S(2)}) async-start(f32[32,20,128]{2,1,0:T(8,128)} %broadcast_in_dim.20), calls=%async_computation.1 | async-start | bytes 786432 | tf_op jit(solution)/shard_map/all_to_all | solution.py:488
  48.5 0.7 pad_add_fusion.misc_ref
  49.2 0.1 pad.63.clone
  49.3 0.8 maximum_maximum_fusion.edge_ref
  50.1 12.7 %all-to-all-done.1.mod_ref = f32[32,20,128]{2,1,0:T(8,128)S(1)} async-done(((f32[32,20,128]{2,1,0:T(8,128)}), f32[32,20,128]{2,1,0:T(8,128)S(1)}, u32[]{:S(2)}, u32[]{:S(2)}) %all-to-all-start.1) | async-done | bytes 327712 | tf_op jit(solution)/shard_map/all_to_all | solution.py:488
  62.8 0.9 copy-done.7
  63.7 4.5 %shard_map.164 = (bf16[64,24,128]{2,1,0:T(8,128)(2,1)}, bf16[144,2048]{1,0:T(8,128)(2,1)}, bf16[128,640]{1,0:T(8,128)(2,1)}, f32[128,256]{1,0:T(8,128)}, f32[8,2048]{1,0:T(8,128)}) custom-call(s32[3]{0:T(128)S(1)} %pad_add_fusion.1.place_ref, f32[32,20,128]{2,1,0:T(8,128)S(1)} %all-to-all-done.1.mod_ref, bf16[32,2048]{1,0:T(8,128)(2,1)S(1)} %bitcast.19, ...), custom_call_target="tpu_custom_call" | custom-call | flops 100000000 | bytes 1048576 | tf_op jit(solution)/shard_map/pallas_call | solution.py:415
  68.2 0.0 copy-start.1
  68.2 0.0 copy-start.3
  68.3 9.8 %all-to-all-start.2 = ((bf16[64,24,128]{2,1,0:T(8,128)(2,1)}), bf16[64,24,128]{2,1,0:T(8,128)(2,1)S(1)}, u32[]{:S(2)}, u32[]{:S(2)}) async-start(bf16[64,24,128]{2,1,0:T(8,128)(2,1)} %get-tuple-element.13), calls=%async_computation.2 | async-start | bytes 786432 | tf_op jit(solution)/shard_map/all_to_all | solution.py:488
  78.0 1.9 %collective-permute-start.7 = (bf16[1024,512]{1,0:T(8,128)(2,1)}, bf16[1024,512]{1,0:T(8,128)(2,1)}, u32[]{:S(2)}, u32[]{:S(2)}) collective-permute-start(bf16[1024,512]{1,0:T(8,128)(2,1)} %own_z.1), channel_id=1, source_target_pairs={{0,1},{1,0},{2,3},{3,2},{4,5},{5,4},{6,7},{7,6},{8,9},{9,8},{10,11... | collective-permute-start | bytes 3145736 | tf_op jit(solution)/shard_map/ppermute | solution.py:484
  80.0 2.4 %collective-permute-start.8 = (bf16[256,2048]{1,0:T(8,128)(2,1)}, bf16[256,2048]{1,0:T(8,128)(2,1)}, u32[]{:S(2)}, u32[]{:S(2)}) collective-permute-start(bf16[256,2048]{1,0:T(8,128)(2,1)} %own_hbm.1), channel_id=1, source_target_pairs={{0,1},{1,0},{2,3},{3,2},{4,5},{5,4},{6,7},{7,6},{8,9},{9,8},{10,11... | collective-permute-start | bytes 3145736 | tf_op jit(solution)/shard_map/ppermute | solution.py:484
  82.4 0.2 dynamic-slice_reduce_fusion.rate_ref
  82.6 0.1 constant_dynamic-slice_fusion
  82.7 0.1 constant_dynamic-slice_fusion.1
  82.8 0.1 fusion.5.tap_ref
  82.9 10.3 %all-to-all-done.2.recv_ref = bf16[64,24,128]{2,1,0:T(8,128)(2,1)S(1)} async-done(((bf16[64,24,128]{2,1,0:T(8,128)(2,1)}), bf16[64,24,128]{2,1,0:T(8,128)(2,1)S(1)}, u32[]{:S(2)}, u32[]{:S(2)}) %all-to-all-start.2) | async-done | bytes 393248 | tf_op jit(solution)/shard_map/all_to_all | solution.py:488
  93.2 2.6 %shard_map.165 = bf16[64,16,128]{2,1,0:T(8,128)(2,1)} custom-call(f32[2]{0:T(128)S(1)} %dynamic-slice_reduce_fusion.rate_ref, bf16[64,24,128]{2,1,0:T(8,128)(2,1)S(1)} %all-to-all-done.2.recv_ref, f32[3,128]{1,0:T(4,128)S(1)} %fusion.5.tap_ref), custom_call_target="tpu_custom_call" | custom-call | flops 100000000 | bytes 1048576 | tf_op jit(solution)/shard_map/pallas_call | solution.py:446
  95.8 4.9 %all-to-all-start.3 = ((bf16[64,16,128]{2,1,0:T(8,128)(2,1)}), bf16[64,16,128]{2,1,0:T(8,128)(2,1)S(1)}, u32[]{:S(2)}, u32[]{:S(2)}) async-start(bf16[64,16,128]{2,1,0:T(8,128)(2,1)} %shard_map.165), calls=%async_computation.3 | async-start | bytes 524288 | tf_op jit(solution)/shard_map/all_to_all | solution.py:488
  100.9 1.1 copy-done.2
  101.9 2.2 %shard_map.166 = (f32[128,512]{1,0:T(8,128)S(1)}, bf16[128,128]{1,0:T(8,128)(2,1)S(1)}, bf16[128,512]{1,0:T(8,128)(2,1)S(1)}) custom-call(s32[3]{0:T(128)S(1)} %pad_add_fusion.1.place_ref, bf16[144,2048]{1,0:T(8,128)(2,1)S(1)} %copy-done.2, bf16[1024,512]{1,0:T(8,128)(2,1)S(1)} %copy-done.1, bf16[1024,512]{1,0:T(8,128)(2,1)} %collective-permute-done.7.other_z, ...), custom_call_target="tpu_custom_call" | custom-call | flops 100000000 | bytes 1048576 | tf_op jit(solution)/shard_map/pallas_call | solution.py:432
  104.1 0.7 copy-done.4
  104.8 9.1 %all-to-all-done.3.state_ref = bf16[64,16,128]{2,1,0:T(8,128)(2,1)S(1)} async-done(((bf16[64,16,128]{2,1,0:T(8,128)(2,1)}), bf16[64,16,128]{2,1,0:T(8,128)(2,1)S(1)}, u32[]{:S(2)}, u32[]{:S(2)}) %all-to-all-start.3) | async-done | bytes 262176 | tf_op jit(solution)/shard_map/all_to_all | solution.py:488
  113.9 2.7 %shard_map.167 = bf16[128,2048]{1,0:T(8,128)(2,1)S(1)} custom-call(s32[3]{0:T(128)S(1)} %pad_add_fusion.1.place_ref, bf16[64,16,128]{2,1,0:T(8,128)(2,1)S(1)} %all-to-all-done.3.state_ref, bf16[1,512]{1,0:T(2,128)(2,1)S(1)} %broadcast_in_dim.22.gain_ref, bf16[128,128]{1,0:T(8,128)(2,1)S(1)} %get-tuple-element.17.c_ref, f32[128,256]{1,0:T(8,128)S(1)} %copy-done.3, ...), custom_call_target="tpu_custom_call" | custom-call | flops 100000000 | bytes 1048576 | tf_op jit(solution)/shard_map/pallas_call | solution.py:456
  116.6 12.1 %all_to_all.25.tile_ref = bf16[4,32,2048]{2,1,0:T(8,128)(2,1)S(1)} all-to-all(bf16[4,32,2048]{2,1,0:T(8,128)(2,1)S(1)} %bitcast.15), channel_id=1, replica_groups=mesh['sp_0'=8,'sp_1'=8,'tp'=4,'dp'=2] {'tp'}, dimensions={0} | all-to-all | bytes 1048576 | tf_op jit(solution)/shard_map/all_to_all | solution.py:488
  128.7 0.7 shard_map.168
  (46 shorter events, 0.1 us)
Async XLA Ops:
  0.0 31.3 %collective-permute-start = (bf16[32,2048]{1,0:T(8,128)(2,1)}, bf16[32,2048]{1,0:T(8,128)(2,1)S(1)}, u32[]{:S(2)}, u32[]{:S(2)}) collective-permute-start(bf16[32,2048]{1,0:T(8,128)(2,1)} %bitcast.16), channel_id=1, source_target_pairs={{0,2},{2,4},{4,6},{6,0},{1,3},{3,5},{5,7},{7,1},{8,10},{10,12},{12... | collective-permute-start | bytes 393224 | tf_op jit(solution)/shard_map/ppermute | solution.py:539
  3.4 27.9 %collective-permute-start.1 = (bf16[32,2048]{1,0:T(8,128)(2,1)}, bf16[32,2048]{1,0:T(8,128)(2,1)S(1)}, u32[]{:S(2)}, u32[]{:S(2)}) collective-permute-start(bf16[32,2048]{1,0:T(8,128)(2,1)} %bitcast.17), channel_id=1, source_target_pairs={{0,4},{2,6},{4,0},{6,2},{1,5},{3,7},{5,1},{7,3},{8,12},{10,14},{12... | collective-permute-start | bytes 393224 | tf_op jit(solution)/shard_map/ppermute | solution.py:539
  8.0 23.3 %collective-permute-start.2 = (bf16[32,2048]{1,0:T(8,128)(2,1)}, bf16[32,2048]{1,0:T(8,128)(2,1)S(1)}, u32[]{:S(2)}, u32[]{:S(2)}) collective-permute-start(bf16[32,2048]{1,0:T(8,128)(2,1)} %bitcast.18), channel_id=1, source_target_pairs={{0,6},{2,0},{4,2},{6,4},{1,7},{3,1},{5,3},{7,5},{8,14},{10,8},{12,... | collective-permute-start | bytes 393224 | tf_op jit(solution)/shard_map/ppermute | solution.py:539
  12.2 0.9 copy-start.11
  13.1 0.7 copy-start.12
  13.8 12.8 %copy-start.13 = (bf16[1024,128]{1,0:T(8,128)(2,1)S(1)}, bf16[1024,128]{1,0:T(8,128)(2,1)}, u32[]{:S(2)}) copy-start(bf16[1024,128]{1,0:T(8,128)(2,1)} %param.25) | copy-start | bytes 786436
  13.8 12.8 %copy-start.14 = (bf16[1024,128]{1,0:T(8,128)(2,1)S(1)}, bf16[1024,128]{1,0:T(8,128)(2,1)}, u32[]{:S(2)}) copy-start(bf16[1024,128]{1,0:T(8,128)(2,1)} %param.24) | copy-start | bytes 786436
  15.2 22.6 %all-to-all-start = ((f32[8,20,128]{2,1,0:T(8,128)}), f32[8,20,128]{2,1,0:T(8,128)}, u32[]{:S(2)}, u32[]{:S(2)}) async-start(f32[8,20,128]{2,1,0:T(8,128)} %shard_map.163), calls=%async_computation | async-start | bytes 196608 | tf_op jit(solution)/shard_map/all_to_all | solution.py:488
  25.5 3.3 %copy-start = (bf16[1024,512]{1,0:T(8,128)(2,1)S(1)}, bf16[1024,512]{1,0:T(8,128)(2,1)}, u32[]{:S(2)}) copy-start(bf16[1024,512]{1,0:T(8,128)(2,1)} %own_x.1) | copy-start | bytes 3145732
  25.5 5.7 %copy-start.19 = (bf16[2048]{0:T(1024)(128)(2,1)S(1)}, bf16[2048]{0:T(1024)(128)(2,1)}, u32[]{:S(2)}) copy-start(bf16[2048]{0:T(1024)(128)(2,1)} %param.22) | copy-start | bytes 12292
  25.5 5.8 %copy-start.5 = (bf16[1,32,2048]{2,1,0:T(8,128)(2,1)S(1)}, bf16[1,32,2048]{2,1,0:T(8,128)(2,1)}, u32[]{:S(2)}) copy-start(bf16[1,32,2048]{2,1,0:T(8,128)(2,1)} %param.17) | copy-start | bytes 393220
  26.7 21.8 %copy-start.15 = (bf16[3,512]{1,0:T(4,128)(2,1)S(1)}, bf16[3,512]{1,0:T(4,128)(2,1)}, u32[]{:S(2)}) copy-start(bf16[3,512]{1,0:T(4,128)(2,1)} %param.28) | copy-start | bytes 9220
  26.7 21.8 %copy-start.16 = (f32[2,8]{1,0:T(2,128)S(1)}, f32[2,8]{1,0:T(2,128)}, u32[]{:S(2)}) copy-start(f32[2,8]{1,0:T(2,128)} %param.31) | copy-start | bytes 196
  26.7 36.1 %copy-start.10 = (bf16[1,8,2048]{2,1,0:T(8,128)(2,1)S(1)}, bf16[1,8,2048]{2,1,0:T(8,128)(2,1)}, u32[]{:S(2)}) copy-start(bf16[1,8,2048]{2,1,0:T(8,128)(2,1)} %param.19) | copy-start | bytes 98308
  26.7 36.1 %collective-permute-start.5 = (bf16[1024,384]{1,0:T(8,128)(2,1)S(1)}, bf16[1024,384]{1,0:T(8,128)(2,1)S(1)}, u32[]{:S(2)}, u32[]{:S(2)}) collective-permute-start(bf16[1024,384]{1,0:T(8,128)(2,1)S(1)} %fusion.1.own_s), channel_id=1, source_target_pairs={{0,1},{1,0},{2,3},{3,2},{4,5},{5,4},{6,7},{7,6},{8,9},{9,8},{10,11... | collective-permute-start | bytes 2359304 | tf_op jit(solution)/shard_map/ppermute | solution.py:484
  28.8 34.0 %collective-permute-start.6 = (bf16[1024,512]{1,0:T(8,128)(2,1)S(1)}, bf16[1024,512]{1,0:T(8,128)(2,1)}, u32[]{:S(2)}, u32[]{:S(2)}) collective-permute-start(bf16[1024,512]{1,0:T(8,128)(2,1)S(1)} %copy-done), channel_id=1, source_target_pairs={{0,1},{1,0},{2,3},{3,2},{4,5},{5,4},{6,7},{7,6},{8,9},{9,8},{10,11... | collective-permute-start | bytes 3145736 | tf_op jit(solution)/shard_map/ppermute | solution.py:484
  31.3 8.2 %copy-start.6 = (bf16[32,2048]{1,0:T(8,128)(2,1)}, bf16[32,2048]{1,0:T(8,128)(2,1)S(1)}, u32[]{:S(2)}) copy-start(bf16[32,2048]{1,0:T(8,128)(2,1)S(1)} %collective-permute-done.2.blk3_ref) | copy-start | bytes 393220
  32.0 17.3 %collective-permute-start.3 = (bf16[1,2048]{1,0:T(2,128)(2,1)}, bf16[1,2048]{1,0:T(2,128)(2,1)S(1)}, u32[]{:S(2)}, u32[]{:S(2)}) collective-permute-start(bf16[1,2048]{1,0:T(2,128)(2,1)} %get-tuple-element.21), channel_id=1, source_target_pairs={{0,8},{8,16},{16,24},{24,32},{32,40},{40,48},{48,56},{56,64},{64,7... | collective-permute-start | bytes 12296 | tf_op jit(solution)/shard_map/ppermute | solution.py:546
  35.5 13.8 %collective-permute-start.4 = (bf16[1,2048]{1,0:T(2,128)(2,1)S(1)}, bf16[1,2048]{1,0:T(2,128)(2,1)}, u32[]{:S(2)}, u32[]{:S(2)}) collective-permute-start(bf16[1,2048]{1,0:T(2,128)(2,1)S(1)} %get-tuple-element.22), channel_id=1, source_target_pairs={{8,0},{16,8},{24,16},{32,24},{40,32},{48,40},{56,48},{64,56},{72,6... | collective-permute-start | bytes 12296 | tf_op jit(solution)/shard_map/ppermute | solution.py:547
  39.5 23.3 %all-to-all-start.1 = ((f32[32,20,128]{2,1,0:T(8,128)}), f32[32,20,128]{2,1,0:T(8,128)S(1)}, u32[]{:S(2)}, u32[]{:S(2)}) async-start(f32[32,20,128]{2,1,0:T(8,128)} %broadcast_in_dim.20), calls=%async_computation.1 | async-start | bytes 786432 | tf_op jit(solution)/shard_map/all_to_all | solution.py:488
  62.8 0.9 copy-start.7
  63.7 18.7 %copy-start.17 = (f32[2,8]{1,0:T(2,128)S(1)}, f32[2,8]{1,0:T(2,128)}, u32[]{:S(2)}) copy-start(f32[2,8]{1,0:T(2,128)} %param.31) | copy-start | bytes 196
  63.7 18.9 %copy-start.18 = (bf16[3,128]{1,0:T(4,128)(2,1)S(1)}, bf16[3,128]{1,0:T(4,128)(2,1)}, u32[]{:S(2)}) copy-start(bf16[3,128]{1,0:T(4,128)(2,1)} %param.29) | copy-start | bytes 2308
  68.2 32.6 %copy-start.20 = (bf16[512]{0:T(512)(128)(2,1)S(1)}, bf16[512]{0:T(512)(128)(2,1)}, u32[]{:S(2)}) copy-start(bf16[512]{0:T(512)(128)(2,1)} %param.32) | copy-start | bytes 3076
  68.2 32.6 %copy-start.1 = (bf16[1024,512]{1,0:T(8,128)(2,1)S(1)}, bf16[1024,512]{1,0:T(8,128)(2,1)}, u32[]{:S(2)}) copy-start(bf16[1024,512]{1,0:T(8,128)(2,1)} %own_z.1) | copy-start | bytes 3145732
  68.2 32.6 %copy-start.3 = (f32[128,256]{1,0:T(8,128)S(1)}, f32[128,256]{1,0:T(8,128)}, u32[]{:S(2)}) copy-start(f32[128,256]{1,0:T(8,128)} %get-tuple-element.16.sr_ref) | copy-start | bytes 393220
  68.3 32.6 %copy-start.8 = (bf16[128,640]{1,0:T(8,128)(2,1)S(1)}, bf16[128,640]{1,0:T(8,128)(2,1)}, u32[]{:S(2)}) copy-start(bf16[128,640]{1,0:T(8,128)(2,1)} %get-tuple-element.15.xb_ref) | copy-start | bytes 491524
  68.3 24.9 %all-to-all-start.2 = ((bf16[64,24,128]{2,1,0:T(8,128)(2,1)}), bf16[64,24,128]{2,1,0:T(8,128)(2,1)S(1)}, u32[]{:S(2)}, u32[]{:S(2)}) async-start(bf16[64,24,128]{2,1,0:T(8,128)(2,1)} %get-tuple-element.13), calls=%async_computation.2 | async-start | bytes 786432 | tf_op jit(solution)/shard_map/all_to_all | solution.py:488
  78.0 22.8 %collective-permute-start.7 = (bf16[1024,512]{1,0:T(8,128)(2,1)}, bf16[1024,512]{1,0:T(8,128)(2,1)}, u32[]{:S(2)}, u32[]{:S(2)}) collective-permute-start(bf16[1024,512]{1,0:T(8,128)(2,1)} %own_z.1), channel_id=1, source_target_pairs={{0,1},{1,0},{2,3},{3,2},{4,5},{5,4},{6,7},{7,6},{8,9},{9,8},{10,11... | collective-permute-start | bytes 3145736 | tf_op jit(solution)/shard_map/ppermute | solution.py:484
  80.0 24.8 %collective-permute-start.8 = (bf16[256,2048]{1,0:T(8,128)(2,1)}, bf16[256,2048]{1,0:T(8,128)(2,1)}, u32[]{:S(2)}, u32[]{:S(2)}) collective-permute-start(bf16[256,2048]{1,0:T(8,128)(2,1)} %own_hbm.1), channel_id=1, source_target_pairs={{0,1},{1,0},{2,3},{3,2},{4,5},{5,4},{6,7},{7,6},{8,9},{9,8},{10,11... | collective-permute-start | bytes 3145736 | tf_op jit(solution)/shard_map/ppermute | solution.py:484
  95.8 18.1 %all-to-all-start.3 = ((bf16[64,16,128]{2,1,0:T(8,128)(2,1)}), bf16[64,16,128]{2,1,0:T(8,128)(2,1)S(1)}, u32[]{:S(2)}, u32[]{:S(2)}) async-start(bf16[64,16,128]{2,1,0:T(8,128)(2,1)} %shard_map.165), calls=%async_computation.3 | async-start | bytes 524288 | tf_op jit(solution)/shard_map/all_to_all | solution.py:488
  100.8 1.1 copy-start.2
  104.1 0.7 copy-start.4
  116.6 12.1 %copy-start.9 = (f32[8,2048]{1,0:T(8,128)S(1)}, f32[8,2048]{1,0:T(8,128)}, u32[]{:S(2)}) copy-start(f32[8,2048]{1,0:T(8,128)} %get-tuple-element.20.gate_ref) | copy-start | bytes 196612

commit v6 on v4

--- a/solution.py
+++ b/solution.py
@@ -24,7 +24,6 @@
 CTX_DEV = 8
 CTX = NSP * CTX_DEV
 XB = INNER + STATE
-XBC = INNER + 2 * STATE
 ROWS = TOK + 16
 
 f32 = jnp.float32
@@ -89,12 +88,8 @@
     )
 
 
-def pack_kernel(part_ref, rows_ref, halo_ref, out_hbm, tail_ref, sems):
-    copies = [
-        pltpu.make_async_copy(rows_ref, out_hbm.at[t, pl.ds(0, OWN)], sems.at[t]) for t in range(4)
-    ]
-    for copy in copies:
-        copy.start()
+def pack_kernel(part_ref, rows_ref, halo_ref, out_ref):
+    out_ref[0:OWN, :] = rows_ref[...]
     total = part_ref[0]
     for y in range(1, 8):
         total = total + part_ref[y]
@@ -108,73 +103,72 @@
         for r in range(7):
             k = r * 16 + m
             rows.append(parts[k // 20][k % 20 : k % 20 + 1] if k < 60 else zero)
-        tail_ref[:, cols] = jnp.concatenate(rows, axis=0).astype(bf16)
-    more = [
-        pltpu.make_async_copy(tail_ref, out_hbm.at[t, pl.ds(OWN, 8)], sems.at[4 + t])
-        for t in range(4)
-    ]
-    for copy in more:
-        copy.start()
-    for copy in copies + more:
-        copy.wait()
+        out_ref[OWN:, cols] = jnp.concatenate(rows, axis=0).astype(bf16)
 
 
 def project_kernel(
-    place_ref, blk_ref, ctx_ref, misc_ref, own_x, other_x, own_s, other_s,
+    place_ref, blk0_ref, blk1_ref, blk2_ref, blk3_ref, ctx_ref, misc_ref,
+    own_x, other_x, own_s, other_s,
     send_hbm, h_hbm, xb_hbm, sr_hbm, gate_hbm,
-    send_ref, h_ref, xb_ref, sr_ref, gate_ref, conv_ref, sems,
+    send_ref, h_ref, xb_ref, sr_ref, gate_ref, conv_ref, mods_ref, edge_ref, sems,
 ):
     def store(i, src, dst):
         copy = pltpu.make_async_copy(src, dst, sems.at[i])
         copy.start()
         return copy
 
-    core, at = place_ref[0], place_ref[1]
-    mods, tails = [], []
-    for t in range(4):
-        tail = blk_ref[t, OWN:, :].astype(f32)
-        tails.append(tail)
-
-        def row(k, tail=tail):
+    core, at, tp = place_ref[0], place_ref[1], place_ref[2]
+    blocks = (blk0_ref, blk1_ref, blk2_ref, blk3_ref)
+    origin = [lax.rem(tp + 4 - s, 4) for s in range(4)]
+    tails = [ref[OWN:, :].astype(f32) for ref in blocks]
+    for s in range(4):
+
+        def row(k, tail=tails[s]):
             return tail[1 + k // 16 : 2 + k // 16, (k % 16) * 128 : (k % 16 + 1) * 128]
 
-        mods.append([row(i) + row(20 + i) + row(40 + i) for i in range(20)])
-
-    def inverse(rows, read):
+        found = [row(i) + row(20 + i) + row(40 + i) for i in range(20)]
+        found += [jnp.zeros((4, 128), f32)]
+        mods_ref[pl.ds(pl.multiple_of(origin[s] * 24, 8), 24), :] = jnp.concatenate(found, axis=0)
+    row8 = rows_of((8, D))
+    before = sum(t * jnp.where(o == 0, 1.0, 0.0) for t, o in zip(tails, origin))
+    after = sum(t * jnp.where(o == 3, 1.0, 0.0) for t, o in zip(tails, origin))
+    edge_ref[...] = jnp.where(
+        row8 == 0, before, jnp.where(row8 == 1, pltpu.roll(after, 1, 0), 0.0)
+    )
+
+    def inverse(ref, rows):
         squares = jnp.zeros((rows, 128), f32)
         for c in range(16):
-            v = read(slice(c * 128, (c + 1) * 128))
+            v = ref[:rows, c * 128 : (c + 1) * 128].astype(f32)
             squares = squares + v * v
         return lax.rsqrt(jnp.sum(squares, axis=1, keepdims=True) * (1.0 / D) + EPSILON)
 
-    row8 = rows_of((8, 128))
-
-    def neighbours(cols):
-        last = pltpu.roll(tails[3][:, cols], 1, 0)
-        return jnp.where(row8 == 0, tails[0][:, cols], jnp.where(row8 == 1, last, 0.0))
-
-    inv = [inverse(OWN, lambda cols, t=t: blk_ref[t, :OWN, cols].astype(f32)) for t in range(4)]
-    inv_halo = inverse(8, neighbours)
-    inv_ctx = inverse(8, lambda cols: ctx_ref[:, cols].astype(f32))
+    inv = [inverse(ref, OWN) for ref in blocks]
+    inv_edge = inverse(edge_ref, 8)
+    inv_ctx = inverse(ctx_ref, 8)
     for c in range(16):
         t, q = c // 4, c % 4
         cols = slice(c * 128, (c + 1) * 128)
+
+        def mod(k, at=24 * t + q):
+            return mods_ref[at + 4 * k : at + 4 * k + 1, :]
+
         gain = misc_ref[0:1, cols]
-        shift, scale = mods[t][q], 1.0 + mods[t][4 + q]
-        cshift, cscale = mods[t][8 + q], 1.0 + mods[t][12 + q]
-        gate_ref[:, cols] = jnp.broadcast_to(mods[t][16 + q], (8, 128))
+        shift, scale, cshift, cscale = mod(0), gain * (1.0 + mod(1)), mod(2), gain * (1.0 + mod(3))
+        gate_ref[:, cols] = jnp.broadcast_to(mod(4), (8, 128))
         for s in range(4):
-            h = blk_ref[s, :OWN, cols].astype(f32) * inv[s] * gain * scale + shift
-            h_ref[s * OWN : (s + 1) * OWN, cols] = h.astype(bf16)
-        halo = neighbours(cols) * inv_halo * gain * scale + shift
-        ctx = ctx_ref[:, cols].astype(f32) * inv_ctx * gain * cscale + cshift
-        h_ref[TOK:ROWS, cols] = jnp.concatenate([halo, ctx], axis=0).astype(bf16)
+            h = blocks[s][:OWN, cols].astype(f32) * inv[s] * scale + shift
+            h_ref[pl.ds(pl.multiple_of(origin[s] * OWN, OWN), OWN), cols] = h.astype(bf16)
+        edge = edge_ref[:, cols] * inv_edge * scale + shift
+        ctx = ctx_ref[:, cols].astype(f32) * inv_ctx * cscale + cshift
+        h_ref[TOK:ROWS, cols] = jnp.concatenate([edge, ctx], axis=0).astype(bf16)
     stores = [store(0, h_ref, h_hbm), store(1, gate_ref, gate_hbm)]
 
     p = projected(h_ref, core, own_s, other_s, slice(2 * STATE, 2 * STATE + 128))
     step = softplus(p[:TOK])
     ctx_dt = p[TOK + 8 :]
-    log_decay = -(misc_ref[4:5, 0:128] * step)
+    rate = misc_ref[4:5, 0:128] + pltpu.roll(misc_ref[4:8, 0:128], HEADS, 1)[1:2]
+    log_decay = -(rate * step)
     ri, ci = rows_of((TOK, TOK)), lanes((TOK, TOK))
     lower = jnp.where(ri >= ci, 1.0, 0.0).astype(f32)
     upper = jnp.where(ri <= ci, 1.0, 0.0).astype(f32)
@@ -331,7 +325,7 @@
 
 def output_kernel(
     place_ref, state_ref, gain_ref, c_ref, sr_ref, z_ref, y_hbm, own_hbm, other_hbm,
-    out_ref, ny_ref, y_ref, own_ref, other_ref, sems,
+    tile0_ref, tile1_ref, tile2_ref, tile3_ref, out_ref, ny_ref, y_ref, own_ref, other_ref, sems,
 ):
     loads = [
         pltpu.make_async_copy(src, dst, sems.at[i])
@@ -376,12 +370,15 @@
         out = jnp.dot(mine, own_ref[:, cols], preferred_element_type=f32)
         out = out + jnp.dot(theirs, other_ref[:, cols], preferred_element_type=f32)
         out_ref[:, cols] = out.astype(bf16)
-
-
-def sum_kernel(tile_ref, gate_ref, out_hbm, out_ref, sem):
-    total = tile_ref[0].astype(f32)
-    for t in range(1, 4):
-        total = total + tile_ref[t].astype(f32)
+    tp = place_ref[2]
+    for s, tile in enumerate((tile0_ref, tile1_ref, tile2_ref, tile3_ref)):
+        tile[...] = out_ref[pl.ds(pl.multiple_of(lax.rem(tp + s, 4) * OWN, OWN), OWN), :]
+
+
+def sum_kernel(tile0_ref, tile1_ref, tile2_ref, tile3_ref, gate_ref, out_hbm, out_ref, sem):
+    total = tile0_ref[...].astype(f32)
+    for tile in (tile1_ref, tile2_ref, tile3_ref):
+        total = total + tile[...].astype(f32)
     out_ref[...] = (gate_ref[0:1, :] * total).astype(bf16)
     copy = pltpu.make_async_copy(out_ref, out_hbm, sem)
     copy.start()
@@ -406,14 +403,7 @@
 
 
 def pack_call(*args):
-    return call(
-        pack_kernel,
-        pltpu.HBM((4, OWN + 8, D), bf16),
-        3,
-        (),
-        [pltpu.VMEM((8, D), bf16), pltpu.SemaphoreType.DMA((8,))],
-        hbm_out=True,
-    )(*args)
+    return call(pack_kernel, jax.ShapeDtypeStruct((OWN + 8, D), bf16), 3, ())(*args)
 
 
 def project_call(*args):
@@ -424,11 +414,13 @@
     return call(
         project_kernel,
         [pltpu.HBM(*o) for o in outs],
-        8,
+        11,
         (0,),
         [
             *(pltpu.VMEM(*o) for o in outs),
             pltpu.VMEM((TOK + 16, INNER), f32),
+            pltpu.VMEM((96, 128), f32),
+            pltpu.VMEM((8, D), f32),
             pltpu.SemaphoreType.DMA((5,)),
         ],
         hbm_out=True,
@@ -462,10 +454,11 @@
 def output_call(*args):
     return call(
         output_kernel,
-        jax.ShapeDtypeStruct((TOK, D), bf16),
+        [jax.ShapeDtypeStruct((OWN, D), bf16)] * 4,
         9,
         (0,),
         [
+            pltpu.VMEM((TOK, D), bf16),
             pltpu.VMEM((TOK, INNER), bf16),
             pltpu.VMEM((TOK, INNER), f32),
             pltpu.VMEM((INNER // 2, D), bf16),
@@ -480,7 +473,7 @@
     return call(
         sum_kernel,
         pltpu.HBM((OWN, D), bf16),
-        2,
+        5,
         (),
         [pltpu.VMEM((OWN, D), bf16), pltpu.SemaphoreType.DMA(())],
         hbm_out=True,
@@ -495,6 +488,10 @@
     return lax.all_to_all(x, axes, 0, 0, tiled=True)
 
 
+def turned(by):
+    return [(i, (i + by) % 4) for i in range(4)]
+
+
 def sent_to_all(x, peers, axes):
     return exchanged(jnp.broadcast_to(x[None], (peers, *x.shape)), axes)
 
@@ -506,15 +503,16 @@
 
 
 def packed_vectors(norm_gain, conv_x, conv_b, conv_c, decay_rate):
-    taps = jnp.concatenate([conv_x, conv_b, conv_c], axis=1).astype(f32)
-    rates = decay_rate.reshape(1, 2 * HEADS)
-    return jnp.concatenate(
-        [
-            norm_gain.astype(f32)[None],
-            jnp.pad(taps, ((0, 0), (0, D - XBC))),
-            jnp.pad(rates, ((0, 3), (0, D - 2 * HEADS))),
-        ],
-        axis=0,
+    def placed(v, row, col):
+        v = v.astype(f32)
+        return jnp.pad(v, ((row, 8 - row - v.shape[0]), (col, D - col - v.shape[1])))
+
+    return (
+        placed(norm_gain[None], 0, 0)
+        + placed(conv_x, 1, 0)
+        + placed(conv_b, 1, INNER)
+        + placed(conv_c, 1, XB)
+        + placed(decay_rate, 4, 0)
     )
 
 
@@ -532,7 +530,7 @@
     at = lax.axis_index(SP)
     core = lax.axis_index("dp")
     tp = lax.axis_index("tp")
-    place = jnp.stack([core, at]).astype(jnp.int32)
+    place = jnp.stack([core, at, tp]).astype(jnp.int32)
     row_count = mod_weight.shape[1]
 
     rows = latent[0]
@@ -551,8 +549,9 @@
     part = sent_to_all(part, 8, "sp_0")
     part = jnp.sum(part, axis=0)
     part = sent_to_all(part, 8, "sp_1")
-    packed = pack_call(part, rows, halo)
-    block = exchanged(packed, "tp")
+    blocks = [pack_call(part, rows, halo)]
+    for s in (1, 2, 3):
+        blocks.append(lax.ppermute(blocks[0], "tp", turned(s)))
 
     small = small_weights(w_b, w_c, w_dt)
     other_x = swapped(w_x)
@@ -565,7 +564,7 @@
     own_rates = lax.dynamic_slice_in_dim(decay_rate, at // 8, 1, 1)[:, 0]
 
     send, h, xb, sr, gate = project_call(
-        place, block, context[0], misc, w_x, other_x, small, other_small
+        place, *blocks, context[0], misc, w_x, other_x, small, other_small
     )
     received = exchanged(send, SP)
     y_in, c_in, z_in = inside_call(
@@ -573,11 +572,13 @@
     )
     entering = owner_call(own_rates, received, own_taps)
     states = exchanged(entering, SP)
-    partial = output_call(
+    tiles = output_call(
         place, states, out_gain[None], c_in, sr, z_in, y_in, w_out, other_out
     )
-    tiles = exchanged(partial.reshape(4, OWN, D), "tp")
-    return sum_call(tiles, gate)[None]
+    received = [tiles[0]]
+    for s in (1, 2, 3):
+        received.append(lax.ppermute(tiles[s], "tp", turned(s)))
+    return sum_call(*received, gate)[None]
 
 
 def solution(mesh):

time: 117 us -> 123 us (1.051)
  the two profiles are of different devices: /device:TPU:8 before, /device:TPU:6 now
where the time goes in v6:
time: 123 us; the launch traced here: 122 us
  starting transfers between devices  62.1 us (50%)
  waiting for transfers between devices  39.4 us (32%)
  Pallas kernels  12.6 us (10%)
  local copies, waits for them, and re-layouts  4.45 us (4%)
  other arithmetic  2.5 us (2%)
    all_to_all x4, starting transfers between devices, exchanged(): return lax.all_to_all(x, axes, 0, 0, tiled=True)  31.3 us
    all_to_all x4, waiting for transfers between devices, exchanged(): return lax.all_to_all(x, axes, 0, 0, tiled=True)  24 us
    ppermute x3, starting transfers between devices, shards(): received.append(lax.ppermute(tiles[s], 'tp', turned(s)))  9.52 us
    ppermute x4, starting transfers between devices, swapped(): return lax.ppermute(x, 'dp', [(0, 1), (1, 0)])  8.78 us
    ppermute x3, starting transfers between devices, shards(): blocks.append(lax.ppermute(blocks[0], 'tp', turned(s)))  8.63 us
    ppermute x3, waiting for transfers between devices, shards(): received.append(lax.ppermute(tiles[s], 'tp', turned(s)))  5.88 us
    ppermute x3, waiting for transfers between devices, shards(): blocks.append(lax.ppermute(blocks[0], 'tp', turned(s)))  5.68 us
    pallas_call x1, Pallas kernels, project_call(): call(project_kernel, [pltpu.HBM(*o) for o in outs], 11, (0,), [*(pltpu.VM...  4.27 us
  transfers between devices with their start and end apart: 15, of which 8 were waited for; matrix products, arithmetic and copies ran while one was open for 2% of the time, Pallas kernels for 4%

profile of v6, /device:TPU:6, one launch (start us, length us, event | category | flops | bytes accessed | tf_op | source)
XLA Modules:
  0.0 121.7 jit_solution(17722137139462202291)
XLA Ops:
  0.0 0.8 fusion.4
  0.8 0.7 fusion.6
  1.5 0.2 fusion.13
  1.8 0.6 broadcast_in_dim.21
  2.4 10.3 %all-to-all-start = ((f32[8,20,128]{2,1,0:T(8,128)}), f32[8,20,128]{2,1,0:T(8,128)S(1)}, u32[]{:S(2)}, u32[]{:S(2)}) async-start(f32[8,20,128]{2,1,0:T(8,128)} %broadcast_in_dim.21), calls=%async_computation | async-start | bytes 196608 | tf_op jit(solution)/shard_map/all_to_all | solution.py:488
  12.8 1.9 %collective-permute-start.4 = (bf16[1024,512]{1,0:T(8,128)(2,1)}, bf16[1024,512]{1,0:T(8,128)(2,1)}, u32[]{:S(2)}, u32[]{:S(2)}) collective-permute-start(bf16[1024,512]{1,0:T(8,128)(2,1)} %own_x.1), channel_id=1, source_target_pairs={{0,1},{1,0},{2,3},{3,2},{4,5},{5,4},{6,7},{7,6},{8,9},{9,8},{10,11... | collective-permute-start | bytes 3145736 | tf_op jit(solution)/shard_map/ppermute | solution.py:484
  14.7 0.7 slice_bitcast_fusion.1
  15.4 0.2 copy.23
  15.6 0.0 copy-start.6
  15.6 0.0 copy-start.15
  15.7 0.0 copy-start.1
  15.7 0.1 fusion.1.own_s
  15.8 2.5 %collective-permute-start.5 = (bf16[1024,384]{1,0:T(8,128)(2,1)S(1)}, bf16[1024,384]{1,0:T(8,128)(2,1)S(1)}, u32[]{:S(2)}, u32[]{:S(2)}) collective-permute-start(bf16[1024,384]{1,0:T(8,128)(2,1)S(1)} %fusion.1.own_s), channel_id=1, source_target_pairs={{0,1},{1,0},{2,3},{3,2},{4,5},{5,4},{6,7},{7,6},{8,9},{9,8},{10,11... | collective-permute-start | bytes 2359304 | tf_op jit(solution)/shard_map/ppermute | solution.py:484
  18.4 3.1 %all-to-all-done = f32[8,20,128]{2,1,0:T(8,128)S(1)} async-done(((f32[8,20,128]{2,1,0:T(8,128)}), f32[8,20,128]{2,1,0:T(8,128)S(1)}, u32[]{:S(2)}, u32[]{:S(2)}) %all-to-all-start) | async-done | bytes 81952 | tf_op jit(solution)/shard_map/all_to_all | solution.py:488
  21.5 0.6 broadcast_in_dim.22
  22.2 7.1 %all-to-all-start.1 = ((f32[8,20,128]{2,1,0:T(8,128)}), f32[8,20,128]{2,1,0:T(8,128)S(1)}, u32[]{:S(2)}, u32[]{:S(2)}) async-start(f32[8,20,128]{2,1,0:T(8,128)} %broadcast_in_dim.22), calls=%async_computation.1 | async-start | bytes 196608 | tf_op jit(solution)/shard_map/all_to_all | solution.py:488
  29.3 3.8 %collective-permute-start = (bf16[1,2048]{1,0:T(2,128)(2,1)S(1)}, bf16[1,2048]{1,0:T(2,128)(2,1)S(1)}, u32[]{:S(2)}, u32[]{:S(2)}) collective-permute-start(bf16[1,2048]{1,0:T(2,128)(2,1)S(1)} %fusion.5), channel_id=1, source_target_pairs={{6,8},{14,16},{22,24},{30,32},{38,40},{46,48},{54,56},{62,64},{70,... | collective-permute-start | bytes 12296 | tf_op jit(solution)/shard_map/ppermute | solution.py:540
  33.2 3.8 %collective-permute-done.halo_ref = bf16[1,2048]{1,0:T(2,128)(2,1)S(1)} collective-permute-done((bf16[1,2048]{1,0:T(2,128)(2,1)S(1)}, bf16[1,2048]{1,0:T(2,128)(2,1)S(1)}, u32[]{:S(2)}, u32[]{:S(2)}) %collective-permute-start) | collective-permute-done | bytes 4128 | tf_op jit(solution)/shard_map/ppermute | solution.py:540
  36.9 1.0 all-to-all-done.1.part_ref
  38.0 2.4 %collective-permute-start.1 = (bf16[40,2048]{1,0:T(8,128)(2,1)S(1)}, bf16[40,2048]{1,0:T(8,128)(2,1)S(1)}, u32[]{:S(2)}, u32[]{:S(2)}) collective-permute-start(bf16[40,2048]{1,0:T(8,128)(2,1)S(1)} %shard_map.163.blk0_ref), channel_id=1, source_target_pairs={{0,2},{2,4},{4,6},{6,0},{1,3},{3,5},{5,7},{7,1},{8,10},{10,12},{12... | collective-permute-start | bytes 491528 | tf_op jit(solution)/shard_map/ppermute | solution.py:554
  40.4 4.3 %collective-permute-start.2 = (bf16[40,2048]{1,0:T(8,128)(2,1)S(1)}, bf16[40,2048]{1,0:T(8,128)(2,1)S(1)}, u32[]{:S(2)}, u32[]{:S(2)}) collective-permute-start(bf16[40,2048]{1,0:T(8,128)(2,1)S(1)} %shard_map.163.blk0_ref), channel_id=1, source_target_pairs={{0,4},{2,6},{4,0},{6,2},{1,5},{3,7},{5,1},{7,3},{8,12},{10,14},{12... | collective-permute-start | bytes 491528 | tf_op jit(solution)/shard_map/ppermute | solution.py:554
  44.8 1.9 %collective-permute-start.3 = (bf16[40,2048]{1,0:T(8,128)(2,1)S(1)}, bf16[40,2048]{1,0:T(8,128)(2,1)S(1)}, u32[]{:S(2)}, u32[]{:S(2)}) collective-permute-start(bf16[40,2048]{1,0:T(8,128)(2,1)S(1)} %shard_map.163.blk0_ref), channel_id=1, source_target_pairs={{0,6},{2,0},{4,2},{6,4},{1,7},{3,1},{5,3},{7,5},{8,14},{10,8},{12,... | collective-permute-start | bytes 491528 | tf_op jit(solution)/shard_map/ppermute | solution.py:554
  46.7 0.7 pad_add_fusion.misc_ref
  47.4 0.1 pad_add_fusion.1.place_ref
  47.5 2.9 %collective-permute-done.2.blk2_ref = bf16[40,2048]{1,0:T(8,128)(2,1)S(1)} collective-permute-done((bf16[40,2048]{1,0:T(8,128)(2,1)S(1)}, bf16[40,2048]{1,0:T(8,128)(2,1)S(1)}, u32[]{:S(2)}, u32[]{:S(2)}) %collective-permute-start.2) | collective-permute-done | bytes 163872 | tf_op jit(solution)/shard_map/ppermute | solution.py:554
  50.5 2.7 %collective-permute-done.3.blk3_ref = bf16[40,2048]{1,0:T(8,128)(2,1)S(1)} collective-permute-done((bf16[40,2048]{1,0:T(8,128)(2,1)S(1)}, bf16[40,2048]{1,0:T(8,128)(2,1)S(1)}, u32[]{:S(2)}, u32[]{:S(2)}) %collective-permute-start.3) | collective-permute-done | bytes 163872 | tf_op jit(solution)/shard_map/ppermute | solution.py:554
  53.2 4.3 %shard_map.164 = (bf16[64,24,128]{2,1,0:T(8,128)(2,1)}, bf16[144,2048]{1,0:T(8,128)(2,1)}, bf16[128,640]{1,0:T(8,128)(2,1)}, f32[128,256]{1,0:T(8,128)}, f32[8,2048]{1,0:T(8,128)}) custom-call(s32[3]{0:T(128)S(1)} %pad_add_fusion.1.place_ref, bf16[40,2048]{1,0:T(8,128)(2,1)S(1)} %shard_map.163.blk0_ref, ...), custom_call_target="tpu_custom_call" | custom-call | flops 100000000 | bytes 1048576 | tf_op jit(solution)/shard_map/pallas_call | solution.py:414
  57.6 9.3 %all-to-all-start.2 = ((bf16[64,24,128]{2,1,0:T(8,128)(2,1)}), bf16[64,24,128]{2,1,0:T(8,128)(2,1)S(1)}, u32[]{:S(2)}, u32[]{:S(2)}) async-start(bf16[64,24,128]{2,1,0:T(8,128)(2,1)} %get-tuple-element.17), calls=%async_computation.2 | async-start | bytes 786432 | tf_op jit(solution)/shard_map/all_to_all | solution.py:488
  66.9 1.9 %collective-permute-start.6 = (bf16[1024,512]{1,0:T(8,128)(2,1)}, bf16[1024,512]{1,0:T(8,128)(2,1)}, u32[]{:S(2)}, u32[]{:S(2)}) collective-permute-start(bf16[1024,512]{1,0:T(8,128)(2,1)} %own_z.1), channel_id=1, source_target_pairs={{0,1},{1,0},{2,3},{3,2},{4,5},{5,4},{6,7},{7,6},{8,9},{9,8},{10,11... | collective-permute-start | bytes 3145736 | tf_op jit(solution)/shard_map/ppermute | solution.py:484
  68.8 2.4 %collective-permute-start.7 = (bf16[256,2048]{1,0:T(8,128)(2,1)}, bf16[256,2048]{1,0:T(8,128)(2,1)}, u32[]{:S(2)}, u32[]{:S(2)}) collective-permute-start(bf16[256,2048]{1,0:T(8,128)(2,1)} %own_hbm.1), channel_id=1, source_target_pairs={{0,1},{1,0},{2,3},{3,2},{4,5},{5,4},{6,7},{7,6},{8,9},{9,8},{10,11... | collective-permute-start | bytes 3145736 | tf_op jit(solution)/shard_map/ppermute | solution.py:484
  71.3 0.2 fusion.9.rate_ref
  71.5 0.1 constant_dynamic-slice_fusion
  71.5 0.1 constant_dynamic-slice_fusion.1
  71.6 0.1 fusion.11.tap_ref
  71.7 10.3 %all-to-all-done.2.recv_ref = bf16[64,24,128]{2,1,0:T(8,128)(2,1)S(1)} async-done(((bf16[64,24,128]{2,1,0:T(8,128)(2,1)}), bf16[64,24,128]{2,1,0:T(8,128)(2,1)S(1)}, u32[]{:S(2)}, u32[]{:S(2)}) %all-to-all-start.2) | async-done | bytes 393248 | tf_op jit(solution)/shard_map/all_to_all | solution.py:488
  81.9 2.6 %shard_map.165 = bf16[64,16,128]{2,1,0:T(8,128)(2,1)} custom-call(f32[2]{0:T(128)S(1)} %fusion.9.rate_ref, bf16[64,24,128]{2,1,0:T(8,128)(2,1)S(1)} %all-to-all-done.2.recv_ref, f32[3,128]{1,0:T(4,128)S(1)} %fusion.11.tap_ref), custom_call_target="tpu_custom_call" | custom-call | flops 100000000 | bytes 1048576 | tf_op jit(solution)/shard_map/pallas_call | solution.py:445
  84.6 4.6 %all-to-all-start.3 = ((bf16[64,16,128]{2,1,0:T(8,128)(2,1)}), bf16[64,16,128]{2,1,0:T(8,128)(2,1)S(1)}, u32[]{:S(2)}, u32[]{:S(2)}) async-start(bf16[64,16,128]{2,1,0:T(8,128)(2,1)} %shard_map.165), calls=%async_computation.3 | async-start | bytes 524288 | tf_op jit(solution)/shard_map/all_to_all | solution.py:488
  89.2 1.1 copy-done.3
  90.3 2.2 %shard_map.166 = (f32[128,512]{1,0:T(8,128)S(1)}, bf16[128,128]{1,0:T(8,128)(2,1)S(1)}, bf16[128,512]{1,0:T(8,128)(2,1)S(1)}) custom-call(s32[3]{0:T(128)S(1)} %pad_add_fusion.1.place_ref, bf16[144,2048]{1,0:T(8,128)(2,1)S(1)} %copy-done.3, bf16[1024,512]{1,0:T(8,128)(2,1)S(1)} %copy-done.2, bf16[1024,512]{1,0:T(8,128)(2,1)} %collective-permute-done.6.other_z, ...), custom_call_target="tpu_custom_call" | custom-call | flops 100000000 | bytes 1048576 | tf_op jit(solution)/shard_map/pallas_call | solution.py:431
  92.5 0.7 copy-done.5
  93.2 9.6 %all-to-all-done.3.state_ref = bf16[64,16,128]{2,1,0:T(8,128)(2,1)S(1)} async-done(((bf16[64,16,128]{2,1,0:T(8,128)(2,1)}), bf16[64,16,128]{2,1,0:T(8,128)(2,1)S(1)}, u32[]{:S(2)}, u32[]{:S(2)}) %all-to-all-start.3) | async-done | bytes 262176 | tf_op jit(solution)/shard_map/all_to_all | solution.py:488
  102.8 2.7 %shard_map.167 = (bf16[32,2048]{1,0:T(8,128)(2,1)S(1)}, bf16[32,2048]{1,0:T(8,128)(2,1)S(1)}, bf16[32,2048]{1,0:T(8,128)(2,1)S(1)}, bf16[32,2048]{1,0:T(8,128)(2,1)S(1)}) custom-call(s32[3]{0:T(128)S(1)} %pad_add_fusion.1.place_ref, bf16[64,16,128]{2,1,0:T(8,128)(2,1)S(1)} %all-to-all-done.3.state_ref, bf16[1,512]{1,0:T(2,128)(2,1)S(1)} %broadcast_in_dim.23.gain_ref, ...), custom_call_target="tpu_custom_call" | custom-call | flops 100000000 | bytes 1048576 | tf_op jit(solution)/shard_map/pallas_call | solution.py:455
  105.5 1.9 %collective-permute-start.10 = (bf16[32,2048]{1,0:T(8,128)(2,1)S(1)}, bf16[32,2048]{1,0:T(8,128)(2,1)S(1)}, u32[]{:S(2)}, u32[]{:S(2)}) collective-permute-start(bf16[32,2048]{1,0:T(8,128)(2,1)S(1)} %get-tuple-element.27), channel_id=1, source_target_pairs={{0,6},{2,0},{4,2},{6,4},{1,7},{3,1},{5,3},{7,5},{8,14},{10,8},{12,... | collective-permute-start | bytes 393224 | tf_op jit(solution)/shard_map/ppermute | solution.py:580
  107.5 5.1 %collective-permute-start.8 = (bf16[32,2048]{1,0:T(8,128)(2,1)S(1)}, bf16[32,2048]{1,0:T(8,128)(2,1)S(1)}, u32[]{:S(2)}, u32[]{:S(2)}) collective-permute-start(bf16[32,2048]{1,0:T(8,128)(2,1)S(1)} %get-tuple-element.25), channel_id=1, source_target_pairs={{0,2},{2,4},{4,6},{6,0},{1,3},{3,5},{5,7},{7,1},{8,10},{10,12},{12... | collective-permute-start | bytes 393224 | tf_op jit(solution)/shard_map/ppermute | solution.py:580
  112.6 2.5 %collective-permute-start.9 = (bf16[32,2048]{1,0:T(8,128)(2,1)S(1)}, bf16[32,2048]{1,0:T(8,128)(2,1)S(1)}, u32[]{:S(2)}, u32[]{:S(2)}) collective-permute-start(bf16[32,2048]{1,0:T(8,128)(2,1)S(1)} %get-tuple-element.26), channel_id=1, source_target_pairs={{0,4},{2,6},{4,0},{6,2},{1,5},{3,7},{5,1},{7,3},{8,12},{10,14},{12... | collective-permute-start | bytes 393224 | tf_op jit(solution)/shard_map/ppermute | solution.py:580
  115.1 0.0 collective-permute-done.8.tile1_ref
  115.1 5.9 %collective-permute-done.9.tile2_ref = bf16[32,2048]{1,0:T(8,128)(2,1)S(1)} collective-permute-done((bf16[32,2048]{1,0:T(8,128)(2,1)S(1)}, bf16[32,2048]{1,0:T(8,128)(2,1)S(1)}, u32[]{:S(2)}, u32[]{:S(2)}) %collective-permute-start.9) | collective-permute-done | bytes 131104 | tf_op jit(solution)/shard_map/ppermute | solution.py:580
  121.0 0.7 shard_map.168
  (45 shorter events, 0.2 us)
Async XLA Ops:
  0.0 1.5 %copy-start = (bf16[3,32,512]{2,1,0:T(8,128)(2,1)S(1)}, bf16[3,32,512]{2,1,0:T(8,128)(2,1)}, u32[]{:S(2)}) copy-start(bf16[3,32,512]{2,1,0:T(8,128)(2,1)} %param.21) | copy-start | bytes 294916
  0.0 15.6 %copy-start.11 = (bf16[1024,128]{1,0:T(8,128)(2,1)S(1)}, bf16[1024,128]{1,0:T(8,128)(2,1)}, u32[]{:S(2)}) copy-start(bf16[1024,128]{1,0:T(8,128)(2,1)} %param.24) | copy-start | bytes 786436
  0.0 15.6 %copy-start.10 = (bf16[1024,128]{1,0:T(8,128)(2,1)S(1)}, bf16[1024,128]{1,0:T(8,128)(2,1)}, u32[]{:S(2)}) copy-start(bf16[1024,128]{1,0:T(8,128)(2,1)} %param.25) | copy-start | bytes 786436
  2.4 19.0 %all-to-all-start = ((f32[8,20,128]{2,1,0:T(8,128)}), f32[8,20,128]{2,1,0:T(8,128)S(1)}, u32[]{:S(2)}, u32[]{:S(2)}) async-start(f32[8,20,128]{2,1,0:T(8,128)} %broadcast_in_dim.21), calls=%async_computation | async-start | bytes 196608 | tf_op jit(solution)/shard_map/all_to_all | solution.py:488
  12.8 40.4 %collective-permute-start.4 = (bf16[1024,512]{1,0:T(8,128)(2,1)}, bf16[1024,512]{1,0:T(8,128)(2,1)}, u32[]{:S(2)}, u32[]{:S(2)}) collective-permute-start(bf16[1024,512]{1,0:T(8,128)(2,1)} %own_x.1), channel_id=1, source_target_pairs={{0,1},{1,0},{2,3},{3,2},{4,5},{5,4},{6,7},{7,6},{8,9},{9,8},{10,11... | collective-permute-start | bytes 3145736 | tf_op jit(solution)/shard_map/ppermute | solution.py:484
  15.6 13.6 %copy-start.6 = (bf16[1,32,2048]{2,1,0:T(8,128)(2,1)S(1)}, bf16[1,32,2048]{2,1,0:T(8,128)(2,1)}, u32[]{:S(2)}) copy-start(bf16[1,32,2048]{2,1,0:T(8,128)(2,1)} %param.17) | copy-start | bytes 393220
  15.6 17.5 %copy-start.15 = (bf16[2048]{0:T(1024)(128)(2,1)S(1)}, bf16[2048]{0:T(1024)(128)(2,1)}, u32[]{:S(2)}) copy-start(bf16[2048]{0:T(1024)(128)(2,1)} %param.22) | copy-start | bytes 12292
  15.7 31.0 %copy-start.12 = (bf16[3,512]{1,0:T(4,128)(2,1)S(1)}, bf16[3,512]{1,0:T(4,128)(2,1)}, u32[]{:S(2)}) copy-start(bf16[3,512]{1,0:T(4,128)(2,1)} %param.28) | copy-start | bytes 9220
  15.7 31.0 %copy-start.13 = (f32[2,8]{1,0:T(2,128)S(1)}, f32[2,8]{1,0:T(2,128)}, u32[]{:S(2)}) copy-start(f32[2,8]{1,0:T(2,128)} %param.31) | copy-start | bytes 196
  15.7 37.5 %copy-start.1 = (bf16[1024,512]{1,0:T(8,128)(2,1)S(1)}, bf16[1024,512]{1,0:T(8,128)(2,1)}, u32[]{:S(2)}) copy-start(bf16[1024,512]{1,0:T(8,128)(2,1)} %own_x.1) | copy-start | bytes 3145732
  15.7 37.5 %copy-start.9 = (bf16[1,8,2048]{2,1,0:T(8,128)(2,1)S(1)}, bf16[1,8,2048]{2,1,0:T(8,128)(2,1)}, u32[]{:S(2)}) copy-start(bf16[1,8,2048]{2,1,0:T(8,128)(2,1)} %param.19) | copy-start | bytes 98308
  15.8 37.4 %collective-permute-start.5 = (bf16[1024,384]{1,0:T(8,128)(2,1)S(1)}, bf16[1024,384]{1,0:T(8,128)(2,1)S(1)}, u32[]{:S(2)}, u32[]{:S(2)}) collective-permute-start(bf16[1024,384]{1,0:T(8,128)(2,1)S(1)} %fusion.1.own_s), channel_id=1, source_target_pairs={{0,1},{1,0},{2,3},{3,2},{4,5},{5,4},{6,7},{7,6},{8,9},{9,8},{10,11... | collective-permute-start | bytes 2359304 | tf_op jit(solution)/shard_map/ppermute | solution.py:484
  22.2 15.8 %all-to-all-start.1 = ((f32[8,20,128]{2,1,0:T(8,128)}), f32[8,20,128]{2,1,0:T(8,128)S(1)}, u32[]{:S(2)}, u32[]{:S(2)}) async-start(f32[8,20,128]{2,1,0:T(8,128)} %broadcast_in_dim.22), calls=%async_computation.1 | async-start | bytes 196608 | tf_op jit(solution)/shard_map/all_to_all | solution.py:488
  29.3 7.7 %collective-permute-start = (bf16[1,2048]{1,0:T(2,128)(2,1)S(1)}, bf16[1,2048]{1,0:T(2,128)(2,1)S(1)}, u32[]{:S(2)}, u32[]{:S(2)}) collective-permute-start(bf16[1,2048]{1,0:T(2,128)(2,1)S(1)} %fusion.5), channel_id=1, source_target_pairs={{6,8},{14,16},{22,24},{30,32},{38,40},{46,48},{54,56},{62,64},{70,... | collective-permute-start | bytes 12296 | tf_op jit(solution)/shard_map/ppermute | solution.py:540
  38.0 9.5 %collective-permute-start.1 = (bf16[40,2048]{1,0:T(8,128)(2,1)S(1)}, bf16[40,2048]{1,0:T(8,128)(2,1)S(1)}, u32[]{:S(2)}, u32[]{:S(2)}) collective-permute-start(bf16[40,2048]{1,0:T(8,128)(2,1)S(1)} %shard_map.163.blk0_ref), channel_id=1, source_target_pairs={{0,2},{2,4},{4,6},{6,0},{1,3},{3,5},{5,7},{7,1},{8,10},{10,12},{12... | collective-permute-start | bytes 491528 | tf_op jit(solution)/shard_map/ppermute | solution.py:554
  40.4 10.0 %collective-permute-start.2 = (bf16[40,2048]{1,0:T(8,128)(2,1)S(1)}, bf16[40,2048]{1,0:T(8,128)(2,1)S(1)}, u32[]{:S(2)}, u32[]{:S(2)}) collective-permute-start(bf16[40,2048]{1,0:T(8,128)(2,1)S(1)} %shard_map.163.blk0_ref), channel_id=1, source_target_pairs={{0,4},{2,6},{4,0},{6,2},{1,5},{3,7},{5,1},{7,3},{8,12},{10,14},{12... | collective-permute-start | bytes 491528 | tf_op jit(solution)/shard_map/ppermute | solution.py:554
  44.8 8.4 %collective-permute-start.3 = (bf16[40,2048]{1,0:T(8,128)(2,1)S(1)}, bf16[40,2048]{1,0:T(8,128)(2,1)S(1)}, u32[]{:S(2)}, u32[]{:S(2)}) collective-permute-start(bf16[40,2048]{1,0:T(8,128)(2,1)S(1)} %shard_map.163.blk0_ref), channel_id=1, source_target_pairs={{0,6},{2,0},{4,2},{6,4},{1,7},{3,1},{5,3},{7,5},{8,14},{10,8},{12,... | collective-permute-start | bytes 491528 | tf_op jit(solution)/shard_map/ppermute | solution.py:554
  53.2 18.2 %copy-start.14 = (bf16[3,128]{1,0:T(4,128)(2,1)S(1)}, bf16[3,128]{1,0:T(4,128)(2,1)}, u32[]{:S(2)}) copy-start(bf16[3,128]{1,0:T(4,128)(2,1)} %param.29) | copy-start | bytes 2308
  57.5 31.7 %copy-start.16 = (bf16[512]{0:T(512)(128)(2,1)S(1)}, bf16[512]{0:T(512)(128)(2,1)}, u32[]{:S(2)}) copy-start(bf16[512]{0:T(512)(128)(2,1)} %param.32) | copy-start | bytes 3076
  57.5 31.7 %copy-start.2 = (bf16[1024,512]{1,0:T(8,128)(2,1)S(1)}, bf16[1024,512]{1,0:T(8,128)(2,1)}, u32[]{:S(2)}) copy-start(bf16[1024,512]{1,0:T(8,128)(2,1)} %own_z.1) | copy-start | bytes 3145732
  57.5 31.7 %copy-start.4 = (f32[128,256]{1,0:T(8,128)S(1)}, f32[128,256]{1,0:T(8,128)}, u32[]{:S(2)}) copy-start(f32[128,256]{1,0:T(8,128)} %get-tuple-element.20.sr_ref) | copy-start | bytes 393220
  57.5 31.7 %copy-start.7 = (bf16[128,640]{1,0:T(8,128)(2,1)S(1)}, bf16[128,640]{1,0:T(8,128)(2,1)}, u32[]{:S(2)}) copy-start(bf16[128,640]{1,0:T(8,128)(2,1)} %get-tuple-element.19.xb_ref) | copy-start | bytes 491524
  57.6 24.4 %all-to-all-start.2 = ((bf16[64,24,128]{2,1,0:T(8,128)(2,1)}), bf16[64,24,128]{2,1,0:T(8,128)(2,1)S(1)}, u32[]{:S(2)}, u32[]{:S(2)}) async-start(bf16[64,24,128]{2,1,0:T(8,128)(2,1)} %get-tuple-element.17), calls=%async_computation.2 | async-start | bytes 786432 | tf_op jit(solution)/shard_map/all_to_all | solution.py:488
  66.9 22.3 %collective-permute-start.6 = (bf16[1024,512]{1,0:T(8,128)(2,1)}, bf16[1024,512]{1,0:T(8,128)(2,1)}, u32[]{:S(2)}, u32[]{:S(2)}) collective-permute-start(bf16[1024,512]{1,0:T(8,128)(2,1)} %own_z.1), channel_id=1, source_target_pairs={{0,1},{1,0},{2,3},{3,2},{4,5},{5,4},{6,7},{7,6},{8,9},{9,8},{10,11... | collective-permute-start | bytes 3145736 | tf_op jit(solution)/shard_map/ppermute | solution.py:484
  68.8 24.4 %collective-permute-start.7 = (bf16[256,2048]{1,0:T(8,128)(2,1)}, bf16[256,2048]{1,0:T(8,128)(2,1)}, u32[]{:S(2)}, u32[]{:S(2)}) collective-permute-start(bf16[256,2048]{1,0:T(8,128)(2,1)} %own_hbm.1), channel_id=1, source_target_pairs={{0,1},{1,0},{2,3},{3,2},{4,5},{5,4},{6,7},{7,6},{8,9},{9,8},{10,11... | collective-permute-start | bytes 3145736 | tf_op jit(solution)/shard_map/ppermute | solution.py:484
  84.6 18.3 %all-to-all-start.3 = ((bf16[64,16,128]{2,1,0:T(8,128)(2,1)}), bf16[64,16,128]{2,1,0:T(8,128)(2,1)S(1)}, u32[]{:S(2)}, u32[]{:S(2)}) async-start(bf16[64,16,128]{2,1,0:T(8,128)(2,1)} %shard_map.165), calls=%async_computation.3 | async-start | bytes 524288 | tf_op jit(solution)/shard_map/all_to_all | solution.py:488
  89.2 1.1 copy-start.3
  92.5 0.7 copy-start.5
  102.8 18.1 %copy-start.8 = (f32[8,2048]{1,0:T(8,128)S(1)}, f32[8,2048]{1,0:T(8,128)}, u32[]{:S(2)}) copy-start(f32[8,2048]{1,0:T(8,128)} %get-tuple-element.28.gate_ref) | copy-start | bytes 196612
  105.5 9.5 %collective-permute-start.10 = (bf16[32,2048]{1,0:T(8,128)(2,1)S(1)}, bf16[32,2048]{1,0:T(8,128)(2,1)S(1)}, u32[]{:S(2)}, u32[]{:S(2)}) collective-permute-start(bf16[32,2048]{1,0:T(8,128)(2,1)S(1)} %get-tuple-element.27), channel_id=1, source_target_pairs={{0,6},{2,0},{4,2},{6,4},{1,7},{3,1},{5,3},{7,5},{8,14},{10,8},{12,... | collective-permute-start | bytes 393224 | tf_op jit(solution)/shard_map/ppermute | solution.py:580
  107.5 7.6 %collective-permute-start.8 = (bf16[32,2048]{1,0:T(8,128)(2,1)S(1)}, bf16[32,2048]{1,0:T(8,128)(2,1)S(1)}, u32[]{:S(2)}, u32[]{:S(2)}) collective-permute-start(bf16[32,2048]{1,0:T(8,128)(2,1)S(1)} %get-tuple-element.25), channel_id=1, source_target_pairs={{0,2},{2,4},{4,6},{6,0},{1,3},{3,5},{5,7},{7,1},{8,10},{10,12},{12... | collective-permute-start | bytes 393224 | tf_op jit(solution)/shard_map/ppermute | solution.py:580
  112.6 8.4 %collective-permute-start.9 = (bf16[32,2048]{1,0:T(8,128)(2,1)S(1)}, bf16[32,2048]{1,0:T(8,128)(2,1)S(1)}, u32[]{:S(2)}, u32[]{:S(2)}) collective-permute-start(bf16[32,2048]{1,0:T(8,128)(2,1)S(1)} %get-tuple-element.26), channel_id=1, source_target_pairs={{0,4},{2,6},{4,0},{6,2},{1,5},{3,7},{5,1},{7,3},{8,12},{10,14},{12... | collective-permute-start | bytes 393224 | tf_op jit(solution)/shard_map/ppermute | solution.py:580

commit v7 on v6

--- a/solution.py
+++ b/solution.py
@@ -164,9 +164,9 @@
         h_ref[TOK:ROWS, cols] = jnp.concatenate([edge, ctx], axis=0).astype(bf16)
     stores = [store(0, h_ref, h_hbm), store(1, gate_ref, gate_hbm)]
 
-    p = projected(h_ref, core, own_s, other_s, slice(2 * STATE, 2 * STATE + 128))
-    step = softplus(p[:TOK])
-    ctx_dt = p[TOK + 8 :]
+    both = projected(h_ref, core, own_s, other_s, slice(0, STATE + 128))
+    step = softplus(both[:TOK, STATE:])
+    ctx_dt = both[TOK + 8 :, STATE:]
     rate = misc_ref[4:5, 0:128] + pltpu.roll(misc_ref[4:8, 0:128], HEADS, 1)[1:2]
     log_decay = -(rate * step)
     ri, ci = rows_of((TOK, TOK)), lanes((TOK, TOK))
@@ -182,9 +182,8 @@
     to_end = jnp.exp(total - run)
 
     before_ok, after_ok = ends(at)
-    p = projected(h_ref, core, own_s, other_s, slice(0, STATE))
-    ctx_b = p[TOK + 8 :]
-    b_in = softened(p, misc_ref, INNER, conv_ref, before_ok, after_ok)
+    ctx_b = both[TOK + 8 :, :STATE]
+    b_in = softened(both[:, :STATE], misc_ref, INNER, conv_ref, before_ok, after_ok)
     xb_ref[:, INNER:] = b_in
     p = projected(h_ref, core, own_x, other_x, slice(0, INNER))
     ctx_x = p[TOK + 8 :]
@@ -231,7 +230,8 @@
         ):
             head = 2 * q + k
             send_ref[head * 8 : head * 8 + 8, 0:16, :] = state.astype(bf16).reshape(8, 16, 128)
-    stores.append(store(4, send_ref, send_hbm))
+        part = pl.ds(16 * q, 16)
+        stores.append(store(4 + q, send_ref.at[part], send_hbm.at[part]))
     for copy in stores:
         copy.wait()
 
@@ -242,7 +242,7 @@
 ):
     core, at = place_ref[0], place_ref[1]
     before_ok, after_ok = ends(at)
-    p = projected(h_ref, core, own_s, other_s, slice(STATE, 2 * STATE))
+    p = projected(h_ref, core, own_s, other_s, slice(STATE + 128, 2 * STATE + 128))
     c_in = softened(p, misc_ref, INNER + STATE, conv_ref, before_ok, after_ok)
     c_out_ref[...] = c_in
     z_ref[...] = projected(h_ref, core, own_z, other_z, slice(0, INNER))[:TOK].astype(bf16)
@@ -325,7 +325,7 @@
 
 def output_kernel(
     place_ref, state_ref, gain_ref, c_ref, sr_ref, z_ref, y_hbm, own_hbm, other_hbm,
-    tile0_ref, tile1_ref, tile2_ref, tile3_ref, out_ref, ny_ref, y_ref, own_ref, other_ref, sems,
+    out_ref, ny_ref, y_ref, own_ref, other_ref, sems,
 ):
     loads = [
         pltpu.make_async_copy(src, dst, sems.at[i])
@@ -370,15 +370,12 @@
         out = jnp.dot(mine, own_ref[:, cols], preferred_element_type=f32)
         out = out + jnp.dot(theirs, other_ref[:, cols], preferred_element_type=f32)
         out_ref[:, cols] = out.astype(bf16)
-    tp = place_ref[2]
-    for s, tile in enumerate((tile0_ref, tile1_ref, tile2_ref, tile3_ref)):
-        tile[...] = out_ref[pl.ds(pl.multiple_of(lax.rem(tp + s, 4) * OWN, OWN), OWN), :]
-
-
-def sum_kernel(tile0_ref, tile1_ref, tile2_ref, tile3_ref, gate_ref, out_hbm, out_ref, sem):
-    total = tile0_ref[...].astype(f32)
-    for tile in (tile1_ref, tile2_ref, tile3_ref):
-        total = total + tile[...].astype(f32)
+
+
+def sum_kernel(tile_ref, gate_ref, out_hbm, out_ref, sem):
+    total = tile_ref[0].astype(f32)
+    for t in range(1, 4):
+        total = total + tile_ref[t].astype(f32)
     out_ref[...] = (gate_ref[0:1, :] * total).astype(bf16)
     copy = pltpu.make_async_copy(out_ref, out_hbm, sem)
     copy.start()
@@ -421,7 +418,7 @@
             pltpu.VMEM((TOK + 16, INNER), f32),
             pltpu.VMEM((96, 128), f32),
             pltpu.VMEM((8, D), f32),
-            pltpu.SemaphoreType.DMA((5,)),
+            pltpu.SemaphoreType.DMA((8,)),
         ],
         hbm_out=True,
     )(*args)
@@ -454,11 +451,10 @@
 def output_call(*args):
     return call(
         output_kernel,
-        [jax.ShapeDtypeStruct((OWN, D), bf16)] * 4,
+        jax.ShapeDtypeStruct((TOK, D), bf16),
         9,
         (0,),
         [
-            pltpu.VMEM((TOK, D), bf16),
             pltpu.VMEM((TOK, INNER), bf16),
             pltpu.VMEM((TOK, INNER), f32),
             pltpu.VMEM((INNER // 2, D), bf16),
@@ -473,7 +469,7 @@
     return call(
         sum_kernel,
         pltpu.HBM((OWN, D), bf16),
-        5,
+        2,
         (),
         [pltpu.VMEM((OWN, D), bf16), pltpu.SemaphoreType.DMA(())],
         hbm_out=True,
@@ -499,7 +495,7 @@
 def small_weights(w_b, w_c, w_dt):
     steps = jnp.concatenate([w_dt[0], w_dt[1]], axis=1)
     steps = jnp.pad(steps, ((0, 0), (0, 128 - steps.shape[1])))
-    return jnp.concatenate([w_b, w_c, steps], axis=1)
+    return jnp.concatenate([w_b, steps, w_c], axis=1)
 
 
 def packed_vectors(norm_gain, conv_x, conv_b, conv_c, decay_rate):
@@ -572,13 +568,11 @@
     )
     entering = owner_call(own_rates, received, own_taps)
     states = exchanged(entering, SP)
-    tiles = output_call(
+    partial = output_call(
         place, states, out_gain[None], c_in, sr, z_in, y_in, w_out, other_out
     )
-    received = [tiles[0]]
-    for s in (1, 2, 3):
-        received.append(lax.ppermute(tiles[s], "tp", turned(s)))
-    return sum_call(*received, gate)[None]
+    tiles = exchanged(partial.reshape(4, OWN, D), "tp")
+    return sum_call(tiles, gate)[None]
 
 
 def solution(mesh):

time: 123 us -> 119 us (0.967)
  the two profiles are of different devices: /device:TPU:6 before, /device:TPU:8 now
where the time goes in v7:
time: 119 us; the launch traced here: 118 us
  starting transfers between devices  57.2 us (48%)
  waiting for transfers between devices  29.1 us (24%)
  Pallas kernels  12.4 us (10%)
  blocking collectives  11.2 us (9%)
  local copies, waits for them, and re-layouts  4.45 us (4%)
  other arithmetic  2.52 us (2%)
    all_to_all x4, starting transfers between devices, exchanged(): return lax.all_to_all(x, axes, 0, 0, tiled=True)  33.4 us
    all_to_all x4, waiting for transfers between devices, exchanged(): return lax.all_to_all(x, axes, 0, 0, tiled=True)  22.1 us
    all_to_all x1, blocking collectives, exchanged(): return lax.all_to_all(x, axes, 0, 0, tiled=True)  11.2 us
    ppermute x3, starting transfers between devices, shards(): blocks.append(lax.ppermute(blocks[0], 'tp', turned(s)))  10.9 us
    ppermute x4, starting transfers between devices, swapped(): return lax.ppermute(x, 'dp', [(0, 1), (1, 0)])  8.78 us
    pallas_call x1, Pallas kernels, project_call(): call(project_kernel, [pltpu.HBM(*o) for o in outs], 11, (0,), [*(pltpu.VM...  4.17 us
    ppermute x1, starting transfers between devices, shards(): halo = lax.ppermute(edge, ALL, pairs)  4.12 us
    ppermute x1, waiting for transfers between devices, shards(): halo = lax.ppermute(edge, ALL, pairs)  3.61 us
  transfers between devices with their start and end apart: 12, of which 5 were waited for; matrix products, arithmetic and copies ran while one was open for 2% of the time, Pallas kernels for 4%

profile of v7, /device:TPU:8, one launch (start us, length us, event | category | flops | bytes accessed | tf_op | source)
XLA Modules:
  0.0 117.6 jit_solution(2907895427975297036)
XLA Ops:
  0.0 0.8 fusion.6
  0.8 0.7 fusion.8
  1.5 0.2 fusion.15
  1.8 0.6 broadcast_in_dim.21
  2.4 10.3 %all-to-all-start = ((f32[8,20,128]{2,1,0:T(8,128)}), f32[8,20,128]{2,1,0:T(8,128)S(1)}, u32[]{:S(2)}, u32[]{:S(2)}) async-start(f32[8,20,128]{2,1,0:T(8,128)} %broadcast_in_dim.21), calls=%async_computation | async-start | bytes 196608 | tf_op jit(solution)/shard_map/all_to_all | solution.py:484
  12.8 1.9 %collective-permute-start.4 = (bf16[1024,512]{1,0:T(8,128)(2,1)}, bf16[1024,512]{1,0:T(8,128)(2,1)}, u32[]{:S(2)}, u32[]{:S(2)}) collective-permute-start(bf16[1024,512]{1,0:T(8,128)(2,1)} %own_x.1), channel_id=1, source_target_pairs={{0,1},{1,0},{2,3},{3,2},{4,5},{5,4},{6,7},{7,6},{8,9},{9,8},{10,11... | collective-permute-start | bytes 3145736 | tf_op jit(solution)/shard_map/ppermute | solution.py:480
  14.7 0.7 slice_bitcast_fusion.1
  15.4 0.2 copy.23
  15.6 0.0 copy-start.6
  15.6 0.0 copy-start.15
  15.7 0.0 copy-start.12
  15.7 0.0 copy-start.13
  15.7 0.0 copy-start.1
  15.7 0.0 copy-start.9
  15.7 0.1 fusion.3.own_s
  15.8 2.5 %collective-permute-start.5 = (bf16[1024,384]{1,0:T(8,128)(2,1)S(1)}, bf16[1024,384]{1,0:T(8,128)(2,1)S(1)}, u32[]{:S(2)}, u32[]{:S(2)}) collective-permute-start(bf16[1024,384]{1,0:T(8,128)(2,1)S(1)} %fusion.3.own_s), channel_id=1, source_target_pairs={{0,1},{1,0},{2,3},{3,2},{4,5},{5,4},{6,7},{7,6},{8,9},{9,8},{10,11... | collective-permute-start | bytes 2359304 | tf_op jit(solution)/shard_map/ppermute | solution.py:480
  18.4 3.1 %all-to-all-done = f32[8,20,128]{2,1,0:T(8,128)S(1)} async-done(((f32[8,20,128]{2,1,0:T(8,128)}), f32[8,20,128]{2,1,0:T(8,128)S(1)}, u32[]{:S(2)}, u32[]{:S(2)}) %all-to-all-start) | async-done | bytes 81952 | tf_op jit(solution)/shard_map/all_to_all | solution.py:484
  21.5 0.6 broadcast_in_dim.22
  22.2 7.5 %all-to-all-start.1 = ((f32[8,20,128]{2,1,0:T(8,128)}), f32[8,20,128]{2,1,0:T(8,128)S(1)}, u32[]{:S(2)}, u32[]{:S(2)}) async-start(f32[8,20,128]{2,1,0:T(8,128)} %broadcast_in_dim.22), calls=%async_computation.1 | async-start | bytes 196608 | tf_op jit(solution)/shard_map/all_to_all | solution.py:484
  29.7 4.1 %collective-permute-start = (bf16[1,2048]{1,0:T(2,128)(2,1)S(1)}, bf16[1,2048]{1,0:T(2,128)(2,1)S(1)}, u32[]{:S(2)}, u32[]{:S(2)}) collective-permute-start(bf16[1,2048]{1,0:T(2,128)(2,1)S(1)} %fusion.7), channel_id=1, source_target_pairs={{6,8},{14,16},{22,24},{30,32},{38,40},{46,48},{54,56},{62,64},{70,... | collective-permute-start | bytes 12296 | tf_op jit(solution)/shard_map/ppermute | solution.py:536
  33.9 3.6 %collective-permute-done.halo_ref = bf16[1,2048]{1,0:T(2,128)(2,1)S(1)} collective-permute-done((bf16[1,2048]{1,0:T(2,128)(2,1)S(1)}, bf16[1,2048]{1,0:T(2,128)(2,1)S(1)}, u32[]{:S(2)}, u32[]{:S(2)}) %collective-permute-start) | collective-permute-done | bytes 4128 | tf_op jit(solution)/shard_map/ppermute | solution.py:536
  37.5 2.9 %collective-permute-start.1 = (bf16[40,2048]{1,0:T(8,128)(2,1)S(1)}, bf16[40,2048]{1,0:T(8,128)(2,1)S(1)}, u32[]{:S(2)}, u32[]{:S(2)}) collective-permute-start(bf16[40,2048]{1,0:T(8,128)(2,1)S(1)} %shard_map.163.blk0_ref), channel_id=1, source_target_pairs={{0,2},{2,4},{4,6},{6,0},{1,3},{3,5},{5,7},{7,1},{8,10},{10,12},{12... | collective-permute-start | bytes 491528 | tf_op jit(solution)/shard_map/ppermute | solution.py:550
  40.4 5.0 %collective-permute-start.2 = (bf16[40,2048]{1,0:T(8,128)(2,1)S(1)}, bf16[40,2048]{1,0:T(8,128)(2,1)S(1)}, u32[]{:S(2)}, u32[]{:S(2)}) collective-permute-start(bf16[40,2048]{1,0:T(8,128)(2,1)S(1)} %shard_map.163.blk0_ref), channel_id=1, source_target_pairs={{0,4},{2,6},{4,0},{6,2},{1,5},{3,7},{5,1},{7,3},{8,12},{10,14},{12... | collective-permute-start | bytes 491528 | tf_op jit(solution)/shard_map/ppermute | solution.py:550
  45.5 2.9 %collective-permute-start.3 = (bf16[40,2048]{1,0:T(8,128)(2,1)S(1)}, bf16[40,2048]{1,0:T(8,128)(2,1)S(1)}, u32[]{:S(2)}, u32[]{:S(2)}) collective-permute-start(bf16[40,2048]{1,0:T(8,128)(2,1)S(1)} %shard_map.163.blk0_ref), channel_id=1, source_target_pairs={{0,6},{2,0},{4,2},{6,4},{1,7},{3,1},{5,3},{7,5},{8,14},{10,8},{12,... | collective-permute-start | bytes 491528 | tf_op jit(solution)/shard_map/ppermute | solution.py:550
  48.5 0.7 pad_add_fusion.misc_ref
  49.2 0.1 pad_add_fusion.1.place_ref
  49.3 3.4 %collective-permute-done.3.blk3_ref = bf16[40,2048]{1,0:T(8,128)(2,1)S(1)} collective-permute-done((bf16[40,2048]{1,0:T(8,128)(2,1)S(1)}, bf16[40,2048]{1,0:T(8,128)(2,1)S(1)}, u32[]{:S(2)}, u32[]{:S(2)}) %collective-permute-start.3) | collective-permute-done | bytes 163872 | tf_op jit(solution)/shard_map/ppermute | solution.py:550
  52.7 0.0 copy-start.14
  52.7 4.2 %shard_map.164 = (bf16[64,24,128]{2,1,0:T(8,128)(2,1)}, bf16[144,2048]{1,0:T(8,128)(2,1)}, bf16[128,640]{1,0:T(8,128)(2,1)}, f32[128,256]{1,0:T(8,128)}, f32[8,2048]{1,0:T(8,128)}) custom-call(s32[3]{0:T(128)S(1)} %pad_add_fusion.1.place_ref, bf16[40,2048]{1,0:T(8,128)(2,1)S(1)} %shard_map.163.blk0_ref, ...), custom_call_target="tpu_custom_call" | custom-call | flops 100000000 | bytes 1048576 | tf_op jit(solution)/shard_map/pallas_call | solution.py:411
  56.9 0.0 copy-start.16
  56.9 0.0 copy-start.4
  57.0 10.5 %all-to-all-start.2 = ((bf16[64,24,128]{2,1,0:T(8,128)(2,1)}), bf16[64,24,128]{2,1,0:T(8,128)(2,1)S(1)}, u32[]{:S(2)}, u32[]{:S(2)}) async-start(bf16[64,24,128]{2,1,0:T(8,128)(2,1)} %get-tuple-element.13), calls=%async_computation.2 | async-start | bytes 786432 | tf_op jit(solution)/shard_map/all_to_all | solution.py:484
  67.4 1.9 %collective-permute-start.6 = (bf16[1024,512]{1,0:T(8,128)(2,1)}, bf16[1024,512]{1,0:T(8,128)(2,1)}, u32[]{:S(2)}, u32[]{:S(2)}) collective-permute-start(bf16[1024,512]{1,0:T(8,128)(2,1)} %own_z.1), channel_id=1, source_target_pairs={{0,1},{1,0},{2,3},{3,2},{4,5},{5,4},{6,7},{7,6},{8,9},{9,8},{10,11... | collective-permute-start | bytes 3145736 | tf_op jit(solution)/shard_map/ppermute | solution.py:480
  69.4 2.4 %collective-permute-start.7 = (bf16[256,2048]{1,0:T(8,128)(2,1)}, bf16[256,2048]{1,0:T(8,128)(2,1)}, u32[]{:S(2)}, u32[]{:S(2)}) collective-permute-start(bf16[256,2048]{1,0:T(8,128)(2,1)} %own_hbm.1), channel_id=1, source_target_pairs={{0,1},{1,0},{2,3},{3,2},{4,5},{5,4},{6,7},{7,6},{8,9},{9,8},{10,11... | collective-permute-start | bytes 3145736 | tf_op jit(solution)/shard_map/ppermute | solution.py:480
  71.8 0.2 fusion.11.rate_ref
  72.0 0.1 constant_dynamic-slice_fusion
  72.1 0.1 constant_dynamic-slice_fusion.1
  72.2 0.1 fusion.13.tap_ref
  72.2 9.9 %all-to-all-done.2.recv_ref = bf16[64,24,128]{2,1,0:T(8,128)(2,1)S(1)} async-done(((bf16[64,24,128]{2,1,0:T(8,128)(2,1)}), bf16[64,24,128]{2,1,0:T(8,128)(2,1)S(1)}, u32[]{:S(2)}, u32[]{:S(2)}) %all-to-all-start.2) | async-done | bytes 393248 | tf_op jit(solution)/shard_map/all_to_all | solution.py:484
  82.2 2.6 %shard_map.165 = bf16[64,16,128]{2,1,0:T(8,128)(2,1)} custom-call(f32[2]{0:T(128)S(1)} %fusion.11.rate_ref, bf16[64,24,128]{2,1,0:T(8,128)(2,1)S(1)} %all-to-all-done.2.recv_ref, f32[3,128]{1,0:T(4,128)S(1)} %fusion.13.tap_ref), custom_call_target="tpu_custom_call" | custom-call | flops 100000000 | bytes 1048576 | tf_op jit(solution)/shard_map/pallas_call | solution.py:442
  84.8 5.1 %all-to-all-start.3 = ((bf16[64,16,128]{2,1,0:T(8,128)(2,1)}), bf16[64,16,128]{2,1,0:T(8,128)(2,1)S(1)}, u32[]{:S(2)}, u32[]{:S(2)}) async-start(bf16[64,16,128]{2,1,0:T(8,128)(2,1)} %shard_map.165), calls=%async_computation.3 | async-start | bytes 524288 | tf_op jit(solution)/shard_map/all_to_all | solution.py:484
  89.9 1.1 copy-done.3
  91.0 2.2 %shard_map.166 = (f32[128,512]{1,0:T(8,128)S(1)}, bf16[128,128]{1,0:T(8,128)(2,1)S(1)}, bf16[128,512]{1,0:T(8,128)(2,1)S(1)}) custom-call(s32[3]{0:T(128)S(1)} %pad_add_fusion.1.place_ref, bf16[144,2048]{1,0:T(8,128)(2,1)S(1)} %copy-done.3, bf16[1024,512]{1,0:T(8,128)(2,1)S(1)} %copy-done.2, bf16[1024,512]{1,0:T(8,128)(2,1)} %collective-permute-done.6.other_z, ...), custom_call_target="tpu_custom_call" | custom-call | flops 100000000 | bytes 1048576 | tf_op jit(solution)/shard_map/pallas_call | solution.py:428
  93.2 0.7 copy-done.5
  93.9 9.0 %all-to-all-done.3.state_ref = bf16[64,16,128]{2,1,0:T(8,128)(2,1)S(1)} async-done(((bf16[64,16,128]{2,1,0:T(8,128)(2,1)}), bf16[64,16,128]{2,1,0:T(8,128)(2,1)S(1)}, u32[]{:S(2)}, u32[]{:S(2)}) %all-to-all-start.3) | async-done | bytes 262176 | tf_op jit(solution)/shard_map/all_to_all | solution.py:484
  102.9 2.7 %shard_map.167 = bf16[128,2048]{1,0:T(8,128)(2,1)S(1)} custom-call(s32[3]{0:T(128)S(1)} %pad_add_fusion.1.place_ref, bf16[64,16,128]{2,1,0:T(8,128)(2,1)S(1)} %all-to-all-done.3.state_ref, bf16[1,512]{1,0:T(2,128)(2,1)S(1)} %broadcast_in_dim.23.gain_ref, bf16[128,128]{1,0:T(8,128)(2,1)S(1)} %get-tuple-element.17.c_ref, f32[128,256]{1,0:T(8,128)S(1)} %copy-done.4, ...), custom_call_target="tpu_custom_call" | custom-call | flops 100000000 | bytes 1048576 | tf_op jit(solution)/shard_map/pallas_call | solution.py:452
  105.6 11.2 %all_to_all.25.tile_ref = bf16[4,32,2048]{2,1,0:T(8,128)(2,1)S(1)} all-to-all(bf16[4,32,2048]{2,1,0:T(8,128)(2,1)S(1)} %bitcast.27), channel_id=1, replica_groups=mesh['sp_0'=8,'sp_1'=8,'tp'=4,'dp'=2] {'tp'}, dimensions={0} | all-to-all | bytes 1048576 | tf_op jit(solution)/shard_map/all_to_all | solution.py:484
  116.8 0.7 shard_map.168
  (40 shorter events, 0.2 us)
Async XLA Ops:
  0.0 1.5 %copy-start = (bf16[3,32,512]{2,1,0:T(8,128)(2,1)S(1)}, bf16[3,32,512]{2,1,0:T(8,128)(2,1)}, u32[]{:S(2)}) copy-start(bf16[3,32,512]{2,1,0:T(8,128)(2,1)} %param.21) | copy-start | bytes 294916
  0.0 15.6 %copy-start.11 = (bf16[1024,128]{1,0:T(8,128)(2,1)S(1)}, bf16[1024,128]{1,0:T(8,128)(2,1)}, u32[]{:S(2)}) copy-start(bf16[1024,128]{1,0:T(8,128)(2,1)} %param.24) | copy-start | bytes 786436
  0.0 15.6 %copy-start.10 = (bf16[1024,128]{1,0:T(8,128)(2,1)S(1)}, bf16[1024,128]{1,0:T(8,128)(2,1)}, u32[]{:S(2)}) copy-start(bf16[1024,128]{1,0:T(8,128)(2,1)} %param.25) | copy-start | bytes 786436
  2.4 19.0 %all-to-all-start = ((f32[8,20,128]{2,1,0:T(8,128)}), f32[8,20,128]{2,1,0:T(8,128)S(1)}, u32[]{:S(2)}, u32[]{:S(2)}) async-start(f32[8,20,128]{2,1,0:T(8,128)} %broadcast_in_dim.21), calls=%async_computation | async-start | bytes 196608 | tf_op jit(solution)/shard_map/all_to_all | solution.py:484
  12.8 39.9 %collective-permute-start.4 = (bf16[1024,512]{1,0:T(8,128)(2,1)}, bf16[1024,512]{1,0:T(8,128)(2,1)}, u32[]{:S(2)}, u32[]{:S(2)}) collective-permute-start(bf16[1024,512]{1,0:T(8,128)(2,1)} %own_x.1), channel_id=1, source_target_pairs={{0,1},{1,0},{2,3},{3,2},{4,5},{5,4},{6,7},{7,6},{8,9},{9,8},{10,11... | collective-permute-start | bytes 3145736 | tf_op jit(solution)/shard_map/ppermute | solution.py:480
  15.6 14.1 %copy-start.6 = (bf16[1,32,2048]{2,1,0:T(8,128)(2,1)S(1)}, bf16[1,32,2048]{2,1,0:T(8,128)(2,1)}, u32[]{:S(2)}) copy-start(bf16[1,32,2048]{2,1,0:T(8,128)(2,1)} %param.17) | copy-start | bytes 393220
  15.6 18.2 %copy-start.15 = (bf16[2048]{0:T(1024)(128)(2,1)S(1)}, bf16[2048]{0:T(1024)(128)(2,1)}, u32[]{:S(2)}) copy-start(bf16[2048]{0:T(1024)(128)(2,1)} %param.22) | copy-start | bytes 12292
  15.7 32.8 %copy-start.12 = (bf16[3,512]{1,0:T(4,128)(2,1)S(1)}, bf16[3,512]{1,0:T(4,128)(2,1)}, u32[]{:S(2)}) copy-start(bf16[3,512]{1,0:T(4,128)(2,1)} %param.28) | copy-start | bytes 9220
  15.7 32.8 %copy-start.13 = (f32[2,8]{1,0:T(2,128)S(1)}, f32[2,8]{1,0:T(2,128)}, u32[]{:S(2)}) copy-start(f32[2,8]{1,0:T(2,128)} %param.31) | copy-start | bytes 196
  15.7 37.0 %copy-start.1 = (bf16[1024,512]{1,0:T(8,128)(2,1)S(1)}, bf16[1024,512]{1,0:T(8,128)(2,1)}, u32[]{:S(2)}) copy-start(bf16[1024,512]{1,0:T(8,128)(2,1)} %own_x.1) | copy-start | bytes 3145732
  15.7 37.0 %copy-start.9 = (bf16[1,8,2048]{2,1,0:T(8,128)(2,1)S(1)}, bf16[1,8,2048]{2,1,0:T(8,128)(2,1)}, u32[]{:S(2)}) copy-start(bf16[1,8,2048]{2,1,0:T(8,128)(2,1)} %param.19) | copy-start | bytes 98308
  15.8 36.9 %collective-permute-start.5 = (bf16[1024,384]{1,0:T(8,128)(2,1)S(1)}, bf16[1024,384]{1,0:T(8,128)(2,1)S(1)}, u32[]{:S(2)}, u32[]{:S(2)}) collective-permute-start(bf16[1024,384]{1,0:T(8,128)(2,1)S(1)} %fusion.3.own_s), channel_id=1, source_target_pairs={{0,1},{1,0},{2,3},{3,2},{4,5},{5,4},{6,7},{7,6},{8,9},{9,8},{10,11... | collective-permute-start | bytes 2359304 | tf_op jit(solution)/shard_map/ppermute | solution.py:480
  22.2 15.3 %all-to-all-start.1 = ((f32[8,20,128]{2,1,0:T(8,128)}), f32[8,20,128]{2,1,0:T(8,128)S(1)}, u32[]{:S(2)}, u32[]{:S(2)}) async-start(f32[8,20,128]{2,1,0:T(8,128)} %broadcast_in_dim.22), calls=%async_computation.1 | async-start | bytes 196608 | tf_op jit(solution)/shard_map/all_to_all | solution.py:484
  29.7 7.8 %collective-permute-start = (bf16[1,2048]{1,0:T(2,128)(2,1)S(1)}, bf16[1,2048]{1,0:T(2,128)(2,1)S(1)}, u32[]{:S(2)}, u32[]{:S(2)}) collective-permute-start(bf16[1,2048]{1,0:T(2,128)(2,1)S(1)} %fusion.7), channel_id=1, source_target_pairs={{6,8},{14,16},{22,24},{30,32},{38,40},{46,48},{54,56},{62,64},{70,... | collective-permute-start | bytes 12296 | tf_op jit(solution)/shard_map/ppermute | solution.py:536
  37.5 11.7 %collective-permute-start.1 = (bf16[40,2048]{1,0:T(8,128)(2,1)S(1)}, bf16[40,2048]{1,0:T(8,128)(2,1)S(1)}, u32[]{:S(2)}, u32[]{:S(2)}) collective-permute-start(bf16[40,2048]{1,0:T(8,128)(2,1)S(1)} %shard_map.163.blk0_ref), channel_id=1, source_target_pairs={{0,2},{2,4},{4,6},{6,0},{1,3},{3,5},{5,7},{7,1},{8,10},{10,12},{12... | collective-permute-start | bytes 491528 | tf_op jit(solution)/shard_map/ppermute | solution.py:550
  40.4 8.8 %collective-permute-start.2 = (bf16[40,2048]{1,0:T(8,128)(2,1)S(1)}, bf16[40,2048]{1,0:T(8,128)(2,1)S(1)}, u32[]{:S(2)}, u32[]{:S(2)}) collective-permute-start(bf16[40,2048]{1,0:T(8,128)(2,1)S(1)} %shard_map.163.blk0_ref), channel_id=1, source_target_pairs={{0,4},{2,6},{4,0},{6,2},{1,5},{3,7},{5,1},{7,3},{8,12},{10,14},{12... | collective-permute-start | bytes 491528 | tf_op jit(solution)/shard_map/ppermute | solution.py:550
  45.5 7.2 %collective-permute-start.3 = (bf16[40,2048]{1,0:T(8,128)(2,1)S(1)}, bf16[40,2048]{1,0:T(8,128)(2,1)S(1)}, u32[]{:S(2)}, u32[]{:S(2)}) collective-permute-start(bf16[40,2048]{1,0:T(8,128)(2,1)S(1)} %shard_map.163.blk0_ref), channel_id=1, source_target_pairs={{0,6},{2,0},{4,2},{6,4},{1,7},{3,1},{5,3},{7,5},{8,14},{10,8},{12,... | collective-permute-start | bytes 491528 | tf_op jit(solution)/shard_map/ppermute | solution.py:550
  52.7 19.3 %copy-start.14 = (bf16[3,128]{1,0:T(4,128)(2,1)S(1)}, bf16[3,128]{1,0:T(4,128)(2,1)}, u32[]{:S(2)}) copy-start(bf16[3,128]{1,0:T(4,128)(2,1)} %param.29) | copy-start | bytes 2308
  56.9 33.0 %copy-start.16 = (bf16[512]{0:T(512)(128)(2,1)S(1)}, bf16[512]{0:T(512)(128)(2,1)}, u32[]{:S(2)}) copy-start(bf16[512]{0:T(512)(128)(2,1)} %param.32) | copy-start | bytes 3076
  56.9 33.0 %copy-start.2 = (bf16[1024,512]{1,0:T(8,128)(2,1)S(1)}, bf16[1024,512]{1,0:T(8,128)(2,1)}, u32[]{:S(2)}) copy-start(bf16[1024,512]{1,0:T(8,128)(2,1)} %own_z.1) | copy-start | bytes 3145732
  56.9 33.0 %copy-start.4 = (f32[128,256]{1,0:T(8,128)S(1)}, f32[128,256]{1,0:T(8,128)}, u32[]{:S(2)}) copy-start(f32[128,256]{1,0:T(8,128)} %get-tuple-element.16.sr_ref) | copy-start | bytes 393220
  57.0 33.0 %copy-start.7 = (bf16[128,640]{1,0:T(8,128)(2,1)S(1)}, bf16[128,640]{1,0:T(8,128)(2,1)}, u32[]{:S(2)}) copy-start(bf16[128,640]{1,0:T(8,128)(2,1)} %get-tuple-element.15.xb_ref) | copy-start | bytes 491524
  57.0 25.2 %all-to-all-start.2 = ((bf16[64,24,128]{2,1,0:T(8,128)(2,1)}), bf16[64,24,128]{2,1,0:T(8,128)(2,1)S(1)}, u32[]{:S(2)}, u32[]{:S(2)}) async-start(bf16[64,24,128]{2,1,0:T(8,128)(2,1)} %get-tuple-element.13), calls=%async_computation.2 | async-start | bytes 786432 | tf_op jit(solution)/shard_map/all_to_all | solution.py:484
  67.4 22.5 %collective-permute-start.6 = (bf16[1024,512]{1,0:T(8,128)(2,1)}, bf16[1024,512]{1,0:T(8,128)(2,1)}, u32[]{:S(2)}, u32[]{:S(2)}) collective-permute-start(bf16[1024,512]{1,0:T(8,128)(2,1)} %own_z.1), channel_id=1, source_target_pairs={{0,1},{1,0},{2,3},{3,2},{4,5},{5,4},{6,7},{7,6},{8,9},{9,8},{10,11... | collective-permute-start | bytes 3145736 | tf_op jit(solution)/shard_map/ppermute | solution.py:480
  69.4 24.5 %collective-permute-start.7 = (bf16[256,2048]{1,0:T(8,128)(2,1)}, bf16[256,2048]{1,0:T(8,128)(2,1)}, u32[]{:S(2)}, u32[]{:S(2)}) collective-permute-start(bf16[256,2048]{1,0:T(8,128)(2,1)} %own_hbm.1), channel_id=1, source_target_pairs={{0,1},{1,0},{2,3},{3,2},{4,5},{5,4},{6,7},{7,6},{8,9},{9,8},{10,11... | collective-permute-start | bytes 3145736 | tf_op jit(solution)/shard_map/ppermute | solution.py:480
  84.8 18.1 %all-to-all-start.3 = ((bf16[64,16,128]{2,1,0:T(8,128)(2,1)}), bf16[64,16,128]{2,1,0:T(8,128)(2,1)S(1)}, u32[]{:S(2)}, u32[]{:S(2)}) async-start(bf16[64,16,128]{2,1,0:T(8,128)(2,1)} %shard_map.165), calls=%async_computation.3 | async-start | bytes 524288 | tf_op jit(solution)/shard_map/all_to_all | solution.py:484
  89.9 1.1 copy-start.3
  93.2 0.7 copy-start.5
  105.6 11.3 %copy-start.8 = (f32[8,2048]{1,0:T(8,128)S(1)}, f32[8,2048]{1,0:T(8,128)}, u32[]{:S(2)}) copy-start(f32[8,2048]{1,0:T(8,128)} %get-tuple-element.20.gate_ref) | copy-start | bytes 196612

commit v8 on v7

--- a/solution.py
+++ b/solution.py
@@ -288,20 +288,15 @@
     rate = jnp.where(left, rate_ref[0], rate_ref[1])
     decay = -(rate * step)
     high = rounded(decay)
-    mid = rounded(decay - high)
-    spot = lane % 4
-    parts = jnp.where(
-        spot == 0, high, jnp.where(spot == 1, mid, jnp.where(spot == 2, decay - high - mid, 0.0))
-    ).astype(bf16)
+    parts = jnp.concatenate([high.astype(bf16), (decay - high).astype(bf16)], axis=1)
     earlier = jnp.where(lanes((CTX, CTX)) < rows_of((CTX, CTX)), 1.0, 0.0).astype(bf16)
     sums = jnp.dot(earlier, parts, preferred_element_type=f32)
-    before_f = sums[:, 0:1] + sums[:, 1:2] + sums[:, 2:3]
-    before_b = sums[:, 64:65] + sums[:, 65:66] + sums[:, 66:67]
-    upto_f = before_f + decay[:, 0:1]
-    later_f = jnp.minimum(upto_f[CTX - 1 :] - upto_f, 0.0)
+    before = sums[:, :128] + sums[:, 128:]
+    upto = before + decay
+    later = jnp.minimum(upto[CTX - 1 :] - upto, 0.0)
     act_wide = act.astype(f32)
     moved = rounded(jnp.where(left, act_wide, pltpu.roll(act_wide, HD, 1)) * step)
-    moved = moved * jnp.exp(jnp.where(left, later_f, before_b))
+    moved = moved * jnp.exp(jnp.where(left, later, before))
     top = rounded(moved)
     dims = (((0,), (0,)), ((), ()))
     start = lax.dot_general(act, top.astype(bf16), dims, preferred_element_type=f32)

time: 119 us -> 118 us (level)
  no operation moved by 1% of the time
where the time goes in v8:
time: 118 us; the launch traced here: 117 us
  starting transfers between devices  57.2 us (48%)
  waiting for transfers between devices  29.1 us (25%)
  Pallas kernels  12.2 us (10%)
  blocking collectives  11.2 us (9%)
  local copies, waits for them, and re-layouts  4.45 us (4%)
  other arithmetic  2.52 us (2%)
    all_to_all x4, starting transfers between devices, exchanged(): return lax.all_to_all(x, axes, 0, 0, tiled=True)  33.4 us
    all_to_all x4, waiting for transfers between devices, exchanged(): return lax.all_to_all(x, axes, 0, 0, tiled=True)  22.1 us
    all_to_all x1, blocking collectives, exchanged(): return lax.all_to_all(x, axes, 0, 0, tiled=True)  11.2 us
    ppermute x3, starting transfers between devices, shards(): blocks.append(lax.ppermute(blocks[0], 'tp', turned(s)))  10.9 us
    ppermute x4, starting transfers between devices, swapped(): return lax.ppermute(x, 'dp', [(0, 1), (1, 0)])  8.78 us
    pallas_call x1, Pallas kernels, project_call(): call(project_kernel, [pltpu.HBM(*o) for o in outs], 11, (0,), [*(pltpu.VM...  4.17 us
    ppermute x1, starting transfers between devices, shards(): halo = lax.ppermute(edge, ALL, pairs)  4.12 us
    ppermute x1, waiting for transfers between devices, shards(): halo = lax.ppermute(edge, ALL, pairs)  3.61 us
  transfers between devices with their start and end apart: 12, of which 5 were waited for; matrix products, arithmetic and copies ran while one was open for 2% of the time, Pallas kernels for 4%

profile of v8, /device:TPU:8, one launch (start us, length us, event | category | flops | bytes accessed | tf_op | source)
XLA Modules:
  0.0 117.4 jit_solution(18376593191310817506)
XLA Ops:
  0.0 0.8 fusion.6
  0.8 0.7 fusion.8
  1.5 0.2 fusion.15
  1.8 0.6 broadcast_in_dim.21
  2.4 10.3 %all-to-all-start = ((f32[8,20,128]{2,1,0:T(8,128)}), f32[8,20,128]{2,1,0:T(8,128)S(1)}, u32[]{:S(2)}, u32[]{:S(2)}) async-start(f32[8,20,128]{2,1,0:T(8,128)} %broadcast_in_dim.21), calls=%async_computation | async-start | bytes 196608 | tf_op jit(solution)/shard_map/all_to_all | solution.py:479
  12.8 1.9 %collective-permute-start.4 = (bf16[1024,512]{1,0:T(8,128)(2,1)}, bf16[1024,512]{1,0:T(8,128)(2,1)}, u32[]{:S(2)}, u32[]{:S(2)}) collective-permute-start(bf16[1024,512]{1,0:T(8,128)(2,1)} %own_x.1), channel_id=1, source_target_pairs={{0,1},{1,0},{2,3},{3,2},{4,5},{5,4},{6,7},{7,6},{8,9},{9,8},{10,11... | collective-permute-start | bytes 3145736 | tf_op jit(solution)/shard_map/ppermute | solution.py:475
  14.7 0.7 slice_bitcast_fusion.1
  15.4 0.2 copy.23
  15.6 0.0 copy-start.6
  15.6 0.0 copy-start.15
  15.7 0.0 copy-start.12
  15.7 0.0 copy-start.13
  15.7 0.0 copy-start.1
  15.7 0.0 copy-start.9
  15.7 0.1 fusion.3.own_s
  15.8 2.5 %collective-permute-start.5 = (bf16[1024,384]{1,0:T(8,128)(2,1)S(1)}, bf16[1024,384]{1,0:T(8,128)(2,1)S(1)}, u32[]{:S(2)}, u32[]{:S(2)}) collective-permute-start(bf16[1024,384]{1,0:T(8,128)(2,1)S(1)} %fusion.3.own_s), channel_id=1, source_target_pairs={{0,1},{1,0},{2,3},{3,2},{4,5},{5,4},{6,7},{7,6},{8,9},{9,8},{10,11... | collective-permute-start | bytes 2359304 | tf_op jit(solution)/shard_map/ppermute | solution.py:475
  18.4 3.1 %all-to-all-done = f32[8,20,128]{2,1,0:T(8,128)S(1)} async-done(((f32[8,20,128]{2,1,0:T(8,128)}), f32[8,20,128]{2,1,0:T(8,128)S(1)}, u32[]{:S(2)}, u32[]{:S(2)}) %all-to-all-start) | async-done | bytes 81952 | tf_op jit(solution)/shard_map/all_to_all | solution.py:479
  21.5 0.6 broadcast_in_dim.22
  22.2 7.5 %all-to-all-start.1 = ((f32[8,20,128]{2,1,0:T(8,128)}), f32[8,20,128]{2,1,0:T(8,128)S(1)}, u32[]{:S(2)}, u32[]{:S(2)}) async-start(f32[8,20,128]{2,1,0:T(8,128)} %broadcast_in_dim.22), calls=%async_computation.1 | async-start | bytes 196608 | tf_op jit(solution)/shard_map/all_to_all | solution.py:479
  29.7 4.1 %collective-permute-start = (bf16[1,2048]{1,0:T(2,128)(2,1)S(1)}, bf16[1,2048]{1,0:T(2,128)(2,1)S(1)}, u32[]{:S(2)}, u32[]{:S(2)}) collective-permute-start(bf16[1,2048]{1,0:T(2,128)(2,1)S(1)} %fusion.7), channel_id=1, source_target_pairs={{6,8},{14,16},{22,24},{30,32},{38,40},{46,48},{54,56},{62,64},{70,... | collective-permute-start | bytes 12296 | tf_op jit(solution)/shard_map/ppermute | solution.py:531
  33.9 3.6 %collective-permute-done.halo_ref = bf16[1,2048]{1,0:T(2,128)(2,1)S(1)} collective-permute-done((bf16[1,2048]{1,0:T(2,128)(2,1)S(1)}, bf16[1,2048]{1,0:T(2,128)(2,1)S(1)}, u32[]{:S(2)}, u32[]{:S(2)}) %collective-permute-start) | collective-permute-done | bytes 4128 | tf_op jit(solution)/shard_map/ppermute | solution.py:531
  37.5 2.9 %collective-permute-start.1 = (bf16[40,2048]{1,0:T(8,128)(2,1)S(1)}, bf16[40,2048]{1,0:T(8,128)(2,1)S(1)}, u32[]{:S(2)}, u32[]{:S(2)}) collective-permute-start(bf16[40,2048]{1,0:T(8,128)(2,1)S(1)} %shard_map.163.blk0_ref), channel_id=1, source_target_pairs={{0,2},{2,4},{4,6},{6,0},{1,3},{3,5},{5,7},{7,1},{8,10},{10,12},{12... | collective-permute-start | bytes 491528 | tf_op jit(solution)/shard_map/ppermute | solution.py:545
  40.4 5.0 %collective-permute-start.2 = (bf16[40,2048]{1,0:T(8,128)(2,1)S(1)}, bf16[40,2048]{1,0:T(8,128)(2,1)S(1)}, u32[]{:S(2)}, u32[]{:S(2)}) collective-permute-start(bf16[40,2048]{1,0:T(8,128)(2,1)S(1)} %shard_map.163.blk0_ref), channel_id=1, source_target_pairs={{0,4},{2,6},{4,0},{6,2},{1,5},{3,7},{5,1},{7,3},{8,12},{10,14},{12... | collective-permute-start | bytes 491528 | tf_op jit(solution)/shard_map/ppermute | solution.py:545
  45.5 2.9 %collective-permute-start.3 = (bf16[40,2048]{1,0:T(8,128)(2,1)S(1)}, bf16[40,2048]{1,0:T(8,128)(2,1)S(1)}, u32[]{:S(2)}, u32[]{:S(2)}) collective-permute-start(bf16[40,2048]{1,0:T(8,128)(2,1)S(1)} %shard_map.163.blk0_ref), channel_id=1, source_target_pairs={{0,6},{2,0},{4,2},{6,4},{1,7},{3,1},{5,3},{7,5},{8,14},{10,8},{12,... | collective-permute-start | bytes 491528 | tf_op jit(solution)/shard_map/ppermute | solution.py:545
  48.5 0.7 pad_add_fusion.misc_ref
  49.2 0.1 pad_add_fusion.1.place_ref
  49.3 3.4 %collective-permute-done.3.blk3_ref = bf16[40,2048]{1,0:T(8,128)(2,1)S(1)} collective-permute-done((bf16[40,2048]{1,0:T(8,128)(2,1)S(1)}, bf16[40,2048]{1,0:T(8,128)(2,1)S(1)}, u32[]{:S(2)}, u32[]{:S(2)}) %collective-permute-start.3) | collective-permute-done | bytes 163872 | tf_op jit(solution)/shard_map/ppermute | solution.py:545
  52.7 0.0 copy-start.14
  52.7 4.2 %shard_map.164 = (bf16[64,24,128]{2,1,0:T(8,128)(2,1)}, bf16[144,2048]{1,0:T(8,128)(2,1)}, bf16[128,640]{1,0:T(8,128)(2,1)}, f32[128,256]{1,0:T(8,128)}, f32[8,2048]{1,0:T(8,128)}) custom-call(s32[3]{0:T(128)S(1)} %pad_add_fusion.1.place_ref, bf16[40,2048]{1,0:T(8,128)(2,1)S(1)} %shard_map.163.blk0_ref, ...), custom_call_target="tpu_custom_call" | custom-call | flops 100000000 | bytes 1048576 | tf_op jit(solution)/shard_map/pallas_call | solution.py:406
  56.9 0.0 copy-start.16
  56.9 0.0 copy-start.4
  57.0 10.5 %all-to-all-start.2 = ((bf16[64,24,128]{2,1,0:T(8,128)(2,1)}), bf16[64,24,128]{2,1,0:T(8,128)(2,1)S(1)}, u32[]{:S(2)}, u32[]{:S(2)}) async-start(bf16[64,24,128]{2,1,0:T(8,128)(2,1)} %get-tuple-element.13), calls=%async_computation.2 | async-start | bytes 786432 | tf_op jit(solution)/shard_map/all_to_all | solution.py:479
  67.4 1.9 %collective-permute-start.6 = (bf16[1024,512]{1,0:T(8,128)(2,1)}, bf16[1024,512]{1,0:T(8,128)(2,1)}, u32[]{:S(2)}, u32[]{:S(2)}) collective-permute-start(bf16[1024,512]{1,0:T(8,128)(2,1)} %own_z.1), channel_id=1, source_target_pairs={{0,1},{1,0},{2,3},{3,2},{4,5},{5,4},{6,7},{7,6},{8,9},{9,8},{10,11... | collective-permute-start | bytes 3145736 | tf_op jit(solution)/shard_map/ppermute | solution.py:475
  69.4 2.4 %collective-permute-start.7 = (bf16[256,2048]{1,0:T(8,128)(2,1)}, bf16[256,2048]{1,0:T(8,128)(2,1)}, u32[]{:S(2)}, u32[]{:S(2)}) collective-permute-start(bf16[256,2048]{1,0:T(8,128)(2,1)} %own_hbm.1), channel_id=1, source_target_pairs={{0,1},{1,0},{2,3},{3,2},{4,5},{5,4},{6,7},{7,6},{8,9},{9,8},{10,11... | collective-permute-start | bytes 3145736 | tf_op jit(solution)/shard_map/ppermute | solution.py:475
  71.8 0.2 fusion.11.rate_ref
  72.0 0.1 constant_dynamic-slice_fusion
  72.1 0.1 constant_dynamic-slice_fusion.1
  72.2 0.1 fusion.13.tap_ref
  72.2 9.9 %all-to-all-done.2.recv_ref = bf16[64,24,128]{2,1,0:T(8,128)(2,1)S(1)} async-done(((bf16[64,24,128]{2,1,0:T(8,128)(2,1)}), bf16[64,24,128]{2,1,0:T(8,128)(2,1)S(1)}, u32[]{:S(2)}, u32[]{:S(2)}) %all-to-all-start.2) | async-done | bytes 393248 | tf_op jit(solution)/shard_map/all_to_all | solution.py:479
  82.2 2.4 %shard_map.165 = bf16[64,16,128]{2,1,0:T(8,128)(2,1)} custom-call(f32[2]{0:T(128)S(1)} %fusion.11.rate_ref, bf16[64,24,128]{2,1,0:T(8,128)(2,1)S(1)} %all-to-all-done.2.recv_ref, f32[3,128]{1,0:T(4,128)S(1)} %fusion.13.tap_ref), custom_call_target="tpu_custom_call" | custom-call | flops 100000000 | bytes 1048576 | tf_op jit(solution)/shard_map/pallas_call | solution.py:437
  84.6 5.1 %all-to-all-start.3 = ((bf16[64,16,128]{2,1,0:T(8,128)(2,1)}), bf16[64,16,128]{2,1,0:T(8,128)(2,1)S(1)}, u32[]{:S(2)}, u32[]{:S(2)}) async-start(bf16[64,16,128]{2,1,0:T(8,128)(2,1)} %shard_map.165), calls=%async_computation.3 | async-start | bytes 524288 | tf_op jit(solution)/shard_map/all_to_all | solution.py:479
  89.7 1.1 copy-done.3
  90.8 2.2 %shard_map.166 = (f32[128,512]{1,0:T(8,128)S(1)}, bf16[128,128]{1,0:T(8,128)(2,1)S(1)}, bf16[128,512]{1,0:T(8,128)(2,1)S(1)}) custom-call(s32[3]{0:T(128)S(1)} %pad_add_fusion.1.place_ref, bf16[144,2048]{1,0:T(8,128)(2,1)S(1)} %copy-done.3, bf16[1024,512]{1,0:T(8,128)(2,1)S(1)} %copy-done.2, bf16[1024,512]{1,0:T(8,128)(2,1)} %collective-permute-done.6.other_z, ...), custom_call_target="tpu_custom_call" | custom-call | flops 100000000 | bytes 1048576 | tf_op jit(solution)/shard_map/pallas_call | solution.py:423
  93.0 0.7 copy-done.5
  93.7 9.0 %all-to-all-done.3.state_ref = bf16[64,16,128]{2,1,0:T(8,128)(2,1)S(1)} async-done(((bf16[64,16,128]{2,1,0:T(8,128)(2,1)}), bf16[64,16,128]{2,1,0:T(8,128)(2,1)S(1)}, u32[]{:S(2)}, u32[]{:S(2)}) %all-to-all-start.3) | async-done | bytes 262176 | tf_op jit(solution)/shard_map/all_to_all | solution.py:479
  102.7 2.7 %shard_map.167 = bf16[128,2048]{1,0:T(8,128)(2,1)S(1)} custom-call(s32[3]{0:T(128)S(1)} %pad_add_fusion.1.place_ref, bf16[64,16,128]{2,1,0:T(8,128)(2,1)S(1)} %all-to-all-done.3.state_ref, bf16[1,512]{1,0:T(2,128)(2,1)S(1)} %broadcast_in_dim.23.gain_ref, bf16[128,128]{1,0:T(8,128)(2,1)S(1)} %get-tuple-element.17.c_ref, f32[128,256]{1,0:T(8,128)S(1)} %copy-done.4, ...), custom_call_target="tpu_custom_call" | custom-call | flops 100000000 | bytes 1048576 | tf_op jit(solution)/shard_map/pallas_call | solution.py:447
  105.4 11.2 %all_to_all.25.tile_ref = bf16[4,32,2048]{2,1,0:T(8,128)(2,1)S(1)} all-to-all(bf16[4,32,2048]{2,1,0:T(8,128)(2,1)S(1)} %bitcast.27), channel_id=1, replica_groups=mesh['sp_0'=8,'sp_1'=8,'tp'=4,'dp'=2] {'tp'}, dimensions={0} | all-to-all | bytes 1048576 | tf_op jit(solution)/shard_map/all_to_all | solution.py:479
  116.6 0.7 shard_map.168
  (40 shorter events, 0.2 us)
Async XLA Ops:
  0.0 1.5 %copy-start = (bf16[3,32,512]{2,1,0:T(8,128)(2,1)S(1)}, bf16[3,32,512]{2,1,0:T(8,128)(2,1)}, u32[]{:S(2)}) copy-start(bf16[3,32,512]{2,1,0:T(8,128)(2,1)} %param.21) | copy-start | bytes 294916
  0.0 15.6 %copy-start.11 = (bf16[1024,128]{1,0:T(8,128)(2,1)S(1)}, bf16[1024,128]{1,0:T(8,128)(2,1)}, u32[]{:S(2)}) copy-start(bf16[1024,128]{1,0:T(8,128)(2,1)} %param.24) | copy-start | bytes 786436
  0.0 15.6 %copy-start.10 = (bf16[1024,128]{1,0:T(8,128)(2,1)S(1)}, bf16[1024,128]{1,0:T(8,128)(2,1)}, u32[]{:S(2)}) copy-start(bf16[1024,128]{1,0:T(8,128)(2,1)} %param.25) | copy-start | bytes 786436
  2.4 19.0 %all-to-all-start = ((f32[8,20,128]{2,1,0:T(8,128)}), f32[8,20,128]{2,1,0:T(8,128)S(1)}, u32[]{:S(2)}, u32[]{:S(2)}) async-start(f32[8,20,128]{2,1,0:T(8,128)} %broadcast_in_dim.21), calls=%async_computation | async-start | bytes 196608 | tf_op jit(solution)/shard_map/all_to_all | solution.py:479
  12.8 39.9 %collective-permute-start.4 = (bf16[1024,512]{1,0:T(8,128)(2,1)}, bf16[1024,512]{1,0:T(8,128)(2,1)}, u32[]{:S(2)}, u32[]{:S(2)}) collective-permute-start(bf16[1024,512]{1,0:T(8,128)(2,1)} %own_x.1), channel_id=1, source_target_pairs={{0,1},{1,0},{2,3},{3,2},{4,5},{5,4},{6,7},{7,6},{8,9},{9,8},{10,11... | collective-permute-start | bytes 3145736 | tf_op jit(solution)/shard_map/ppermute | solution.py:475
  15.6 14.1 %copy-start.6 = (bf16[1,32,2048]{2,1,0:T(8,128)(2,1)S(1)}, bf16[1,32,2048]{2,1,0:T(8,128)(2,1)}, u32[]{:S(2)}) copy-start(bf16[1,32,2048]{2,1,0:T(8,128)(2,1)} %param.17) | copy-start | bytes 393220
  15.6 18.2 %copy-start.15 = (bf16[2048]{0:T(1024)(128)(2,1)S(1)}, bf16[2048]{0:T(1024)(128)(2,1)}, u32[]{:S(2)}) copy-start(bf16[2048]{0:T(1024)(128)(2,1)} %param.22) | copy-start | bytes 12292
  15.7 32.8 %copy-start.12 = (bf16[3,512]{1,0:T(4,128)(2,1)S(1)}, bf16[3,512]{1,0:T(4,128)(2,1)}, u32[]{:S(2)}) copy-start(bf16[3,512]{1,0:T(4,128)(2,1)} %param.28) | copy-start | bytes 9220
  15.7 32.8 %copy-start.13 = (f32[2,8]{1,0:T(2,128)S(1)}, f32[2,8]{1,0:T(2,128)}, u32[]{:S(2)}) copy-start(f32[2,8]{1,0:T(2,128)} %param.31) | copy-start | bytes 196
  15.7 37.0 %copy-start.1 = (bf16[1024,512]{1,0:T(8,128)(2,1)S(1)}, bf16[1024,512]{1,0:T(8,128)(2,1)}, u32[]{:S(2)}) copy-start(bf16[1024,512]{1,0:T(8,128)(2,1)} %own_x.1) | copy-start | bytes 3145732
  15.7 37.0 %copy-start.9 = (bf16[1,8,2048]{2,1,0:T(8,128)(2,1)S(1)}, bf16[1,8,2048]{2,1,0:T(8,128)(2,1)}, u32[]{:S(2)}) copy-start(bf16[1,8,2048]{2,1,0:T(8,128)(2,1)} %param.19) | copy-start | bytes 98308
  15.8 36.9 %collective-permute-start.5 = (bf16[1024,384]{1,0:T(8,128)(2,1)S(1)}, bf16[1024,384]{1,0:T(8,128)(2,1)S(1)}, u32[]{:S(2)}, u32[]{:S(2)}) collective-permute-start(bf16[1024,384]{1,0:T(8,128)(2,1)S(1)} %fusion.3.own_s), channel_id=1, source_target_pairs={{0,1},{1,0},{2,3},{3,2},{4,5},{5,4},{6,7},{7,6},{8,9},{9,8},{10,11... | collective-permute-start | bytes 2359304 | tf_op jit(solution)/shard_map/ppermute | solution.py:475
  22.2 15.3 %all-to-all-start.1 = ((f32[8,20,128]{2,1,0:T(8,128)}), f32[8,20,128]{2,1,0:T(8,128)S(1)}, u32[]{:S(2)}, u32[]{:S(2)}) async-start(f32[8,20,128]{2,1,0:T(8,128)} %broadcast_in_dim.22), calls=%async_computation.1 | async-start | bytes 196608 | tf_op jit(solution)/shard_map/all_to_all | solution.py:479
  29.7 7.8 %collective-permute-start = (bf16[1,2048]{1,0:T(2,128)(2,1)S(1)}, bf16[1,2048]{1,0:T(2,128)(2,1)S(1)}, u32[]{:S(2)}, u32[]{:S(2)}) collective-permute-start(bf16[1,2048]{1,0:T(2,128)(2,1)S(1)} %fusion.7), channel_id=1, source_target_pairs={{6,8},{14,16},{22,24},{30,32},{38,40},{46,48},{54,56},{62,64},{70,... | collective-permute-start | bytes 12296 | tf_op jit(solution)/shard_map/ppermute | solution.py:531
  37.5 11.7 %collective-permute-start.1 = (bf16[40,2048]{1,0:T(8,128)(2,1)S(1)}, bf16[40,2048]{1,0:T(8,128)(2,1)S(1)}, u32[]{:S(2)}, u32[]{:S(2)}) collective-permute-start(bf16[40,2048]{1,0:T(8,128)(2,1)S(1)} %shard_map.163.blk0_ref), channel_id=1, source_target_pairs={{0,2},{2,4},{4,6},{6,0},{1,3},{3,5},{5,7},{7,1},{8,10},{10,12},{12... | collective-permute-start | bytes 491528 | tf_op jit(solution)/shard_map/ppermute | solution.py:545
  40.4 8.8 %collective-permute-start.2 = (bf16[40,2048]{1,0:T(8,128)(2,1)S(1)}, bf16[40,2048]{1,0:T(8,128)(2,1)S(1)}, u32[]{:S(2)}, u32[]{:S(2)}) collective-permute-start(bf16[40,2048]{1,0:T(8,128)(2,1)S(1)} %shard_map.163.blk0_ref), channel_id=1, source_target_pairs={{0,4},{2,6},{4,0},{6,2},{1,5},{3,7},{5,1},{7,3},{8,12},{10,14},{12... | collective-permute-start | bytes 491528 | tf_op jit(solution)/shard_map/ppermute | solution.py:545
  45.5 7.2 %collective-permute-start.3 = (bf16[40,2048]{1,0:T(8,128)(2,1)S(1)}, bf16[40,2048]{1,0:T(8,128)(2,1)S(1)}, u32[]{:S(2)}, u32[]{:S(2)}) collective-permute-start(bf16[40,2048]{1,0:T(8,128)(2,1)S(1)} %shard_map.163.blk0_ref), channel_id=1, source_target_pairs={{0,6},{2,0},{4,2},{6,4},{1,7},{3,1},{5,3},{7,5},{8,14},{10,8},{12,... | collective-permute-start | bytes 491528 | tf_op jit(solution)/shard_map/ppermute | solution.py:545
  52.7 19.3 %copy-start.14 = (bf16[3,128]{1,0:T(4,128)(2,1)S(1)}, bf16[3,128]{1,0:T(4,128)(2,1)}, u32[]{:S(2)}) copy-start(bf16[3,128]{1,0:T(4,128)(2,1)} %param.29) | copy-start | bytes 2308
  56.9 32.7 %copy-start.16 = (bf16[512]{0:T(512)(128)(2,1)S(1)}, bf16[512]{0:T(512)(128)(2,1)}, u32[]{:S(2)}) copy-start(bf16[512]{0:T(512)(128)(2,1)} %param.32) | copy-start | bytes 3076
  56.9 32.7 %copy-start.2 = (bf16[1024,512]{1,0:T(8,128)(2,1)S(1)}, bf16[1024,512]{1,0:T(8,128)(2,1)}, u32[]{:S(2)}) copy-start(bf16[1024,512]{1,0:T(8,128)(2,1)} %own_z.1) | copy-start | bytes 3145732
  56.9 32.7 %copy-start.4 = (f32[128,256]{1,0:T(8,128)S(1)}, f32[128,256]{1,0:T(8,128)}, u32[]{:S(2)}) copy-start(f32[128,256]{1,0:T(8,128)} %get-tuple-element.16.sr_ref) | copy-start | bytes 393220
  57.0 32.7 %copy-start.7 = (bf16[128,640]{1,0:T(8,128)(2,1)S(1)}, bf16[128,640]{1,0:T(8,128)(2,1)}, u32[]{:S(2)}) copy-start(bf16[128,640]{1,0:T(8,128)(2,1)} %get-tuple-element.15.xb_ref) | copy-start | bytes 491524
  57.0 25.2 %all-to-all-start.2 = ((bf16[64,24,128]{2,1,0:T(8,128)(2,1)}), bf16[64,24,128]{2,1,0:T(8,128)(2,1)S(1)}, u32[]{:S(2)}, u32[]{:S(2)}) async-start(bf16[64,24,128]{2,1,0:T(8,128)(2,1)} %get-tuple-element.13), calls=%async_computation.2 | async-start | bytes 786432 | tf_op jit(solution)/shard_map/all_to_all | solution.py:479
  67.4 22.2 %collective-permute-start.6 = (bf16[1024,512]{1,0:T(8,128)(2,1)}, bf16[1024,512]{1,0:T(8,128)(2,1)}, u32[]{:S(2)}, u32[]{:S(2)}) collective-permute-start(bf16[1024,512]{1,0:T(8,128)(2,1)} %own_z.1), channel_id=1, source_target_pairs={{0,1},{1,0},{2,3},{3,2},{4,5},{5,4},{6,7},{7,6},{8,9},{9,8},{10,11... | collective-permute-start | bytes 3145736 | tf_op jit(solution)/shard_map/ppermute | solution.py:475
  69.4 24.3 %collective-permute-start.7 = (bf16[256,2048]{1,0:T(8,128)(2,1)}, bf16[256,2048]{1,0:T(8,128)(2,1)}, u32[]{:S(2)}, u32[]{:S(2)}) collective-permute-start(bf16[256,2048]{1,0:T(8,128)(2,1)} %own_hbm.1), channel_id=1, source_target_pairs={{0,1},{1,0},{2,3},{3,2},{4,5},{5,4},{6,7},{7,6},{8,9},{9,8},{10,11... | collective-permute-start | bytes 3145736 | tf_op jit(solution)/shard_map/ppermute | solution.py:475
  84.6 18.1 %all-to-all-start.3 = ((bf16[64,16,128]{2,1,0:T(8,128)(2,1)}), bf16[64,16,128]{2,1,0:T(8,128)(2,1)S(1)}, u32[]{:S(2)}, u32[]{:S(2)}) async-start(bf16[64,16,128]{2,1,0:T(8,128)(2,1)} %shard_map.165), calls=%async_computation.3 | async-start | bytes 524288 | tf_op jit(solution)/shard_map/all_to_all | solution.py:479
  89.7 1.1 copy-start.3
  93.0 0.7 copy-start.5
  105.4 11.3 %copy-start.8 = (f32[8,2048]{1,0:T(8,128)S(1)}, f32[8,2048]{1,0:T(8,128)}, u32[]{:S(2)}) copy-start(f32[8,2048]{1,0:T(8,128)} %get-tuple-element.20.gate_ref) | copy-start | bytes 196612
